TPU v7x, 32 devices: a whole 2x2x4 slice. The times are simulated.
32 devices in a mesh: fs: 16 (over z, y, x), tp: 2 (over core).
Axes of the slice: x: 2, y: 2, z: 4, core: 2. Of those that a mesh axis runs over, the one named last changes fastest.
Arguments:
- saved_inputs: bfloat16 [12288, 2048], P('fs'), may hold values from -8 to 8
- input_cot: bfloat16 [12288, 2048], P('fs', 'tp'), may hold values from -0.0546875 to 0.0546875
- gate_cot: bfloat16 [12288, 2048], P('fs', 'tp'), may hold values from -0.0546875 to 0.0546875
- input_master: float32 [2048, 2048], P('fs', 'tp'), may hold values from -6 to 6
- gate_master: float32 [2048, 2048], P('fs', 'tp'), may hold values from -6 to 6
- input_factor: bfloat16 [2048, 256], P('fs'), may hold values from -2 to 2
- gate_factor: bfloat16 [2048, 256], P('fs'), may hold values from -2 to 2
- input_first: float32 [256, 2048], P('fs', 'tp'), may hold values from -6 to 6
- input_second: float32 [256, 2048], P('fs', 'tp'), may hold values from 0.2 to 17
- gate_first: float32 [256, 2048], P('fs', 'tp'), may hold values from -6 to 6
- gate_second: float32 [256, 2048], P('fs', 'tp'), may hold values from 0.2 to 17
Outputs:
- input_step: float32 [2048, 2048], P('fs', 'tp')
- gate_step: float32 [2048, 2048], P('fs', 'tp')
- input_first_new: float32 [256, 2048], P('fs', 'tp')
- input_second_new: float32 [256, 2048], P('fs', 'tp')
- gate_first_new: float32 [256, 2048], P('fs', 'tp')
- gate_second_new: float32 [256, 2048], P('fs', 'tp')
- input_copy: bfloat16 [2048, 2048], P(None, 'tp')
- gate_copy: bfloat16 [2048, 2048], P(None, 'tp')
All inputs are finite; a program needn't handle non-finite values.
Results may differ from a plain program's by a relative error of at most 0.0004.
Values may be sent and summed in bfloat16 or wider, within the bound.
No kernel may reach another device: no remote copies, remote signals or barrier semaphores. Data moves between devices by JAX's collectives and lax.ppermute only.
A program may use at most 64 MiB of HBM per device.

v0:
```python
import jax
import jax.numpy as jnp
from jax import lax
from jax.sharding import PartitionSpec as P

D = 2048
W = 2048


first_decay = 0.9
second_decay = 0.9
ratio_floor = 1e-08
mean_floor = 1e-06
step_size = 0.05


def moments(low_rank, first, second):
    first_new = first_decay * first + (1.0 - first_decay) * low_rank
    second_new = second_decay * second + (1.0 - second_decay) * low_rank * low_rank
    ratio = first_new / (jnp.sqrt(second_new) + ratio_floor)
    return (first_new, second_new, ratio)


def local(
    saved_inputs,
    input_cot,
    gate_cot,
    input_master,
    gate_master,
    input_factor,
    gate_factor,
    input_first,
    input_second,
    gate_first,
    gate_second,
):
    col_width = input_cot.shape[1]
    contract = (((0,), (0,)), ((), ()))
    factor_in = input_factor.astype(jnp.float32)
    factor_gate = gate_factor.astype(jnp.float32)
    whole_in, whole_gate = (
        lax.all_gather(input_factor, "fs", axis=0, tiled=True),
        lax.all_gather(gate_factor, "fs", axis=0, tiled=True),
    )
    partial_in = lax.dot_general(
        saved_inputs, input_cot, contract, preferred_element_type=jnp.float32
    )
    partial_gate = lax.dot_general(
        saved_inputs, gate_cot, contract, preferred_element_type=jnp.float32
    )
    cols_in = whole_in.astype(jnp.float32)
    cols_gate = whole_gate.astype(jnp.float32)
    term_in = lax.dot_general(cols_in, partial_in, contract, precision=lax.Precision.HIGHEST)
    term_gate = lax.dot_general(cols_gate, partial_gate, contract, precision=lax.Precision.HIGHEST)
    summed = lax.psum_scatter(
        jnp.concatenate([term_in, term_gate], axis=1), "fs", scatter_dimension=0, tiled=True
    )
    low_in = summed[:, :col_width]
    low_gate = summed[:, col_width:]
    first_in, second_in, ratio_in = moments(low_in, input_first, input_second)
    first_gate, second_gate, ratio_gate = moments(low_gate, gate_first, gate_second)
    piece_in = lax.all_gather(ratio_in, "fs", axis=0, tiled=True)
    piece_gate = lax.all_gather(ratio_gate, "fs", axis=0, tiled=True)
    cols_in = factor_in
    cols_gate = factor_gate
    dir_in = jnp.dot(cols_in, piece_in, precision=lax.Precision.HIGHEST)
    dir_gate = jnp.dot(cols_gate, piece_gate, precision=lax.Precision.HIGHEST)
    square_in, square_gate = lax.psum(
        (jnp.sum(dir_in * dir_in), jnp.sum(dir_gate * dir_gate)), ("fs", "tp")
    )
    step_in = dir_in * lax.rsqrt(square_in / (D * W) + mean_floor)
    step_gate = dir_gate * lax.rsqrt(square_gate / (D * W) + mean_floor)
    local_in = (input_master - step_size * step_in).astype(jnp.bfloat16)
    local_gate = (gate_master - step_size * step_gate).astype(jnp.bfloat16)
    copy_in, copy_gate = (
        lax.all_gather(local_in, "fs", axis=0, tiled=True),
        lax.all_gather(local_gate, "fs", axis=0, tiled=True),
    )
    return (step_in, step_gate, first_in, second_in, first_gate, second_gate, copy_in, copy_gate)


def solution(mesh):
    return jax.shard_map(
        local,
        mesh=mesh,
        in_specs=(
            P("fs", None),
            P("fs", "tp"),
            P("fs", "tp"),
            P("fs", "tp"),
            P("fs", "tp"),
            P("fs", None),
            P("fs", None),
            P("fs", "tp"),
            P("fs", "tp"),
            P("fs", "tp"),
            P("fs", "tp"),
        ),
        out_specs=(
            P("fs", "tp"),
            P("fs", "tp"),
            P("fs", "tp"),
            P("fs", "tp"),
            P("fs", "tp"),
            P("fs", "tp"),
            P(None, "tp"),
            P(None, "tp"),
        ),
        check_vma=False,
    )
```

profile of v0, /device:TPU:0, one launch (start us, length us, event | category | flops | bytes accessed | tf_op | source)
XLA Modules:
  0.0 569.3 jit_solution(10387800890137530023)
XLA Ops:
  7.2 0.0 copy-start
  7.2 0.0 all-gather.7.cloned.1.call-start
  7.2 0.7 all-gather.7.cloned.1.call-update
  7.9 0.0 all-gather.9.cloned.1.call-start
  8.0 0.7 all-gather.9.cloned.1.call-update
  8.7 0.0 reduce-scatter.4.cloned.1.call-start
  8.7 0.3 copy-done
  9.1 7.2 %fusion.4 = f32[2048,1024]{1,0:T(8,128)} fusion(bf16[768,2048]{1,0:T(8,128)(2,1)S(1)} %copy-done, bf16[768,1024]{1,0:T(8,128)(2,1)} %param.12), kind=kOutput, calls=%fused_computation.17 | convolution fusion | flops 3221225472 | bytes 13107200 | tf_op jit(solution)/shard_map/dot_general | solution.py:45
  16.2 0.0 copy-done.8
  16.2 5.7 %fusion.5 = f32[2048,1024]{1,0:T(8,128)} fusion(bf16[768,2048]{1,0:T(8,128)(2,1)S(1)} %copy-done, bf16[768,1024]{1,0:T(8,128)(2,1)S(1)} %copy-done.8), kind=kOutput, calls=%fused_computation.18 | convolution fusion | flops 3221225472 | bytes 13107200 | tf_op jit(solution)/shard_map/dot_general | solution.py:48
  21.9 46.7 %all-gather.7.cloned.1.call-done = bf16[2048,256]{1,0:T(8,128)(2,1)} async-done(((bf16[128,256]{1,0:T(8,128)(2,1)}), bf16[2048,256]{1,0:T(8,128)(2,1)}) %all-gather.7.cloned.1.call-update) | async-done | bytes 1048592 | tf_op jit(solution)/shard_map/all_gather | solution.py:42
  68.6 11.2 %convolution_bitcast_fusion.1 = f32[256,1024]{0,1:T(8,128)} fusion(f32[2048,1024]{1,0:T(8,128)} %fusion.4, bf16[2048,256]{1,0:T(8,128)(2,1)} %all-gather.7.cloned.1.call-done), kind=kOutput, calls=%fused_computation.2 | convolution fusion | flops 6442450944 | bytes 10485760 | tf_op jit(solution)/shard_map/dot_general | solution.py:53
  79.8 45.5 %all-gather.9.cloned.1.call-done = bf16[2048,256]{1,0:T(8,128)(2,1)} async-done(((bf16[128,256]{1,0:T(8,128)(2,1)}), bf16[2048,256]{1,0:T(8,128)(2,1)}) %all-gather.9.cloned.1.call-update) | async-done | bytes 1048592 | tf_op jit(solution)/shard_map/all_gather | solution.py:43
  125.3 9.5 %convolution_bitcast_fusion = f32[256,1024]{0,1:T(8,128)S(1)} fusion(f32[2048,1024]{1,0:T(8,128)} %fusion.5, bf16[2048,256]{1,0:T(8,128)(2,1)} %all-gather.9.cloned.1.call-done), kind=kOutput, calls=%fused_computation.1 | convolution fusion | flops 6442450944 | bytes 10485760 | tf_op jit(solution)/shard_map/dot_general | solution.py:54
  134.8 0.0 copy-done.1
  134.8 1.5 pad_maximum_fusion
  136.2 0.0 copy-start.2
  136.3 2.9 copy.65
  139.2 0.0 reduce-scatter.4.cloned.1.call-update
  139.2 0.0 all-gather.13.cloned.1.call-start
  139.3 80.6 %reduce-scatter.4.cloned.1.call-done = f32[16,2048]{1,0:T(8,128)} async-done(((f32[256,2048]{1,0:T(8,128)}), f32[16,2048]{1,0:T(8,128)}) %reduce-scatter.4.cloned.1.call-update) | async-done | bytes 131088 | tf_op jit(solution)/shard_map/reduce_scatter | solution.py:55
  219.9 0.0 copy-done.4
  219.9 0.0 copy-done.5
  219.9 0.0 copy-done.7
  219.9 1.6 add_divide_fusion
  221.5 0.0 all-gather.13.cloned.1.call-update
  221.5 0.0 all-gather.11.cloned.1.call-start
  221.6 0.5 all-gather.11.cloned.1.call-update
  222.1 0.0 all-gather.15.cloned.1.call-start
  222.2 2.0 copy.59
  224.2 50.4 %all-gather.13.cloned.1.call-done = f32[256,1024]{1,0:T(8,128)} async-done(((f32[16,1024]{1,0:T(8,128)}), f32[256,1024]{1,0:T(8,128)}) %all-gather.13.cloned.1.call-update) | async-done | bytes 1048592 | tf_op jit(solution)/shard_map/all_gather | solution.py:63
  274.6 0.0 copy-done.2
  274.6 3.7 multiply_reduce_fusion
  278.3 53.4 %all-gather.11.cloned.1.call-done = f32[256,1024]{1,0:T(8,128)} async-done(((f32[16,1024]{1,0:T(8,128)}), f32[256,1024]{1,0:T(8,128)}) %all-gather.11.cloned.1.call-update) | async-done | bytes 1048592 | tf_op jit(solution)/shard_map/all_gather | solution.py:62
  331.7 3.6 multiply_reduce_fusion.1
  335.4 38.6 %all-reduce = (f32[]{:T(128)}, f32[]{:T(128)}) all-reduce(f32[]{:T(128)} %get-tuple-element.47, f32[]{:T(128)} %get-tuple-element.49), channel_id=1, replica_groups=mesh['fs'=16,'tp'=2] {'fs','tp'}, use_global_device_ids=true, to_apply=%region_2.0 | all-reduce | flops 2 | bytes 16 | tf_op jit(solution)/shard_map/psum | solution.py:68
  374.7 2.2 subtract_convert_fusion.1
  376.8 0.0 all-gather.15.cloned.1.call-update
  376.9 0.0 all-gather.17.cloned.1.call-start
  376.9 2.0 copy.60
  379.7 2.2 subtract_convert_fusion
  381.8 0.0 all-gather.17.cloned.1.call-update
  381.9 2.0 copy.61
  383.9 2.0 copy.62
  385.9 80.5 %all-gather.15.cloned.1.call-done = bf16[2048,1024]{0,1:T(8,128)(2,1)} async-done(((bf16[128,1024]{0,1:T(8,128)(2,1)}), bf16[2048,1024]{0,1:T(8,128)(2,1)}) %all-gather.15.cloned.1.call-update) | async-done | bytes 4194320 | tf_op jit(solution)/shard_map/all_gather | solution.py:76
  466.4 6.4 %copy.63 = bf16[2048,1024]{1,0:T(8,128)(2,1)} copy(bf16[2048,1024]{0,1:T(8,128)(2,1)} %all-gather.15.cloned.1.call-done) | data formatting | bytes 8388608
  472.8 83.2 %all-gather.17.cloned.1.call-done = bf16[2048,1024]{0,1:T(8,128)(2,1)} async-done(((bf16[128,1024]{0,1:T(8,128)(2,1)}), bf16[2048,1024]{0,1:T(8,128)(2,1)}) %all-gather.17.cloned.1.call-update) | async-done | bytes 4194320 | tf_op jit(solution)/shard_map/all_gather | solution.py:77
  556.0 6.4 %copy.64 = bf16[2048,1024]{1,0:T(8,128)(2,1)} copy(bf16[2048,1024]{0,1:T(8,128)(2,1)} %all-gather.17.cloned.1.call-done) | data formatting | bytes 8388608
  (9 shorter events, 0.0 us)
Async XLA Ops:
  7.2 1.9 copy-start
  7.2 61.4 %all-gather.7.cloned.1.call-start = ((), (), s32[]{:S(2)}) async-start(), calls=%async_computation.1 | async-start | bytes 1114112 | tf_op jit(solution)/shard_map/all_gather | solution.py:42
  7.9 117.4 %all-gather.9.cloned.1.call-start = ((), (), s32[]{:S(2)}) async-start(), calls=%async_computation.2 | async-start | bytes 1114112 | tf_op jit(solution)/shard_map/all_gather | solution.py:43
  8.7 211.2 %reduce-scatter.4.cloned.1.call-start = ((), (), s32[]{:S(2)}) async-start(), calls=%async_computation.7 | async-start | bytes 2228224 | tf_op jit(solution)/shard_map/reduce_scatter | solution.py:55
  9.1 7.2 %copy-start.8 = (bf16[768,1024]{1,0:T(8,128)(2,1)S(1)}, bf16[768,1024]{1,0:T(8,128)(2,1)}, u32[]{:S(2)}) copy-start(bf16[768,1024]{1,0:T(8,128)(2,1)} %param.13) | copy-start | bytes 4718596
  125.3 9.5 %copy-start.1 = (f32[256,1024]{0,1:T(8,128)S(1)}, f32[256,1024]{0,1:T(8,128)}, u32[]{:S(2)}) copy-start(f32[256,1024]{0,1:T(8,128)} %convolution_bitcast_fusion.1) | copy-start | bytes 3145732
  136.2 83.6 %copy-start.4 = (f32[16,1024]{1,0:T(8,128)S(1)}, f32[16,1024]{1,0:T(8,128)}, u32[]{:S(2)}) copy-start(f32[16,1024]{1,0:T(8,128)} %param.21) | copy-start | bytes 196612
  136.2 83.6 %copy-start.5 = (f32[16,1024]{1,0:T(8,128)S(1)}, f32[16,1024]{1,0:T(8,128)}, u32[]{:S(2)}) copy-start(f32[16,1024]{1,0:T(8,128)} %param.20) | copy-start | bytes 196612
  136.2 83.6 %copy-start.6 = (f32[16,1024]{1,0:T(8,128)S(1)}, f32[16,1024]{1,0:T(8,128)}, u32[]{:S(2)}) copy-start(f32[16,1024]{1,0:T(8,128)} %param.19) | copy-start | bytes 196612
  136.2 83.6 %copy-start.7 = (f32[16,1024]{1,0:T(8,128)S(1)}, f32[16,1024]{1,0:T(8,128)}, u32[]{:S(2)}) copy-start(f32[16,1024]{1,0:T(8,128)} %param.18) | copy-start | bytes 196612
  136.2 138.3 %copy-start.2 = (bf16[128,256]{1,0:T(8,128)(2,1)S(1)}, bf16[128,256]{1,0:T(8,128)(2,1)}, u32[]{:S(2)}) copy-start(bf16[128,256]{1,0:T(8,128)(2,1)} %param.17) | copy-start | bytes 196612
  139.2 192.5 %copy-start.3 = (bf16[128,256]{1,0:T(8,128)(2,1)S(1)}, bf16[128,256]{1,0:T(8,128)(2,1)}, u32[]{:S(2)}) copy-start(bf16[128,256]{1,0:T(8,128)(2,1)} %param.16) | copy-start | bytes 196612
  139.2 135.4 %all-gather.13.cloned.1.call-start = ((), (), s32[]{:S(2)}) async-start(), calls=%async_computation.4 | async-start | bytes 1114112 | tf_op jit(solution)/shard_map/all_gather | solution.py:63
  221.5 110.2 %all-gather.11.cloned.1.call-start = ((), (), s32[]{:S(2)}) async-start(), calls=%async_computation.3 | async-start | bytes 1114112 | tf_op jit(solution)/shard_map/all_gather | solution.py:62
  222.1 244.3 %all-gather.15.cloned.1.call-start = ((), (), s32[]{:S(2)}) async-start(), calls=%async_computation.5 | async-start | bytes 4456448 | tf_op jit(solution)/shard_map/all_gather | solution.py:76
  376.9 179.2 %all-gather.17.cloned.1.call-start = ((), (), s32[]{:S(2)}) async-start(), calls=%async_computation.6 | async-start | bytes 4456448 | tf_op jit(solution)/shard_map/all_gather | solution.py:77
Sparse Core Ops, SparseCore 0:
  10.7 57.7 all-gather.6
  71.3 53.9 all-gather.8
  139.3 80.4 reduce-scatter.3
  223.0 51.4 all-gather.12
  277.8 53.9 all-gather.10
  377.0 89.3 all-gather.14
  469.1 86.8 all-gather.16
where the time goes:
time: 570 us; the launch traced here: 569 us
  waiting for transfers between devices  442 us (78%)
  matrix products  40.9 us (7%)
  blocking collectives  38.6 us (7%)
  local copies, waits for them, and re-layouts  24.3 us (4%)
  between operations  15.6 us (3%)
  other arithmetic  7.42 us (1%)
    all_gather x1, waiting for transfers between devices, local(): lax.all_gather(local_gate, 'fs', axis=0, tiled=True)  83.2 us
    reduce_scatter x1, waiting for transfers between devices, local(): lax.psum_scatter(jnp.concatenate([term_in, term_gate], axis=1), 'fs', sca...  80.6 us
    all_gather x1, waiting for transfers between devices, local(): lax.all_gather(local_in, 'fs', axis=0, tiled=True)  80.5 us
    all_gather x1, waiting for transfers between devices, local(): piece_in = lax.all_gather(ratio_in, 'fs', axis=0, tiled=True)  53.4 us
    all_gather x1, waiting for transfers between devices, local(): piece_gate = lax.all_gather(ratio_gate, 'fs', axis=0, tiled=True)  50.4 us
    all_gather x1, waiting for transfers between devices, local(): lax.all_gather(input_factor, 'fs', axis=0, tiled=True)  46.7 us
    all_gather x1, waiting for transfers between devices, local(): lax.all_gather(gate_factor, 'fs', axis=0, tiled=True)  45.5 us
    psum x1, blocking collectives, local(): lax.psum((jnp.sum(dir_in * dir_in), jnp.sum(dir_gate * dir_gate)), ('fs',...  38.6 us
  transfers between devices with their start and end apart: 7, of which 7 were waited for; matrix products, arithmetic and copies ran while one was open for 8% of the time, Pallas kernels for 0%

commit v1 on v0

v1 whole, which is shorter than its diff:
```python
import jax
import jax.numpy as jnp
from jax import lax
from jax.experimental import pallas as pl
from jax.experimental.pallas import tpu as pltpu
from jax.sharding import PartitionSpec as P

first_decay = 0.9
second_decay = 0.9
ratio_floor = 1e-08
mean_floor = 1e-06
step_size = 0.05
bf16 = jnp.bfloat16
f32 = jnp.float32
contract = (((0,), (0,)), ((), ()))
plain = (((1,), (0,)), ((), ()))


def swap(a, axis, mask):
    size = lax.axis_size(axis)
    return lax.ppermute(a, axis, [(i, i ^ mask) for i in range(size)])


def split(a, terms):
    out = []
    for _ in range(terms):
        top = lax.reduce_precision(a, 8, 7)
        out.append(top.astype(bf16))
        a = a - top
    return out


def dot(a, b, dims):
    return lax.dot_general(a, b, dims, preferred_element_type=f32)


def moments(low_rank, first, second):
    first_new = first_decay * first + (1.0 - first_decay) * low_rank
    second_new = second_decay * second + (1.0 - second_decay) * low_rank * low_rank
    ratio = first_new / (jnp.sqrt(second_new) + ratio_floor)
    return (first_new, second_new, ratio)


def pick(a, index, axis):
    return lax.dynamic_index_in_dim(a, index, axis, keepdims=False)


def gather(own):
    lines = lax.axis_size("fs") // 4
    line = [swap(own, "fs", 4 * k) for k in range(1, lines)]
    line = jnp.stack([own] + line)
    return [line] + [swap(line, "fs", c) for c in (1, 2, 3)]


def specs():
    return (pl.BlockSpec(memory_space=space) for space in (pltpu.SMEM, pltpu.VMEM, pl.ANY))


def directions(stacks, gram, factor, me):
    lines, rows, width = stacks[0].shape
    rank = gram.shape[0]
    if rows % 8:
        whole = jnp.zeros((4 * lines, rows, width), f32)
        for c, stack in enumerate(stacks):
            for k in range(lines):
                whole = lax.dynamic_update_index_in_dim(whole, stack[k], me ^ (4 * k + c), 0)
        stacks, lines = [whole.reshape(1, rank, width)], 1

    def terms_of(a, count):
        for _ in range(count):
            top = a.astype(bf16)
            yield top
            a = a - top.astype(f32)

    def kernel(me_ref, gram_ref, factor_ref, *refs):
        pieces, (moved_ref, square_ref, ratio_ref) = refs[:-3], refs[-3:]
        for c, stack in enumerate(pieces):
            for k in range(lines):
                if rows % 8:
                    ratio_ref[...] = stack[k]
                else:
                    owner = me_ref[0] ^ (4 * k + c)
                    ratio_ref[pl.ds(pl.multiple_of(owner * rows, rows), rows), :] = stack[k]
        ratio = ratio_ref[...]
        high, middle, low = terms_of(ratio, 3)
        some = factor_ref[...]
        moved_ref[...] = jnp.dot(
            jnp.concatenate([some] * 3, axis=1),
            jnp.concatenate([high, middle, low]),
            preferred_element_type=f32,
        )
        gram_high, gram_low = terms_of(gram_ref[...], 2)
        applied = jnp.dot(
            jnp.concatenate([gram_high, gram_high, gram_low], axis=1),
            jnp.concatenate([high, middle, high]),
            preferred_element_type=f32,
        )
        by_column = jnp.sum(ratio * applied, axis=0, keepdims=True)
        square = jnp.sum(by_column, axis=1, keepdims=True)
        square_ref[...] = jnp.broadcast_to(square, square_ref.shape)

    smem, vmem, _ = specs()
    return pl.pallas_call(
        kernel,
        out_shape=(
            jax.ShapeDtypeStruct((factor.shape[0], width), f32),
            jax.ShapeDtypeStruct((8, 128), f32),
        ),
        in_specs=[smem] + [vmem] * (2 + len(stacks)),
        out_specs=(vmem, vmem),
        scratch_shapes=[pltpu.VMEM((rank, width), f32)],
        cost_estimate=pl.CostEstimate(
            flops=6 * rank * width * (rank + factor.shape[0]),
            bytes_accessed=8 * rank * width,
            transcendentals=0,
        ),
        name="directions",
    )(me.astype(jnp.int32).reshape(1), gram, factor, *stacks)


def finish(moved, square, others, master, count):
    def kernel(moved_ref, square_ref, others_ref, master_ref, step_ref, copy_ref):
        mean = (square_ref[0:1, 0:1] + others_ref[0:1, 0:1]) / count
        step = moved_ref[...] * lax.rsqrt(mean + mean_floor)
        step_ref[...] = step
        copy_ref[...] = (master_ref[...] - step_size * step).astype(bf16)

    _, vmem, _ = specs()
    return pl.pallas_call(
        kernel,
        out_shape=(
            jax.ShapeDtypeStruct(moved.shape, f32),
            jax.ShapeDtypeStruct(moved.shape, bf16),
        ),
        in_specs=[vmem] * 4,
        out_specs=(vmem, vmem),
        cost_estimate=pl.CostEstimate(
            flops=4 * moved.size, bytes_accessed=14 * moved.size, transcendentals=0
        ),
        name="finish",
    )(moved, square, others, master)


def spread(own):
    lines = lax.axis_size("fs") // 4
    blocks = {}
    for k in range(lines):
        if k % 2 and k > 1:
            block = swap(blocks[4 * k - 4], "fs", 4)
        else:
            block = swap(own, "fs", 4 * k) if k else own
        across = swap(block, "fs", 1)
        along = swap(block, "fs", 2)
        if k % 2:
            corner = swap(blocks[4 * k - 1], "fs", 4)
        elif k % 4:
            corner = swap(along, "fs", 1)
        else:
            corner = swap(across, "fs", 2)
        blocks |= {4 * k: block, 4 * k + 1: across, 4 * k + 2: along, 4 * k + 3: corner}
    return blocks


def place_copies(blocks, me):
    lines = len(blocks) // 4
    order = []
    for k in range(lines):
        order += [4 * k, 4 * k + 1, 4 * k + 2] + [4 * k - 1] * (k > 0)
    order.append(4 * lines - 1)
    rows, width = blocks[0].shape
    out = None
    for start in range(0, len(order), 4):
        group = order[start : start + 4]

        def kernel(me_ref, *refs, group=group):
            sources, out_ref, sems = refs[: len(group)], refs[-2], refs[-1]
            copies = []
            for i, mask in enumerate(group):
                target = pl.ds(pl.multiple_of((me_ref[0] ^ mask) * rows, rows), rows)
                copies.append(pltpu.make_async_copy(sources[i], out_ref.at[target, :], sems.at[i]))
                copies[-1].start()
            for copy in copies:
                copy.wait()

        smem, vmem, anywhere = specs()
        n = len(group)
        call = pl.pallas_call(
            kernel,
            out_shape=jax.ShapeDtypeStruct((len(order) * rows, width), bf16),
            in_specs=[smem] + [vmem] * n + [anywhere] * (out is not None),
            out_specs=pl.BlockSpec(memory_space=pltpu.HBM),
            scratch_shapes=[pltpu.SemaphoreType.DMA((n,))],
            input_output_aliases={} if out is None else {1 + n: 0},
            cost_estimate=pl.CostEstimate(
                flops=0, bytes_accessed=4 * n * rows * width, transcendentals=0
            ),
            name="place_copies",
        )
        out = call(
            me.astype(jnp.int32).reshape(1),
            *(blocks[mask] for mask in group),
            *([] if out is None else [out]),
        )
    return out


def order_factors(mine, other, me, core):
    lines, rows, columns = mine[0].shape
    count = 4 * lines

    def kernel(me_ref, core_ref, *refs):
        sources, (out_in, out_gate) = refs[:-2], refs[-2:]
        first = core_ref[0] == 0
        for c in range(4):
            for k in range(lines):
                owner = me_ref[0] ^ (4 * k + c)
                target = pl.ds(pl.multiple_of(owner * rows, rows), rows)
                a, b = sources[c][k], sources[4 + c][k]
                out_in[target, :] = jnp.where(first, a, b)
                out_gate[target, :] = jnp.where(first, b, a)

    smem, vmem = (pl.BlockSpec(memory_space=space) for space in (pltpu.SMEM, pltpu.VMEM))
    shape = jax.ShapeDtypeStruct((count * rows, columns), mine[0].dtype)
    return pl.pallas_call(
        kernel,
        out_shape=(shape, shape),
        in_specs=[smem, smem] + [vmem] * 8,
        out_specs=(vmem, vmem),
        cost_estimate=pl.CostEstimate(
            flops=0, bytes_accessed=8 * count * rows * columns, transcendentals=0
        ),
        name="order_factors",
    )(me.astype(jnp.int32).reshape(1), core.astype(jnp.int32).reshape(1), *mine, *other)


def local(
    saved_inputs,
    input_cot,
    gate_cot,
    input_master,
    gate_master,
    input_factor,
    gate_factor,
    input_first,
    input_second,
    gate_first,
    gate_second,
):
    fs, tp = lax.axis_size("fs"), lax.axis_size("tp")
    me, core = lax.axis_index("fs"), lax.axis_index("tp")
    lines = fs // 4
    here_x, here_y, here_z = me & 1, (me >> 1) & 1, me >> 2
    rank = input_factor.shape[1]
    width = input_cot.shape[1]
    half = width // 2
    count = fs * input_master.shape[0] * tp * width

    if tp == 2:
        mine = gather(jnp.where(core == 0, input_factor, gate_factor))
        other = [swap(stack, "tp", 1) for stack in mine]
        whole_in, whole_gate = order_factors(mine, other, me, core)
    else:
        zero = jnp.zeros_like(core)
        whole_in, whole_gate = order_factors(gather(input_factor), gather(gate_factor), me, zero)

    def chain(cot, master, own_factor, factor, first, second):
        projected = split(dot(saved_inputs, factor, plain), 2)
        term = sum(dot(piece, cot, contract) for piece in projected)
        term = term.reshape(lines, 2, 2, rank // fs, width)
        left, right = term[..., :half], term[..., half:]
        left = pick(left, here_x, 2) + swap(pick(left, 1 - here_x, 2), "fs", 1)
        right = pick(right, here_y, 1) + swap(pick(right, 1 - here_y, 1), "fs", 2)
        left = pick(left, here_y, 1) + swap(pick(left, 1 - here_y, 1), "fs", 2)
        right = pick(right, here_x, 1) + swap(pick(right, 1 - here_x, 1), "fs", 1)
        both = jnp.concatenate([left, right], axis=-1)
        low_rank = pick(both, here_z, 0)
        for k in range(1, lines):
            low_rank = low_rank + swap(pick(both, here_z ^ k, 0), "fs", 4 * k)
        first_new, second_new, ratio = moments(low_rank, first, second)
        stacks = gather(ratio)
        gram = dot(factor, factor, contract)
        moved, square = directions(stacks, gram, own_factor, me)
        if tp == 2:
            others = swap(square, "tp", 1)
        else:
            others = lax.psum(square, "tp") - square
        step, local_copy = finish(moved, square, others, master, count)
        copy = place_copies(spread(local_copy), me)
        return step, first_new, second_new, copy

    step_gate, first_gate, second_gate, copy_gate = chain(
        gate_cot, gate_master, gate_factor, whole_gate, gate_first, gate_second
    )
    step_in, first_in, second_in, copy_in = chain(
        input_cot, input_master, input_factor, whole_in, input_first, input_second
    )
    return (step_in, step_gate, first_in, second_in, first_gate, second_gate, copy_in, copy_gate)


def solution(mesh):
    rows, tokens = P("fs", "tp"), P("fs", None)

    return jax.shard_map(
        local,
        mesh=mesh,
        in_specs=(tokens, rows, rows, rows, rows, tokens, tokens, rows, rows, rows, rows),
        out_specs=(rows,) * 6 + (P(None, "tp"),) * 2,
        check_vma=False,
    )
```

time: 570 us -> 195 us (0.34)
  waiting for transfers between devices: 442 us -> 87.5 us
  starting transfers between devices: 0.28 us -> 61.4 us
  blocking collectives: 38.6 us -> 0 us
  matrix products: 40.9 us -> 8.13 us
  Pallas kernels: 0 us -> 30.6 us
  local copies, waits for them, and re-layouts: 24.3 us -> 2.35 us
  between operations: 15.6 us -> 1.36 us
    all_gather x6 -> x0, waiting for transfers between devices: 360 us -> none  [the longest x1 83.2 us: local(): lax.all_gather(local_gate, 'fs', axis=0, tiled=True)]
    ppermute x0 -> x68, waiting for transfers between devices: none -> 87.5 us  [swap(): return lax.ppermute(a, axis, [(i, i ^ mask) for i in range(size)])]
    reduce_scatter x1 -> x0, waiting for transfers between devices: 80.6 us -> none  [local(): lax.psum_scatter(jnp.concatenate([term_in, term_gate], axis=1), 'fs', sca...]
    ppermute x0 -> x68, starting transfers between devices: none -> 61.4 us  [swap(): return lax.ppermute(a, axis, [(i, i ^ mask) for i in range(size)])]
    psum x1 -> x0, blocking collectives: 38.6 us -> none  [local(): lax.psum((jnp.sum(dir_in * dir_in), jnp.sum(dir_gate * dir_gate)), ('fs',...]
    dot_general x6 -> x8, matrix products: 40.9 us -> 8.13 us  [dot(): return lax.dot_general(a, b, dims, preferred_element_type=f32)]
    pallas_call x0 -> x13, Pallas kernels: none -> 30.6 us  [the longest x8 17.5 us: place_copies(): call(me.astype(jnp.int32).reshape(1), *(blocks[mask] for mask in group),...]
    unnamed x25 -> x66, local copies, waits for them, and re-layouts: 24.3 us -> 2.03 us
  transfers between devices with their start and end apart: 7 -> 68, of which waited for: 7 -> 29; matrix products, arithmetic and copies ran while one was open for 8% -> 4% of each run, Pallas kernels for 0% -> 13%
where the time goes in v1:
time: 195 us
  waiting for transfers between devices  87.5 us (45%)
  starting transfers between devices  61.4 us (31%)
  Pallas kernels  30.6 us (16%)
  matrix products  8.13 us (4%)
  other arithmetic  3.46 us (2%)
  local copies, waits for them, and re-layouts  2.35 us (1%)
    ppermute x68, waiting for transfers between devices, swap(): return lax.ppermute(a, axis, [(i, i ^ mask) for i in range(size)])  87.5 us
    ppermute x68, starting transfers between devices, swap(): return lax.ppermute(a, axis, [(i, i ^ mask) for i in range(size)])  61.4 us
    pallas_call x8, Pallas kernels, place_copies(): call(me.astype(jnp.int32).reshape(1), *(blocks[mask] for mask in group),...  17.5 us
    dot_general x8, matrix products, dot(): return lax.dot_general(a, b, dims, preferred_element_type=f32)  8.13 us
    pallas_call x2, Pallas kernels, directions(): pl.pallas_call(kernel, out_shape=(jax.ShapeDtypeStruct((factor.shape[0],...  5.76 us
    pallas_call x2, Pallas kernels, finish(): pl.pallas_call(kernel, out_shape=(jax.ShapeDtypeStruct(moved.shape, f32),...  4.37 us
  transfers between devices with their start and end apart: 68, of which 29 were waited for; matrix products, arithmetic and copies ran while one was open for 4% of the time, Pallas kernels for 13%

profile of v1, /device:TPU:0, one launch (start us, length us, event | category | flops | bytes accessed | tf_op | source)
XLA Modules:
  0.0 194.7 jit_solution(260692127833681537)
XLA Ops:
  1.7 3.1 %collective-permute-start = (bf16[128,256]{1,0:T(8,128)(2,1)S(1)}, bf16[128,256]{1,0:T(8,128)(2,1)S(1)}, u32[]{:S(2)}, u32[]{:S(2)}) collective-permute-start(bf16[128,256]{1,0:T(8,128)(2,1)S(1)} %broadcast_select_fusion), channel_id=1, source_target_pairs={{0,8},{2,10},{4,12},{6,14},{8,0},{10,2},{12,4},{14,6},{16,24},{18,... | collective-permute-start | bytes 196616 | tf_op jit(solution)/shard_map/ppermute | solution.py:21
  4.8 2.6 %collective-permute-start.1 = (bf16[128,256]{1,0:T(8,128)(2,1)S(1)}, bf16[128,256]{1,0:T(8,128)(2,1)S(1)}, u32[]{:S(2)}, u32[]{:S(2)}) collective-permute-start(bf16[128,256]{1,0:T(8,128)(2,1)S(1)} %broadcast_select_fusion), channel_id=1, source_target_pairs={{0,16},{2,18},{4,20},{6,22},{8,24},{10,26},{12,28},{14,30},{16,0},... | collective-permute-start | bytes 196616 | tf_op jit(solution)/shard_map/ppermute | solution.py:21
  7.4 4.7 %collective-permute-done.1 = bf16[128,256]{1,0:T(8,128)(2,1)S(1)} collective-permute-done((bf16[128,256]{1,0:T(8,128)(2,1)S(1)}, bf16[128,256]{1,0:T(8,128)(2,1)S(1)}, u32[]{:S(2)}, u32[]{:S(2)}) %collective-permute-start.1) | collective-permute-done | bytes 65568 | tf_op jit(solution)/shard_map/ppermute | solution.py:21
  13.5 1.6 collective-permute-start.3
  15.1 1.5 collective-permute-start.4
  17.1 5.8 %collective-permute-done.3.refs_1_ = bf16[4,128,256]{2,1,0:T(8,128)(2,1)} collective-permute-done((bf16[4,128,256]{2,1,0:T(8,128)(2,1)S(1)}, bf16[4,128,256]{2,1,0:T(8,128)(2,1)}, u32[]{:S(2)}, u32[]{:S(2)}) %collective-permute-start.3) | collective-permute-done | bytes 262176 | tf_op jit(solution)/shard_map/ppermute | solution.py:21
  22.9 4.1 %collective-permute-done.4.refs_2_ = bf16[4,128,256]{2,1,0:T(8,128)(2,1)} collective-permute-done((bf16[4,128,256]{2,1,0:T(8,128)(2,1)S(1)}, bf16[4,128,256]{2,1,0:T(8,128)(2,1)}, u32[]{:S(2)}, u32[]{:S(2)}) %collective-permute-start.4) | collective-permute-done | bytes 262176 | tf_op jit(solution)/shard_map/ppermute | solution.py:21
  29.2 3.0 %order_factors.1 = (bf16[2048,256]{1,0:T(8,128)(2,1)}, bf16[2048,256]{1,0:T(8,128)(2,1)}) custom-call(s32[1]{0:T(128)} %bitcast.me_ref, s32[1]{0:T(128)} %bitcast.1.core_ref, bf16[4,128,256]{2,1,0:T(8,128)(2,1)} %copy-done.5, bf16[4,128,256]{2,1,0:T(8,128)(2,1)} %collective-permute-done.3.refs_1_, bf16[4,128,256]{2,1,0:T(8,128)(2,1)} %collective-permute-done.4.refs_2_, ...), custom_call_target="tpu_custom_call" | custom-call | bytes 4194304 | tf_op jit(solution)/shard_map/order_factors/pallas_call | solution.py:224
  32.2 2.4 %convolution_bitcast_fusion = f32[768,256]{0,1:T(8,128)S(1)} fusion(bf16[2048,256]{1,0:T(8,128)(2,1)} %get-tuple-element.22, bf16[768,2048]{1,0:T(8,128)(2,1)S(1)} %copy-done), kind=kOutput, calls=%fused_computation.2 | convolution fusion | flops 805306368 | bytes 4980736 | tf_op jit(solution)/shard_map/dot_general | solution.py:34
  35.9 1.6 collective-permute-start.26
  42.6 2.5 %collective-permute-done.26 = f32[4,2,16,512]{3,2,1,0:T(8,128)S(1)} collective-permute-done((f32[4,2,16,512]{3,2,1,0:T(8,128)S(1)}, f32[4,2,16,512]{3,2,1,0:T(8,128)S(1)}, u32[]{:S(2)}, u32[]{:S(2)}) %collective-permute-start.26) | collective-permute-done | bytes 262176 | tf_op jit(solution)/shard_map/ppermute | solution.py:21
  47.5 3.3 %collective-permute-done.12 = f32[4,2,16,512]{3,2,1,0:T(8,128)S(1)} collective-permute-done((f32[4,2,16,512]{3,2,1,0:T(8,128)S(1)}, f32[4,2,16,512]{3,2,1,0:T(8,128)S(1)}, u32[]{:S(2)}, u32[]{:S(2)}) %collective-permute-start.12) | collective-permute-done | bytes 262176 | tf_op jit(solution)/shard_map/ppermute | solution.py:21
  53.0 2.1 %collective-permute-done.27 = f32[4,16,512]{2,1,0:T(8,128)S(1)} collective-permute-done((f32[4,16,512]{2,1,0:T(8,128)S(1)}, f32[4,16,512]{2,1,0:T(8,128)S(1)}, u32[]{:S(2)}, u32[]{:S(2)}) %collective-permute-start.27) | collective-permute-done | bytes 131104 | tf_op jit(solution)/shard_map/ppermute | solution.py:21
  57.4 2.2 %collective-permute-start.30 = (f32[16,1024]{1,0:T(8,128)S(1)}, f32[16,1024]{1,0:T(8,128)S(1)}, u32[]{:S(2)}, u32[]{:S(2)}) collective-permute-start(f32[16,1024]{1,0:T(8,128)S(1)} %get-tuple-element.40), channel_id=1, source_target_pairs={{0,24},{2,26},{4,28},{6,30},{8,16},{10,18},{12,20},{14,22},{16,8},... | collective-permute-start | bytes 196616 | tf_op jit(solution)/shard_map/ppermute | solution.py:21
  59.8 2.1 %collective-permute-start.15 = (f32[16,1024]{1,0:T(8,128)S(1)}, f32[16,1024]{1,0:T(8,128)S(1)}, u32[]{:S(2)}, u32[]{:S(2)}) collective-permute-start(f32[16,1024]{1,0:T(8,128)S(1)} %get-tuple-element.42), channel_id=1, source_target_pairs={{0,16},{2,18},{4,20},{6,22},{8,24},{10,26},{12,28},{14,30},{16,0},... | collective-permute-start | bytes 196616 | tf_op jit(solution)/shard_map/ppermute | solution.py:21
  62.0 2.2 %collective-permute-start.16 = (f32[16,1024]{1,0:T(8,128)S(1)}, f32[16,1024]{1,0:T(8,128)S(1)}, u32[]{:S(2)}, u32[]{:S(2)}) collective-permute-start(f32[16,1024]{1,0:T(8,128)S(1)} %get-tuple-element.43), channel_id=1, source_target_pairs={{0,24},{2,26},{4,28},{6,30},{8,16},{10,18},{12,20},{14,22},{16,8},... | collective-permute-start | bytes 196616 | tf_op jit(solution)/shard_map/ppermute | solution.py:21
  65.5 4.7 %collective-permute-start.31 = (f32[16,1024]{1,0:T(8,128)S(1)}, f32[16,1024]{1,0:T(8,128)S(1)}, u32[]{:S(2)}, u32[]{:S(2)}) collective-permute-start(f32[16,1024]{1,0:T(8,128)S(1)} %get-tuple-element.28), channel_id=1, source_target_pairs={{0,8},{2,10},{4,12},{6,14},{8,0},{10,2},{12,4},{14,6},{16,24},{18,... | collective-permute-start | bytes 196616 | tf_op jit(solution)/shard_map/ppermute | solution.py:21
  74.4 2.0 %collective-permute-start.18 = (f32[16,1024]{1,0:T(8,128)S(1)}, f32[16,1024]{1,0:T(8,128)S(1)}, u32[]{:S(2)}, u32[]{:S(2)}) collective-permute-start(f32[16,1024]{1,0:T(8,128)S(1)} %get-tuple-element.31), channel_id=1, source_target_pairs={{0,16},{2,18},{4,20},{6,22},{8,24},{10,26},{12,28},{14,30},{16,0},... | collective-permute-start | bytes 196616 | tf_op jit(solution)/shard_map/ppermute | solution.py:21
  80.3 2.5 %collective-permute-start.36 = (f32[4,16,1024]{2,1,0:T(8,128)S(1)}, f32[4,16,1024]{2,1,0:T(8,128)}, u32[]{:S(2)}, u32[]{:S(2)}) collective-permute-start(f32[4,16,1024]{2,1,0:T(8,128)S(1)} %pad_maximum_fusion.2.refs_0_), channel_id=1, source_target_pairs={{0,6},{2,4},{4,2},{6,0},{8,14},{10,12},{12,10},{14,8},{16,22},{18,... | collective-permute-start | bytes 786440 | tf_op jit(solution)/shard_map/ppermute | solution.py:21
  84.6 2.8 %collective-permute-done.34.refs_1_ = f32[4,16,1024]{2,1,0:T(8,128)S(1)} collective-permute-done((f32[4,16,1024]{2,1,0:T(8,128)S(1)}, f32[4,16,1024]{2,1,0:T(8,128)S(1)}, u32[]{:S(2)}, u32[]{:S(2)}) %collective-permute-start.34) | collective-permute-done | bytes 262176 | tf_op jit(solution)/shard_map/ppermute | solution.py:21
  88.9 4.1 %collective-permute-done.35.refs_2_ = f32[4,16,1024]{2,1,0:T(8,128)S(1)} collective-permute-done((f32[4,16,1024]{2,1,0:T(8,128)S(1)}, f32[4,16,1024]{2,1,0:T(8,128)S(1)}, u32[]{:S(2)}, u32[]{:S(2)}) %collective-permute-start.35) | collective-permute-done | bytes 262176 | tf_op jit(solution)/shard_map/ppermute | solution.py:21
  93.8 2.9 %directions.3 = (f32[128,1024]{1,0:T(8,128)}, f32[8,128]{1,0:T(8,128)}) custom-call(s32[1]{0:T(128)} %bitcast.me_ref, f32[256,256]{1,0:T(8,128)} %fusion.37.gram_ref, bf16[128,256]{1,0:T(8,128)(2,1)} %factor_ref.3, f32[4,16,1024]{2,1,0:T(8,128)} %copy-done.21, f32[4,16,1024]{2,1,0:T(8,128)} %copy-done.31, f32[4,16,1024]{2,1,0:T(8,128)} %copy-done.32, ...), custom_call_target="tpu_custom_call" | custom-call | flops 603979776 | bytes 2097152 | tf_op jit(solution)/shard_map/directions/pallas_call | solution.py:103
  96.7 2.1 %collective-permute-done.21.refs_2_ = f32[4,16,1024]{2,1,0:T(8,128)} collective-permute-done((f32[4,16,1024]{2,1,0:T(8,128)}, f32[4,16,1024]{2,1,0:T(8,128)}, u32[]{:S(2)}, u32[]{:S(2)}) %collective-permute-start.21) | collective-permute-done | bytes 262176 | tf_op jit(solution)/shard_map/ppermute | solution.py:21
  98.8 2.9 %directions.2 = (f32[128,1024]{1,0:T(8,128)}, f32[8,128]{1,0:T(8,128)}) custom-call(s32[1]{0:T(128)} %bitcast.me_ref, f32[256,256]{1,0:T(8,128)} %fusion.36.gram_ref, bf16[128,256]{1,0:T(8,128)(2,1)} %factor_ref.2, f32[4,16,1024]{2,1,0:T(8,128)} %pad_maximum_fusion.1.refs_0_, f32[4,16,1024]{2,1,0:T(8,128)} %collective-permute-done.20.refs_1_, ...), custom_call_target="tpu_custom_call" | custom-call | flops 603979776 | bytes 2097152 | tf_op jit(solution)/shard_map/directions/pallas_call | solution.py:103
  102.3 2.2 %finish.3 = (f32[128,1024]{1,0:T(8,128)}, bf16[128,1024]{1,0:T(8,128)(2,1)}) custom-call(f32[128,1024]{1,0:T(8,128)} %get-tuple-element.23.moved_ref, f32[8,128]{1,0:T(8,128)} %get-tuple-element.24.square_ref, f32[8,128]{1,0:T(8,128)} %copy-done.30, f32[128,1024]{1,0:T(8,128)} %master_ref.3), custom_call_target="tpu_custom_call" | custom-call | flops 524288 | bytes 1835008 | tf_op jit(solution)/shard_map/finish/pallas_call | solution.py:129
  109.7 2.2 %finish.2 = (f32[128,1024]{1,0:T(8,128)}, bf16[128,1024]{1,0:T(8,128)(2,1)}) custom-call(f32[128,1024]{1,0:T(8,128)} %get-tuple-element.19.moved_ref, f32[8,128]{1,0:T(8,128)} %get-tuple-element.20.square_ref, f32[8,128]{1,0:T(8,128)} %copy-done.29, f32[128,1024]{1,0:T(8,128)} %master_ref.2), custom_call_target="tpu_custom_call" | custom-call | flops 524288 | bytes 1835008 | tf_op jit(solution)/shard_map/finish/pallas_call | solution.py:129
  114.8 5.1 %collective-permute-done.64.refs_3_ = bf16[128,1024]{1,0:T(8,128)(2,1)} collective-permute-done((bf16[128,1024]{1,0:T(8,128)(2,1)}, bf16[128,1024]{1,0:T(8,128)(2,1)}, u32[]{:S(2)}, u32[]{:S(2)}) %collective-permute-start.64) | collective-permute-done | bytes 262176 | tf_op jit(solution)/shard_map/ppermute | solution.py:21
  120.6 2.0 %collective-permute-done.53.refs_3_ = bf16[128,1024]{1,0:T(8,128)(2,1)S(1)} collective-permute-done((bf16[128,1024]{1,0:T(8,128)(2,1)}, bf16[128,1024]{1,0:T(8,128)(2,1)S(1)}, u32[]{:S(2)}, u32[]{:S(2)}) %collective-permute-start.53) | collective-permute-done | bytes 262176 | tf_op jit(solution)/shard_map/ppermute | solution.py:21
  125.3 5.0 %collective-permute-done.49.refs_3_ = bf16[128,1024]{1,0:T(8,128)(2,1)S(1)} collective-permute-done((bf16[128,1024]{1,0:T(8,128)(2,1)}, bf16[128,1024]{1,0:T(8,128)(2,1)S(1)}, u32[]{:S(2)}, u32[]{:S(2)}) %collective-permute-start.49) | collective-permute-done | bytes 262176 | tf_op jit(solution)/shard_map/ppermute | solution.py:21
  130.4 3.4 %collective-permute-done.38.refs_3_ = bf16[128,1024]{1,0:T(8,128)(2,1)S(1)} collective-permute-done((bf16[128,1024]{1,0:T(8,128)(2,1)}, bf16[128,1024]{1,0:T(8,128)(2,1)S(1)}, u32[]{:S(2)}, u32[]{:S(2)}) %collective-permute-start.38) | collective-permute-done | bytes 262176 | tf_op jit(solution)/shard_map/ppermute | solution.py:21
  133.7 1.6 collective-permute-start.57
  137.1 2.6 %collective-permute-done.66.refs_1_ = bf16[128,1024]{1,0:T(8,128)(2,1)S(1)} collective-permute-done((bf16[128,1024]{1,0:T(8,128)(2,1)}, bf16[128,1024]{1,0:T(8,128)(2,1)S(1)}, u32[]{:S(2)}, u32[]{:S(2)}) %collective-permute-start.66) | collective-permute-done | bytes 262176 | tf_op jit(solution)/shard_map/ppermute | solution.py:21
  140.9 4.4 %collective-permute-done.57.refs_1_ = bf16[128,1024]{1,0:T(8,128)(2,1)S(1)} collective-permute-done((bf16[128,1024]{1,0:T(8,128)(2,1)S(1)}, bf16[128,1024]{1,0:T(8,128)(2,1)S(1)}, u32[]{:S(2)}, u32[]{:S(2)}) %collective-permute-start.57) | collective-permute-done | bytes 262176 | tf_op jit(solution)/shard_map/ppermute | solution.py:21
  145.4 5.5 %collective-permute-done.47.refs_2_ = bf16[128,1024]{1,0:T(8,128)(2,1)S(1)} collective-permute-done((bf16[128,1024]{1,0:T(8,128)(2,1)S(1)}, bf16[128,1024]{1,0:T(8,128)(2,1)S(1)}, u32[]{:S(2)}, u32[]{:S(2)}) %collective-permute-start.47) | collective-permute-done | bytes 262176 | tf_op jit(solution)/shard_map/ppermute | solution.py:21
  151.0 5.5 %collective-permute-done.51.refs_1_ = bf16[128,1024]{1,0:T(8,128)(2,1)S(1)} collective-permute-done((bf16[128,1024]{1,0:T(8,128)(2,1)S(1)}, bf16[128,1024]{1,0:T(8,128)(2,1)S(1)}, u32[]{:S(2)}, u32[]{:S(2)}) %collective-permute-start.51) | collective-permute-done | bytes 262176 | tf_op jit(solution)/shard_map/ppermute | solution.py:21
  156.5 2.0 %collective-permute-start.55 = (bf16[128,1024]{1,0:T(8,128)(2,1)}, bf16[128,1024]{1,0:T(8,128)(2,1)S(1)}, u32[]{:S(2)}, u32[]{:S(2)}) collective-permute-start(bf16[128,1024]{1,0:T(8,128)(2,1)} %collective-permute-done.54.refs_3_), channel_id=1, source_target_pairs={{0,2},{2,0},{4,6},{6,4},{8,10},{10,8},{12,14},{14,12},{16,18},{18,... | collective-permute-start | bytes 786440 | tf_op jit(solution)/shard_map/ppermute | solution.py:21
  158.5 2.1 %collective-permute-done.42.refs_1_ = bf16[128,1024]{1,0:T(8,128)(2,1)S(1)} collective-permute-done((bf16[128,1024]{1,0:T(8,128)(2,1)S(1)}, bf16[128,1024]{1,0:T(8,128)(2,1)S(1)}, u32[]{:S(2)}, u32[]{:S(2)}) %collective-permute-start.42) | collective-permute-done | bytes 262176 | tf_op jit(solution)/shard_map/ppermute | solution.py:21
  162.0 3.8 %collective-permute-done.58.refs_2_ = bf16[128,1024]{1,0:T(8,128)(2,1)} collective-permute-done((bf16[128,1024]{1,0:T(8,128)(2,1)S(1)}, bf16[128,1024]{1,0:T(8,128)(2,1)}, u32[]{:S(2)}, u32[]{:S(2)}) %collective-permute-start.58) | collective-permute-done | bytes 262176 | tf_op jit(solution)/shard_map/ppermute | solution.py:21
  165.8 5.5 %collective-permute-done.55.refs_0_ = bf16[128,1024]{1,0:T(8,128)(2,1)S(1)} collective-permute-done((bf16[128,1024]{1,0:T(8,128)(2,1)}, bf16[128,1024]{1,0:T(8,128)(2,1)S(1)}, u32[]{:S(2)}, u32[]{:S(2)}) %collective-permute-start.55) | collective-permute-done | bytes 262176 | tf_op jit(solution)/shard_map/ppermute | solution.py:21
  171.4 5.6 %collective-permute-done.43.refs_2_ = bf16[128,1024]{1,0:T(8,128)(2,1)} collective-permute-done((bf16[128,1024]{1,0:T(8,128)(2,1)S(1)}, bf16[128,1024]{1,0:T(8,128)(2,1)}, u32[]{:S(2)}, u32[]{:S(2)}) %collective-permute-start.43) | collective-permute-done | bytes 262176 | tf_op jit(solution)/shard_map/ppermute | solution.py:21
  177.1 2.2 %place_copies.12.refs_4_ = bf16[2048,1024]{1,0:T(8,128)(2,1)} custom-call(s32[1]{0:T(128)} %bitcast.me_ref, bf16[128,1024]{1,0:T(8,128)(2,1)} %get-tuple-element.27.refs_0_, bf16[128,1024]{1,0:T(8,128)(2,1)} %collective-permute-done.61.refs_1_, bf16[128,1024]{1,0:T(8,128)(2,1)} %collective-permute-done.67.refs_2_, ...), custom_call_target="tpu_custom_call" | custom-call | bytes 2097152 | tf_op jit(solution)/shard_map/place_copies/pallas_call | solution.py:199
  179.3 2.2 %place_copies.8.refs_4_ = bf16[2048,1024]{1,0:T(8,128)(2,1)} custom-call(s32[1]{0:T(128)} %bitcast.me_ref, bf16[128,1024]{1,0:T(8,128)(2,1)} %get-tuple-element.26.refs_0_, bf16[128,1024]{1,0:T(8,128)(2,1)} %copy-done.22, bf16[128,1024]{1,0:T(8,128)(2,1)} %copy-done.24, bf16[128,1024]{1,0:T(8,128)(2,1)} %copy-done.23), custom_call_target="tpu_custom_call" | custom-call | bytes 2097152 | tf_op jit(solution)/shard_map/place_copies/pallas_call | solution.py:199
  181.5 2.2 %place_copies.13.refs_4_ = bf16[2048,1024]{1,0:T(8,128)(2,1)} custom-call(s32[1]{0:T(128)} %bitcast.me_ref, bf16[128,1024]{1,0:T(8,128)(2,1)} %copy-done.9, bf16[128,1024]{1,0:T(8,128)(2,1)} %copy-done.10, bf16[128,1024]{1,0:T(8,128)(2,1)} %copy-done.8, bf16[128,1024]{1,0:T(8,128)(2,1)} %copy-done.6, ...), custom_call_target="tpu_custom_call", output_to_operand_aliasing={{}: (5, {})} | custom-call | bytes 2097152 | tf_op jit(solution)/shard_map/place_copies/pallas_call | solution.py:199
  183.7 2.2 %place_copies.9.refs_4_ = bf16[2048,1024]{1,0:T(8,128)(2,1)} custom-call(s32[1]{0:T(128)} %bitcast.me_ref, bf16[128,1024]{1,0:T(8,128)(2,1)} %copy-done.14, bf16[128,1024]{1,0:T(8,128)(2,1)} %copy-done.15, bf16[128,1024]{1,0:T(8,128)(2,1)} %copy-done.13, bf16[128,1024]{1,0:T(8,128)(2,1)} %copy-done.7, ...), custom_call_target="tpu_custom_call", output_to_operand_aliasing={{}: (5, {})} | custom-call | bytes 2097152 | tf_op jit(solution)/shard_map/place_copies/pallas_call | solution.py:199
  185.9 2.2 %place_copies.14.refs_4_ = bf16[2048,1024]{1,0:T(8,128)(2,1)} custom-call(s32[1]{0:T(128)} %bitcast.me_ref, bf16[128,1024]{1,0:T(8,128)(2,1)} %copy-done.12, bf16[128,1024]{1,0:T(8,128)(2,1)} %copy-done.11, bf16[128,1024]{1,0:T(8,128)(2,1)} %copy-done.19, bf16[128,1024]{1,0:T(8,128)(2,1)} %collective-permute-done.54.refs_3_, ...), custom_call_target="tpu_custom_call", output_to_operand_aliasing={{}: (5, {})} | custom-call | bytes 2097152 | tf_op jit(solution)/shard_map/place_copies/pallas_call | solution.py:199
  188.1 2.2 %place_copies.10.refs_4_ = bf16[2048,1024]{1,0:T(8,128)(2,1)} custom-call(s32[1]{0:T(128)} %bitcast.me_ref, bf16[128,1024]{1,0:T(8,128)(2,1)} %copy-done.17, bf16[128,1024]{1,0:T(8,128)(2,1)} %copy-done.16, bf16[128,1024]{1,0:T(8,128)(2,1)} %copy-done.20, bf16[128,1024]{1,0:T(8,128)(2,1)} %collective-permute-done.39.refs_3_, ...), custom_call_target="tpu_custom_call", output_to_operand_aliasing={{}: (5, {})} | custom-call | bytes 2097152 | tf_op jit(solution)/shard_map/place_copies/pallas_call | solution.py:199
  190.3 2.2 %place_copies.15 = bf16[2048,1024]{1,0:T(8,128)(2,1)} custom-call(s32[1]{0:T(128)} %bitcast.me_ref, bf16[128,1024]{1,0:T(8,128)(2,1)} %copy-done.18, bf16[128,1024]{1,0:T(8,128)(2,1)} %collective-permute-done.56.refs_1_, bf16[128,1024]{1,0:T(8,128)(2,1)} %collective-permute-done.58.refs_2_, ...), custom_call_target="tpu_custom_call", output_to_operand_aliasing={{}: (5, {})} | custom-call | bytes 2097152 | tf_op jit(solution)/shard_map/place_copies/pallas_call | solution.py:199
  192.6 2.2 %place_copies.11 = bf16[2048,1024]{1,0:T(8,128)(2,1)} custom-call(s32[1]{0:T(128)} %bitcast.me_ref, bf16[128,1024]{1,0:T(8,128)(2,1)} %collective-permute-done.40.refs_0_, bf16[128,1024]{1,0:T(8,128)(2,1)} %collective-permute-done.41.refs_1_, bf16[128,1024]{1,0:T(8,128)(2,1)} %collective-permute-done.43.refs_2_, ...), custom_call_target="tpu_custom_call", output_to_operand_aliasing={{}: (5, {})} | custom-call | bytes 2097152 | tf_op jit(solution)/shard_map/place_copies/pallas_call | solution.py:199
  (201 shorter events, 48.9 us)
Async XLA Ops:
  13.5 9.3 %collective-permute-start.3 = (bf16[4,128,256]{2,1,0:T(8,128)(2,1)S(1)}, bf16[4,128,256]{2,1,0:T(8,128)(2,1)}, u32[]{:S(2)}, u32[]{:S(2)}) collective-permute-start(bf16[4,128,256]{2,1,0:T(8,128)(2,1)S(1)} %pad_maximum_fusion.refs_0_), channel_id=1, source_target_pairs={{0,2},{2,0},{4,6},{6,4},{8,10},{10,8},{12,14},{14,12},{16,18},{18,... | collective-permute-start | bytes 786440 | tf_op jit(solution)/shard_map/ppermute | solution.py:21
  15.1 11.9 %collective-permute-start.4 = (bf16[4,128,256]{2,1,0:T(8,128)(2,1)S(1)}, bf16[4,128,256]{2,1,0:T(8,128)(2,1)}, u32[]{:S(2)}, u32[]{:S(2)}) collective-permute-start(bf16[4,128,256]{2,1,0:T(8,128)(2,1)S(1)} %pad_maximum_fusion.refs_0_), channel_id=1, source_target_pairs={{0,4},{2,6},{4,0},{6,2},{8,12},{10,14},{12,8},{14,10},{16,20},{18,... | collective-permute-start | bytes 786440 | tf_op jit(solution)/shard_map/ppermute | solution.py:21
  16.6 10.4 %collective-permute-start.5 = (bf16[4,128,256]{2,1,0:T(8,128)(2,1)S(1)}, bf16[4,128,256]{2,1,0:T(8,128)(2,1)}, u32[]{:S(2)}, u32[]{:S(2)}) collective-permute-start(bf16[4,128,256]{2,1,0:T(8,128)(2,1)S(1)} %pad_maximum_fusion.refs_0_), channel_id=1, source_target_pairs={{0,6},{2,4},{4,2},{6,0},{8,14},{10,12},{12,10},{14,8},{16,22},{18,... | collective-permute-start | bytes 786440 | tf_op jit(solution)/shard_map/ppermute | solution.py:21
  17.1 10.4 %collective-permute-start.6 = (bf16[4,128,256]{2,1,0:T(8,128)(2,1)S(1)}, bf16[4,128,256]{2,1,0:T(8,128)(2,1)}, u32[]{:S(2)}, u32[]{:S(2)}) collective-permute-start(bf16[4,128,256]{2,1,0:T(8,128)(2,1)S(1)} %pad_maximum_fusion.refs_0_), channel_id=1, source_target_pairs={{0,1},{1,0},{2,3},{3,2},{4,5},{5,4},{6,7},{7,6},{8,9},{9,8},{10,11... | collective-permute-start | bytes 786440 | tf_op jit(solution)/shard_map/ppermute | solution.py:21
  35.9 9.2 %collective-permute-start.26 = (f32[4,2,16,512]{3,2,1,0:T(8,128)S(1)}, f32[4,2,16,512]{3,2,1,0:T(8,128)S(1)}, u32[]{:S(2)}, u32[]{:S(2)}) collective-permute-start(f32[4,2,16,512]{3,2,1,0:T(8,128)S(1)} %dynamic-slice_bitcast_fusion), channel_id=1, source_target_pairs={{0,4},{2,6},{4,0},{6,2},{8,12},{10,14},{12,8},{14,10},{16,20},{18,... | collective-permute-start | bytes 786440 | tf_op jit(solution)/shard_map/ppermute | solution.py:21
  37.4 9.2 %collective-permute-start.24 = (f32[4,2,16,512]{3,2,1,0:T(8,128)S(1)}, f32[4,2,16,512]{3,2,1,0:T(8,128)S(1)}, u32[]{:S(2)}, u32[]{:S(2)}) collective-permute-start(f32[4,2,16,512]{3,2,1,0:T(8,128)S(1)} %dynamic-slice_bitcast_fusion.1), channel_id=1, source_target_pairs={{0,2},{2,0},{4,6},{6,4},{8,10},{10,8},{12,14},{14,12},{16,18},{18,... | collective-permute-start | bytes 786440 | tf_op jit(solution)/shard_map/ppermute | solution.py:21
  40.5 10.3 %collective-permute-start.12 = (f32[4,2,16,512]{3,2,1,0:T(8,128)S(1)}, f32[4,2,16,512]{3,2,1,0:T(8,128)S(1)}, u32[]{:S(2)}, u32[]{:S(2)}) collective-permute-start(f32[4,2,16,512]{3,2,1,0:T(8,128)S(1)} %dynamic-slice_bitcast_fusion.2), channel_id=1, source_target_pairs={{0,4},{2,6},{4,0},{6,2},{8,12},{10,14},{12,8},{14,10},{16,20},{18,... | collective-permute-start | bytes 786440 | tf_op jit(solution)/shard_map/ppermute | solution.py:21
  41.4 10.9 %collective-permute-start.10 = (f32[4,2,16,512]{3,2,1,0:T(8,128)S(1)}, f32[4,2,16,512]{3,2,1,0:T(8,128)S(1)}, u32[]{:S(2)}, u32[]{:S(2)}) collective-permute-start(f32[4,2,16,512]{3,2,1,0:T(8,128)S(1)} %dynamic-slice_bitcast_fusion.3), channel_id=1, source_target_pairs={{0,2},{2,0},{4,6},{6,4},{8,10},{10,8},{12,14},{14,12},{16,18},{18,... | collective-permute-start | bytes 786440 | tf_op jit(solution)/shard_map/ppermute | solution.py:21
  45.2 9.9 %collective-permute-start.27 = (f32[4,16,512]{2,1,0:T(8,128)S(1)}, f32[4,16,512]{2,1,0:T(8,128)S(1)}, u32[]{:S(2)}, u32[]{:S(2)}) collective-permute-start(f32[4,16,512]{2,1,0:T(8,128)S(1)} %dynamic-slice_bitcast_fusion.4), channel_id=1, source_target_pairs={{0,2},{2,0},{4,6},{6,4},{8,10},{10,8},{12,14},{14,12},{16,18},{18,... | collective-permute-start | bytes 393224 | tf_op jit(solution)/shard_map/ppermute | solution.py:21
  59.8 11.5 %collective-permute-start.14 = (f32[16,1024]{1,0:T(8,128)S(1)}, f32[16,1024]{1,0:T(8,128)S(1)}, u32[]{:S(2)}, u32[]{:S(2)}) collective-permute-start(f32[16,1024]{1,0:T(8,128)S(1)} %get-tuple-element.41), channel_id=1, source_target_pairs={{0,8},{2,10},{4,12},{6,14},{8,0},{10,2},{12,4},{14,6},{16,24},{18,... | collective-permute-start | bytes 196616 | tf_op jit(solution)/shard_map/ppermute | solution.py:21
  59.8 12.9 %collective-permute-start.15 = (f32[16,1024]{1,0:T(8,128)S(1)}, f32[16,1024]{1,0:T(8,128)S(1)}, u32[]{:S(2)}, u32[]{:S(2)}) collective-permute-start(f32[16,1024]{1,0:T(8,128)S(1)} %get-tuple-element.42), channel_id=1, source_target_pairs={{0,16},{2,18},{4,20},{6,22},{8,24},{10,26},{12,28},{14,30},{16,0},... | collective-permute-start | bytes 196616 | tf_op jit(solution)/shard_map/ppermute | solution.py:21
  62.0 10.8 %collective-permute-start.16 = (f32[16,1024]{1,0:T(8,128)S(1)}, f32[16,1024]{1,0:T(8,128)S(1)}, u32[]{:S(2)}, u32[]{:S(2)}) collective-permute-start(f32[16,1024]{1,0:T(8,128)S(1)} %get-tuple-element.43), channel_id=1, source_target_pairs={{0,24},{2,26},{4,28},{6,30},{8,16},{10,18},{12,20},{14,22},{16,8},... | collective-permute-start | bytes 196616 | tf_op jit(solution)/shard_map/ppermute | solution.py:21
  65.5 10.9 %collective-permute-start.31 = (f32[16,1024]{1,0:T(8,128)S(1)}, f32[16,1024]{1,0:T(8,128)S(1)}, u32[]{:S(2)}, u32[]{:S(2)}) collective-permute-start(f32[16,1024]{1,0:T(8,128)S(1)} %get-tuple-element.28), channel_id=1, source_target_pairs={{0,8},{2,10},{4,12},{6,14},{8,0},{10,2},{12,4},{14,6},{16,24},{18,... | collective-permute-start | bytes 196616 | tf_op jit(solution)/shard_map/ppermute | solution.py:21
  78.1 9.2 %collective-permute-start.34 = (f32[4,16,1024]{2,1,0:T(8,128)S(1)}, f32[4,16,1024]{2,1,0:T(8,128)S(1)}, u32[]{:S(2)}, u32[]{:S(2)}) collective-permute-start(f32[4,16,1024]{2,1,0:T(8,128)S(1)} %pad_maximum_fusion.2.refs_0_), channel_id=1, source_target_pairs={{0,2},{2,0},{4,6},{6,4},{8,10},{10,8},{12,14},{14,12},{16,18},{18,... | collective-permute-start | bytes 786440 | tf_op jit(solution)/shard_map/ppermute | solution.py:21
  79.9 13.1 %collective-permute-start.35 = (f32[4,16,1024]{2,1,0:T(8,128)S(1)}, f32[4,16,1024]{2,1,0:T(8,128)S(1)}, u32[]{:S(2)}, u32[]{:S(2)}) collective-permute-start(f32[4,16,1024]{2,1,0:T(8,128)S(1)} %pad_maximum_fusion.2.refs_0_), channel_id=1, source_target_pairs={{0,4},{2,6},{4,0},{6,2},{8,12},{10,14},{12,8},{14,10},{16,20},{18,... | collective-permute-start | bytes 786440 | tf_op jit(solution)/shard_map/ppermute | solution.py:21
  80.3 13.4 %collective-permute-start.36 = (f32[4,16,1024]{2,1,0:T(8,128)S(1)}, f32[4,16,1024]{2,1,0:T(8,128)}, u32[]{:S(2)}, u32[]{:S(2)}) collective-permute-start(f32[4,16,1024]{2,1,0:T(8,128)S(1)} %pad_maximum_fusion.2.refs_0_), channel_id=1, source_target_pairs={{0,6},{2,4},{4,2},{6,0},{8,14},{10,12},{12,10},{14,8},{16,22},{18,... | collective-permute-start | bytes 786440 | tf_op jit(solution)/shard_map/ppermute | solution.py:21
  83.6 13.0 %collective-permute-start.20 = (f32[4,16,1024]{2,1,0:T(8,128)}, f32[4,16,1024]{2,1,0:T(8,128)}, u32[]{:S(2)}, u32[]{:S(2)}) collective-permute-start(f32[4,16,1024]{2,1,0:T(8,128)} %pad_maximum_fusion.1.refs_0_), channel_id=1, source_target_pairs={{0,2},{2,0},{4,6},{6,4},{8,10},{10,8},{12,14},{14,12},{16,18},{18,... | collective-permute-start | bytes 786440 | tf_op jit(solution)/shard_map/ppermute | solution.py:21
  84.1 14.6 %collective-permute-start.21 = (f32[4,16,1024]{2,1,0:T(8,128)}, f32[4,16,1024]{2,1,0:T(8,128)}, u32[]{:S(2)}, u32[]{:S(2)}) collective-permute-start(f32[4,16,1024]{2,1,0:T(8,128)} %pad_maximum_fusion.1.refs_0_), channel_id=1, source_target_pairs={{0,4},{2,6},{4,0},{6,2},{8,12},{10,14},{12,8},{14,10},{16,20},{18,... | collective-permute-start | bytes 786440 | tf_op jit(solution)/shard_map/ppermute | solution.py:21
  87.4 11.4 %collective-permute-start.22 = (f32[4,16,1024]{2,1,0:T(8,128)}, f32[4,16,1024]{2,1,0:T(8,128)}, u32[]{:S(2)}, u32[]{:S(2)}) collective-permute-start(f32[4,16,1024]{2,1,0:T(8,128)} %pad_maximum_fusion.1.refs_0_), channel_id=1, source_target_pairs={{0,6},{2,4},{4,2},{6,0},{8,14},{10,12},{12,10},{14,8},{16,22},{18,... | collective-permute-start | bytes 786440 | tf_op jit(solution)/shard_map/ppermute | solution.py:21
  105.9 13.9 %collective-permute-start.64 = (bf16[128,1024]{1,0:T(8,128)(2,1)}, bf16[128,1024]{1,0:T(8,128)(2,1)}, u32[]{:S(2)}, u32[]{:S(2)}) collective-permute-start(bf16[128,1024]{1,0:T(8,128)(2,1)} %get-tuple-element.27.refs_0_), channel_id=1, source_target_pairs={{0,8},{2,10},{4,12},{6,14},{8,0},{10,2},{12,4},{14,6},{16,24},{18,... | collective-permute-start | bytes 786440 | tf_op jit(solution)/shard_map/ppermute | solution.py:21
  107.2 12.7 %collective-permute-start.67 = (bf16[128,1024]{1,0:T(8,128)(2,1)}, bf16[128,1024]{1,0:T(8,128)(2,1)}, u32[]{:S(2)}, u32[]{:S(2)}) collective-permute-start(bf16[128,1024]{1,0:T(8,128)(2,1)} %get-tuple-element.27.refs_0_), channel_id=1, source_target_pairs={{0,4},{2,6},{4,0},{6,2},{8,12},{10,14},{12,8},{14,10},{16,20},{18,... | collective-permute-start | bytes 786440 | tf_op jit(solution)/shard_map/ppermute | solution.py:21
  107.7 14.9 %collective-permute-start.53 = (bf16[128,1024]{1,0:T(8,128)(2,1)}, bf16[128,1024]{1,0:T(8,128)(2,1)S(1)}, u32[]{:S(2)}, u32[]{:S(2)}) collective-permute-start(bf16[128,1024]{1,0:T(8,128)(2,1)} %get-tuple-element.27.refs_0_), channel_id=1, source_target_pairs={{0,16},{2,18},{4,20},{6,22},{8,24},{10,26},{12,28},{14,30},{16,0},... | collective-permute-start | bytes 786440 | tf_op jit(solution)/shard_map/ppermute | solution.py:21
  111.8 12.2 %collective-permute-start.46 = (bf16[128,1024]{1,0:T(8,128)(2,1)}, bf16[128,1024]{1,0:T(8,128)(2,1)S(1)}, u32[]{:S(2)}, u32[]{:S(2)}) collective-permute-start(bf16[128,1024]{1,0:T(8,128)(2,1)} %get-tuple-element.26.refs_0_), channel_id=1, source_target_pairs={{0,2},{2,0},{4,6},{6,4},{8,10},{10,8},{12,14},{14,12},{16,18},{18,... | collective-permute-start | bytes 786440 | tf_op jit(solution)/shard_map/ppermute | solution.py:21
  113.5 16.8 %collective-permute-start.49 = (bf16[128,1024]{1,0:T(8,128)(2,1)}, bf16[128,1024]{1,0:T(8,128)(2,1)S(1)}, u32[]{:S(2)}, u32[]{:S(2)}) collective-permute-start(bf16[128,1024]{1,0:T(8,128)(2,1)} %get-tuple-element.26.refs_0_), channel_id=1, source_target_pairs={{0,8},{2,10},{4,12},{6,14},{8,0},{10,2},{12,4},{14,6},{16,24},{18,... | collective-permute-start | bytes 786440 | tf_op jit(solution)/shard_map/ppermute | solution.py:21
  119.9 10.4 %collective-permute-start.52 = (bf16[128,1024]{1,0:T(8,128)(2,1)}, bf16[128,1024]{1,0:T(8,128)(2,1)S(1)}, u32[]{:S(2)}, u32[]{:S(2)}) collective-permute-start(bf16[128,1024]{1,0:T(8,128)(2,1)} %get-tuple-element.26.refs_0_), channel_id=1, source_target_pairs={{0,4},{2,6},{4,0},{6,2},{8,12},{10,14},{12,8},{14,10},{16,20},{18,... | collective-permute-start | bytes 786440 | tf_op jit(solution)/shard_map/ppermute | solution.py:21
  119.9 13.9 %collective-permute-start.38 = (bf16[128,1024]{1,0:T(8,128)(2,1)}, bf16[128,1024]{1,0:T(8,128)(2,1)S(1)}, u32[]{:S(2)}, u32[]{:S(2)}) collective-permute-start(bf16[128,1024]{1,0:T(8,128)(2,1)} %get-tuple-element.26.refs_0_), channel_id=1, source_target_pairs={{0,16},{2,18},{4,20},{6,22},{8,24},{10,26},{12,28},{14,30},{16,0},... | collective-permute-start | bytes 786440 | tf_op jit(solution)/shard_map/ppermute | solution.py:21
  122.6 12.7 %collective-permute-start.62 = (bf16[128,1024]{1,0:T(8,128)(2,1)}, bf16[128,1024]{1,0:T(8,128)(2,1)S(1)}, u32[]{:S(2)}, u32[]{:S(2)}) collective-permute-start(bf16[128,1024]{1,0:T(8,128)(2,1)} %collective-permute-done.61.refs_1_), channel_id=1, source_target_pairs={{0,4},{2,6},{4,0},{6,2},{8,12},{10,14},{12,8},{14,10},{16,20},{18,... | collective-permute-start | bytes 786440 | tf_op jit(solution)/shard_map/ppermute | solution.py:21
  124.0 11.8 %collective-permute-start.65 = (bf16[128,1024]{1,0:T(8,128)(2,1)}, bf16[128,1024]{1,0:T(8,128)(2,1)S(1)}, u32[]{:S(2)}, u32[]{:S(2)}) collective-permute-start(bf16[128,1024]{1,0:T(8,128)(2,1)} %collective-permute-done.64.refs_3_), channel_id=1, source_target_pairs={{0,2},{2,0},{4,6},{6,4},{8,10},{10,8},{12,14},{14,12},{16,18},{18,... | collective-permute-start | bytes 786440 | tf_op jit(solution)/shard_map/ppermute | solution.py:21
  130.3 9.4 %collective-permute-start.66 = (bf16[128,1024]{1,0:T(8,128)(2,1)}, bf16[128,1024]{1,0:T(8,128)(2,1)S(1)}, u32[]{:S(2)}, u32[]{:S(2)}) collective-permute-start(bf16[128,1024]{1,0:T(8,128)(2,1)} %collective-permute-done.64.refs_3_), channel_id=1, source_target_pairs={{0,4},{2,6},{4,0},{6,2},{8,12},{10,14},{12,8},{14,10},{16,20},{18,... | collective-permute-start | bytes 786440 | tf_op jit(solution)/shard_map/ppermute | solution.py:21
  130.3 9.4 %collective-permute-start.54 = (bf16[128,1024]{1,0:T(8,128)(2,1)S(1)}, bf16[128,1024]{1,0:T(8,128)(2,1)}, u32[]{:S(2)}, u32[]{:S(2)}) collective-permute-start(bf16[128,1024]{1,0:T(8,128)(2,1)S(1)} %collective-permute-done.53.refs_3_), channel_id=1, source_target_pairs={{0,8},{2,10},{4,12},{6,14},{8,0},{10,2},{12,4},{14,6},{16,24},{18,... | collective-permute-start | bytes 786440 | tf_op jit(solution)/shard_map/ppermute | solution.py:21
  133.7 11.5 %collective-permute-start.57 = (bf16[128,1024]{1,0:T(8,128)(2,1)S(1)}, bf16[128,1024]{1,0:T(8,128)(2,1)S(1)}, u32[]{:S(2)}, u32[]{:S(2)}) collective-permute-start(bf16[128,1024]{1,0:T(8,128)(2,1)S(1)} %collective-permute-done.53.refs_3_), channel_id=1, source_target_pairs={{0,4},{2,6},{4,0},{6,2},{8,12},{10,14},{12,8},{14,10},{16,20},{18,... | collective-permute-start | bytes 786440 | tf_op jit(solution)/shard_map/ppermute | solution.py:21
  135.3 10.0 %collective-permute-start.60 = (bf16[128,1024]{1,0:T(8,128)(2,1)S(1)}, bf16[128,1024]{1,0:T(8,128)(2,1)S(1)}, u32[]{:S(2)}, u32[]{:S(2)}) collective-permute-start(bf16[128,1024]{1,0:T(8,128)(2,1)S(1)} %collective-permute-done.53.refs_3_), channel_id=1, source_target_pairs={{0,2},{2,0},{4,6},{6,4},{8,10},{10,8},{12,14},{14,12},{16,18},{18,... | collective-permute-start | bytes 786440 | tf_op jit(solution)/shard_map/ppermute | solution.py:21
  135.8 15.0 %collective-permute-start.47 = (bf16[128,1024]{1,0:T(8,128)(2,1)S(1)}, bf16[128,1024]{1,0:T(8,128)(2,1)S(1)}, u32[]{:S(2)}, u32[]{:S(2)}) collective-permute-start(bf16[128,1024]{1,0:T(8,128)(2,1)S(1)} %collective-permute-done.46.refs_1_), channel_id=1, source_target_pairs={{0,4},{2,6},{4,0},{6,2},{8,12},{10,14},{12,8},{14,10},{16,20},{18,... | collective-permute-start | bytes 786440 | tf_op jit(solution)/shard_map/ppermute | solution.py:21
  139.6 11.3 %collective-permute-start.50 = (bf16[128,1024]{1,0:T(8,128)(2,1)S(1)}, bf16[128,1024]{1,0:T(8,128)(2,1)S(1)}, u32[]{:S(2)}, u32[]{:S(2)}) collective-permute-start(bf16[128,1024]{1,0:T(8,128)(2,1)S(1)} %collective-permute-done.49.refs_3_), channel_id=1, source_target_pairs={{0,2},{2,0},{4,6},{6,4},{8,10},{10,8},{12,14},{14,12},{16,18},{18,... | collective-permute-start | bytes 786440 | tf_op jit(solution)/shard_map/ppermute | solution.py:21
  139.7 16.8 %collective-permute-start.51 = (bf16[128,1024]{1,0:T(8,128)(2,1)S(1)}, bf16[128,1024]{1,0:T(8,128)(2,1)S(1)}, u32[]{:S(2)}, u32[]{:S(2)}) collective-permute-start(bf16[128,1024]{1,0:T(8,128)(2,1)S(1)} %collective-permute-done.49.refs_3_), channel_id=1, source_target_pairs={{0,4},{2,6},{4,0},{6,2},{8,12},{10,14},{12,8},{14,10},{16,20},{18,... | collective-permute-start | bytes 786440 | tf_op jit(solution)/shard_map/ppermute | solution.py:21
  145.3 11.2 %collective-permute-start.39 = (bf16[128,1024]{1,0:T(8,128)(2,1)S(1)}, bf16[128,1024]{1,0:T(8,128)(2,1)}, u32[]{:S(2)}, u32[]{:S(2)}) collective-permute-start(bf16[128,1024]{1,0:T(8,128)(2,1)S(1)} %collective-permute-done.38.refs_3_), channel_id=1, source_target_pairs={{0,8},{2,10},{4,12},{6,14},{8,0},{10,2},{12,4},{14,6},{16,24},{18,... | collective-permute-start | bytes 786440 | tf_op jit(solution)/shard_map/ppermute | solution.py:21
  145.3 15.3 %collective-permute-start.42 = (bf16[128,1024]{1,0:T(8,128)(2,1)S(1)}, bf16[128,1024]{1,0:T(8,128)(2,1)S(1)}, u32[]{:S(2)}, u32[]{:S(2)}) collective-permute-start(bf16[128,1024]{1,0:T(8,128)(2,1)S(1)} %collective-permute-done.38.refs_3_), channel_id=1, source_target_pairs={{0,4},{2,6},{4,0},{6,2},{8,12},{10,14},{12,8},{14,10},{16,20},{18,... | collective-permute-start | bytes 786440 | tf_op jit(solution)/shard_map/ppermute | solution.py:21
  150.9 9.7 %collective-permute-start.45 = (bf16[128,1024]{1,0:T(8,128)(2,1)S(1)}, bf16[128,1024]{1,0:T(8,128)(2,1)S(1)}, u32[]{:S(2)}, u32[]{:S(2)}) collective-permute-start(bf16[128,1024]{1,0:T(8,128)(2,1)S(1)} %collective-permute-done.38.refs_3_), channel_id=1, source_target_pairs={{0,2},{2,0},{4,6},{6,4},{8,10},{10,8},{12,14},{14,12},{16,18},{18,... | collective-permute-start | bytes 786440 | tf_op jit(solution)/shard_map/ppermute | solution.py:21
  150.9 9.8 %collective-permute-start.63 = (bf16[128,1024]{1,0:T(8,128)(2,1)S(1)}, bf16[128,1024]{1,0:T(8,128)(2,1)S(1)}, u32[]{:S(2)}, u32[]{:S(2)}) collective-permute-start(bf16[128,1024]{1,0:T(8,128)(2,1)S(1)} %collective-permute-done.62.refs_2_), channel_id=1, source_target_pairs={{0,8},{2,10},{4,12},{6,14},{8,0},{10,2},{12,4},{14,6},{16,24},{18,... | collective-permute-start | bytes 786440 | tf_op jit(solution)/shard_map/ppermute | solution.py:21
  156.5 9.3 %collective-permute-start.58 = (bf16[128,1024]{1,0:T(8,128)(2,1)S(1)}, bf16[128,1024]{1,0:T(8,128)(2,1)}, u32[]{:S(2)}, u32[]{:S(2)}) collective-permute-start(bf16[128,1024]{1,0:T(8,128)(2,1)S(1)} %collective-permute-done.57.refs_1_), channel_id=1, source_target_pairs={{0,2},{2,0},{4,6},{6,4},{8,10},{10,8},{12,14},{14,12},{16,18},{18,... | collective-permute-start | bytes 786440 | tf_op jit(solution)/shard_map/ppermute | solution.py:21
  156.5 14.8 %collective-permute-start.55 = (bf16[128,1024]{1,0:T(8,128)(2,1)}, bf16[128,1024]{1,0:T(8,128)(2,1)S(1)}, u32[]{:S(2)}, u32[]{:S(2)}) collective-permute-start(bf16[128,1024]{1,0:T(8,128)(2,1)} %collective-permute-done.54.refs_3_), channel_id=1, source_target_pairs={{0,2},{2,0},{4,6},{6,4},{8,10},{10,8},{12,14},{14,12},{16,18},{18,... | collective-permute-start | bytes 786440 | tf_op jit(solution)/shard_map/ppermute | solution.py:21
  160.6 10.7 %collective-permute-start.48 = (bf16[128,1024]{1,0:T(8,128)(2,1)S(1)}, bf16[128,1024]{1,0:T(8,128)(2,1)S(1)}, u32[]{:S(2)}, u32[]{:S(2)}) collective-permute-start(bf16[128,1024]{1,0:T(8,128)(2,1)S(1)} %collective-permute-done.47.refs_2_), channel_id=1, source_target_pairs={{0,8},{2,10},{4,12},{6,14},{8,0},{10,2},{12,4},{14,6},{16,24},{18,... | collective-permute-start | bytes 786440 | tf_op jit(solution)/shard_map/ppermute | solution.py:21
  160.7 16.4 %collective-permute-start.43 = (bf16[128,1024]{1,0:T(8,128)(2,1)S(1)}, bf16[128,1024]{1,0:T(8,128)(2,1)}, u32[]{:S(2)}, u32[]{:S(2)}) collective-permute-start(bf16[128,1024]{1,0:T(8,128)(2,1)S(1)} %collective-permute-done.42.refs_1_), channel_id=1, source_target_pairs={{0,2},{2,0},{4,6},{6,4},{8,10},{10,8},{12,14},{14,12},{16,18},{18,... | collective-permute-start | bytes 786440 | tf_op jit(solution)/shard_map/ppermute | solution.py:21
  160.8 29.5 %collective-permute-start.56 = (bf16[128,1024]{1,0:T(8,128)(2,1)}, bf16[128,1024]{1,0:T(8,128)(2,1)}, u32[]{:S(2)}, u32[]{:S(2)}) collective-permute-start(bf16[128,1024]{1,0:T(8,128)(2,1)} %collective-permute-done.54.refs_3_), channel_id=1, source_target_pairs={{0,4},{2,6},{4,0},{6,2},{8,12},{10,14},{12,8},{14,10},{16,20},{18,... | collective-permute-start | bytes 786440 | tf_op jit(solution)/shard_map/ppermute | solution.py:21
  165.8 26.7 %collective-permute-start.40 = (bf16[128,1024]{1,0:T(8,128)(2,1)}, bf16[128,1024]{1,0:T(8,128)(2,1)}, u32[]{:S(2)}, u32[]{:S(2)}) collective-permute-start(bf16[128,1024]{1,0:T(8,128)(2,1)} %collective-permute-done.39.refs_3_), channel_id=1, source_target_pairs={{0,2},{2,0},{4,6},{6,4},{8,10},{10,8},{12,14},{14,12},{16,18},{18,... | collective-permute-start | bytes 786440 | tf_op jit(solution)/shard_map/ppermute | solution.py:21
  171.3 19.0 %collective-permute-start.59 = (bf16[128,1024]{1,0:T(8,128)(2,1)}, bf16[128,1024]{1,0:T(8,128)(2,1)}, u32[]{:S(2)}, u32[]{:S(2)}) collective-permute-start(bf16[128,1024]{1,0:T(8,128)(2,1)} %collective-permute-done.58.refs_2_), channel_id=1, source_target_pairs={{0,8},{2,10},{4,12},{6,14},{8,0},{10,2},{12,4},{14,6},{16,24},{18,... | collective-permute-start | bytes 786440 | tf_op jit(solution)/shard_map/ppermute | solution.py:21
  171.3 21.2 %collective-permute-start.41 = (bf16[128,1024]{1,0:T(8,128)(2,1)}, bf16[128,1024]{1,0:T(8,128)(2,1)}, u32[]{:S(2)}, u32[]{:S(2)}) collective-permute-start(bf16[128,1024]{1,0:T(8,128)(2,1)} %collective-permute-done.39.refs_3_), channel_id=1, source_target_pairs={{0,4},{2,6},{4,0},{6,2},{8,12},{10,14},{12,8},{14,10},{16,20},{18,... | collective-permute-start | bytes 786440 | tf_op jit(solution)/shard_map/ppermute | solution.py:21
  177.1 15.5 %collective-permute-start.44 = (bf16[128,1024]{1,0:T(8,128)(2,1)}, bf16[128,1024]{1,0:T(8,128)(2,1)}, u32[]{:S(2)}, u32[]{:S(2)}) collective-permute-start(bf16[128,1024]{1,0:T(8,128)(2,1)} %collective-permute-done.43.refs_2_), channel_id=1, source_target_pairs={{0,8},{2,10},{4,12},{6,14},{8,0},{10,2},{12,4},{14,6},{16,24},{18,... | collective-permute-start | bytes 786440 | tf_op jit(solution)/shard_map/ppermute | solution.py:21
  (53 other events, 709.0 us)

commit v2 on v1

--- a/solution.py
+++ b/solution.py
@@ -49,6 +49,18 @@
     lines = lax.axis_size("fs") // 4
     line = [swap(own, "fs", 4 * k) for k in range(1, lines)]
     line = jnp.stack([own] + line)
+    return [line] + [swap(line, "fs", c) for c in (1, 2, 3)]
+
+
+def gather_rows(own, me):
+    lines = lax.axis_size("fs") // 4
+    line = [own] + [swap(own, "fs", 4 * k) for k in range(1, lines)]
+    bit = 1
+    while bit < lines:
+        crossed = (me >> 2) & bit > 0
+        line = [jnp.where(crossed, line[k ^ bit], line[k]) for k in range(lines)]
+        bit *= 2
+    line = jnp.concatenate(line)
     return [line] + [swap(line, "fs", c) for c in (1, 2, 3)]
 
 
@@ -128,10 +140,7 @@
     _, vmem, _ = specs()
     return pl.pallas_call(
         kernel,
-        out_shape=(
-            jax.ShapeDtypeStruct(moved.shape, f32),
-            jax.ShapeDtypeStruct(moved.shape, bf16),
-        ),
+        out_shape=(jax.ShapeDtypeStruct(moved.shape, f32), jax.ShapeDtypeStruct(moved.shape, bf16)),
         in_specs=[vmem] * 4,
         out_specs=(vmem, vmem),
         cost_estimate=pl.CostEstimate(
@@ -161,76 +170,54 @@
     return blocks
 
 
-def place_copies(blocks, me):
-    lines = len(blocks) // 4
-    order = []
-    for k in range(lines):
-        order += [4 * k, 4 * k + 1, 4 * k + 2] + [4 * k - 1] * (k > 0)
-    order.append(4 * lines - 1)
-    rows, width = blocks[0].shape
-    out = None
-    for start in range(0, len(order), 4):
-        group = order[start : start + 4]
-
-        def kernel(me_ref, *refs, group=group):
-            sources, out_ref, sems = refs[: len(group)], refs[-2], refs[-1]
+def place_copies(gate, other, me):
+    lines = len(gate) // 4
+    everything = list(range(4 * lines))
+    early = [0, 1, 2, 4]
+    middle = [4 * k + c for k in range(1, lines - 2) for c in (0, 1, 2)]
+    middle += [4 * k for k in range(max(lines - 2, 1), lines)]
+    later = [3] + [4 * k + c for k in range(max(lines - 2, 0), lines - 1) for c in (1, 2)]
+    groups = [(early, early), (middle, middle), (everything[:-1], later), (everything, everything)]
+    rows, width = gate[0].shape
+    shape = jax.ShapeDtypeStruct((4 * lines * rows, width), bf16)
+    smem, vmem, anywhere = specs()
+    outs, placed = (), (set(), set())
+    for masks in groups:
+        todo = []
+        for i in (0, 1):
+            todo += [(i, mask) for mask in masks[i] if mask < 4 * lines and mask not in placed[i]]
+            placed[i].update(masks[i])
+        n = len(todo)
+        if not n:
+            continue
+
+        def kernel(me_ref, *refs, todo=todo, n=n):
+            sources, targets, sems = refs[:n], refs[-3:-1], refs[-1]
             copies = []
-            for i, mask in enumerate(group):
-                target = pl.ds(pl.multiple_of((me_ref[0] ^ mask) * rows, rows), rows)
-                copies.append(pltpu.make_async_copy(sources[i], out_ref.at[target, :], sems.at[i]))
+            for at, (i, mask) in enumerate(todo):
+                owner = me_ref[0] ^ mask
+                rows_at = pl.ds(pl.multiple_of(owner * rows, rows), rows)
+                target = targets[i].at[rows_at, :]
+                copies.append(pltpu.make_async_copy(sources[at], target, sems.at[at]))
                 copies[-1].start()
             for copy in copies:
                 copy.wait()
 
-        smem, vmem, anywhere = specs()
-        n = len(group)
         call = pl.pallas_call(
             kernel,
-            out_shape=jax.ShapeDtypeStruct((len(order) * rows, width), bf16),
-            in_specs=[smem] + [vmem] * n + [anywhere] * (out is not None),
-            out_specs=pl.BlockSpec(memory_space=pltpu.HBM),
+            out_shape=(shape, shape),
+            in_specs=[smem] + [vmem] * n + [anywhere] * len(outs),
+            out_specs=(pl.BlockSpec(memory_space=pltpu.HBM),) * 2,
             scratch_shapes=[pltpu.SemaphoreType.DMA((n,))],
-            input_output_aliases={} if out is None else {1 + n: 0},
+            input_output_aliases={1 + n + i: i for i in range(len(outs))},
             cost_estimate=pl.CostEstimate(
                 flops=0, bytes_accessed=4 * n * rows * width, transcendentals=0
             ),
             name="place_copies",
         )
-        out = call(
-            me.astype(jnp.int32).reshape(1),
-            *(blocks[mask] for mask in group),
-            *([] if out is None else [out]),
-        )
-    return out
-
-
-def order_factors(mine, other, me, core):
-    lines, rows, columns = mine[0].shape
-    count = 4 * lines
-
-    def kernel(me_ref, core_ref, *refs):
-        sources, (out_in, out_gate) = refs[:-2], refs[-2:]
-        first = core_ref[0] == 0
-        for c in range(4):
-            for k in range(lines):
-                owner = me_ref[0] ^ (4 * k + c)
-                target = pl.ds(pl.multiple_of(owner * rows, rows), rows)
-                a, b = sources[c][k], sources[4 + c][k]
-                out_in[target, :] = jnp.where(first, a, b)
-                out_gate[target, :] = jnp.where(first, b, a)
-
-    smem, vmem = (pl.BlockSpec(memory_space=space) for space in (pltpu.SMEM, pltpu.VMEM))
-    shape = jax.ShapeDtypeStruct((count * rows, columns), mine[0].dtype)
-    return pl.pallas_call(
-        kernel,
-        out_shape=(shape, shape),
-        in_specs=[smem, smem] + [vmem] * 8,
-        out_specs=(vmem, vmem),
-        cost_estimate=pl.CostEstimate(
-            flops=0, bytes_accessed=8 * count * rows * columns, transcendentals=0
-        ),
-        name="order_factors",
-    )(me.astype(jnp.int32).reshape(1), core.astype(jnp.int32).reshape(1), *mine, *other)
+        blocks = [(gate, other)[i][mask] for i, mask in todo]
+        outs = call(me.astype(jnp.int32).reshape(1), *blocks, *outs)
+    return outs
 
 
 def local(
@@ -256,15 +243,21 @@
     count = fs * input_master.shape[0] * tp * width
 
     if tp == 2:
-        mine = gather(jnp.where(core == 0, input_factor, gate_factor))
-        other = [swap(stack, "tp", 1) for stack in mine]
-        whole_in, whole_gate = order_factors(mine, other, me, core)
+        mine = gather_rows(jnp.where(core == 0, input_factor, gate_factor), me)
+        other = [swap(piece, "tp", 1) for piece in mine]
+        factors_in = [jnp.where(core == 0, a, b) for a, b in zip(mine, other)]
+        factors_gate = [jnp.where(core == 0, b, a) for a, b in zip(mine, other)]
     else:
-        zero = jnp.zeros_like(core)
-        whole_in, whole_gate = order_factors(gather(input_factor), gather(gate_factor), me, zero)
-
-    def chain(cot, master, own_factor, factor, first, second):
-        projected = split(dot(saved_inputs, factor, plain), 2)
+        factors_in = gather_rows(input_factor, me)
+        factors_gate = gather_rows(gate_factor, me)
+    columns = saved_inputs.reshape(-1, lines, 4, input_factor.shape[0])
+    columns = [pick(columns, (me & 3) ^ c, 2).reshape(saved_inputs.shape[0], -1) for c in range(4)]
+
+    def chain(cot, master, own_factor, factors, first, second):
+        projected = 0.0
+        for c in range(4):
+            projected += dot(columns[c], factors[c], plain)
+        projected = split(projected, 2)
         term = sum(dot(piece, cot, contract) for piece in projected)
         term = term.reshape(lines, 2, 2, rank // fs, width)
         left, right = term[..., :half], term[..., half:]
@@ -278,22 +271,23 @@
             low_rank = low_rank + swap(pick(both, here_z ^ k, 0), "fs", 4 * k)
         first_new, second_new, ratio = moments(low_rank, first, second)
         stacks = gather(ratio)
-        gram = dot(factor, factor, contract)
+        gram = sum(dot(piece, piece, contract) for piece in factors)
         moved, square = directions(stacks, gram, own_factor, me)
         if tp == 2:
             others = swap(square, "tp", 1)
         else:
             others = lax.psum(square, "tp") - square
         step, local_copy = finish(moved, square, others, master, count)
-        copy = place_copies(spread(local_copy), me)
-        return step, first_new, second_new, copy
-
-    step_gate, first_gate, second_gate, copy_gate = chain(
-        gate_cot, gate_master, gate_factor, whole_gate, gate_first, gate_second
+        blocks = spread(local_copy)
+        return step, first_new, second_new, blocks
+
+    step_gate, first_gate, second_gate, blocks_gate = chain(
+        gate_cot, gate_master, gate_factor, factors_gate, gate_first, gate_second
     )
-    step_in, first_in, second_in, copy_in = chain(
-        input_cot, input_master, input_factor, whole_in, input_first, input_second
+    step_in, first_in, second_in, blocks_in = chain(
+        input_cot, input_master, input_factor, factors_in, input_first, input_second
     )
+    copy_gate, copy_in = place_copies(blocks_gate, blocks_in, me)
     return (step_in, step_gate, first_in, second_in, first_gate, second_gate, copy_in, copy_gate)
 
 

time: 195 us -> 196 us (level)
  Pallas kernels: 30.6 us -> 21.7 us
  local copies, waits for them, and re-layouts: 2.35 us -> 10.8 us
  starting transfers between devices: 61.4 us -> 69.2 us
  waiting for transfers between devices: 87.5 us -> 80.4 us
    pallas_call x9 -> x4, Pallas kernels: 20.4 us -> 11.5 us  [place_copies(): outs = call(me.astype(jnp.int32).reshape(1), *blocks, *outs)]
    ppermute x68, starting transfers between devices: 61.4 us -> 69.2 us  [swap(): return lax.ppermute(a, axis, [(i, i ^ mask) for i in range(size)])]
    ppermute x68, waiting for transfers between devices: 87.5 us -> 80.4 us  [swap(): return lax.ppermute(a, axis, [(i, i ^ mask) for i in range(size)])]
    unnamed x66 -> x73, local copies, waits for them, and re-layouts: 2.03 us -> 8.4 us
    dynamic_slice x0 -> x1, local copies, waits for them, and re-layouts: none -> 2.12 us  [pick(): return lax.dynamic_index_in_dim(a, index, axis, keepdims=False)]
    dot_general x8 -> x20, matrix products: 8.13 us -> 9.36 us  [dot(): return lax.dot_general(a, b, dims, preferred_element_type=f32)]
  transfers between devices with their start and end apart: 68 -> 68, of which waited for: 29 -> 27; matrix products, arithmetic and copies ran while one was open for 4% -> 8% of each run, Pallas kernels for 13% -> 10%
where the time goes in v2:
time: 196 us
  waiting for transfers between devices  80.4 us (41%)
  starting transfers between devices  69.2 us (35%)
  Pallas kernels  21.7 us (11%)
  local copies, waits for them, and re-layouts  10.8 us (6%)
  matrix products  9.36 us (5%)
  other arithmetic  2.72 us (1%)
    ppermute x68, waiting for transfers between devices, swap(): return lax.ppermute(a, axis, [(i, i ^ mask) for i in range(size)])  80.4 us
    ppermute x68, starting transfers between devices, swap(): return lax.ppermute(a, axis, [(i, i ^ mask) for i in range(size)])  69.2 us
    pallas_call x4, Pallas kernels, place_copies(): outs = call(me.astype(jnp.int32).reshape(1), *blocks, *outs)  11.5 us
    dot_general x20, matrix products, dot(): return lax.dot_general(a, b, dims, preferred_element_type=f32)  9.36 us
    unnamed x73, local copies, waits for them, and re-layouts  8.4 us
    pallas_call x2, Pallas kernels, directions(): pl.pallas_call(kernel, out_shape=(jax.ShapeDtypeStruct((factor.shape[0],...  5.76 us
    pallas_call x2, Pallas kernels, finish(): pl.pallas_call(kernel, out_shape=(jax.ShapeDtypeStruct(moved.shape, f32),...  4.4 us
  transfers between devices with their start and end apart: 68, of which 27 were waited for; matrix products, arithmetic and copies ran while one was open for 8% of the time, Pallas kernels for 10%

profile of v2, /device:TPU:0, one launch (start us, length us, event | category | flops | bytes accessed | tf_op | source)
XLA Modules:
  0.0 195.7 jit_solution(16087641487202547459)
XLA Ops:
  1.6 5.1 %collective-permute-start = (bf16[128,256]{1,0:T(8,128)(2,1)S(1)}, bf16[128,256]{1,0:T(8,128)(2,1)S(1)}, u32[]{:S(2)}, u32[]{:S(2)}) collective-permute-start(bf16[128,256]{1,0:T(8,128)(2,1)S(1)} %broadcast_select_fusion.24), channel_id=1, source_target_pairs={{0,24},{2,26},{4,28},{6,30},{8,16},{10,18},{12,20},{14,22},{16,8},... | collective-permute-start | bytes 196616 | tf_op jit(solution)/shard_map/ppermute | solution.py:21
  7.4 1.8 collective-permute-done
  9.3 3.1 %collective-permute-done.1 = bf16[128,256]{1,0:T(8,128)(2,1)S(1)} collective-permute-done((bf16[128,256]{1,0:T(8,128)(2,1)S(1)}, bf16[128,256]{1,0:T(8,128)(2,1)S(1)}, u32[]{:S(2)}, u32[]{:S(2)}) %collective-permute-start.1) | collective-permute-done | bytes 65568 | tf_op jit(solution)/shard_map/ppermute | solution.py:21
  12.4 1.6 collective-permute-start.4
  14.0 4.6 %copy.29 = bf16[768,2048]{0,1:T(8,128)(2,1)} copy(bf16[768,2048]{1,0:T(8,128)(2,1)} %param.11) | data formatting | bytes 6291456 | tf_op args[0]
  18.6 2.1 %constant_dynamic-slice_fusion.1 = (bf16[768,4,1,128]{0,3,2,1:T(8,128)(2,1)S(1)}, bf16[768,4,1,128]{0,3,2,1:T(8,128)(2,1)S(1)}, bf16[768,4,1,128]{0,3,2,1:T(8,128)(2,1)S(1)}, bf16[768,4,1,128]{0,3,2,1:T(8,128)(2,1)S(1)}) fusion(bf16[768,4,4,128]{0,3,2,1:T(8,128)(2,1)} %bitcast.104, s32[]{:T(128)S(6)} %select_n.156, s32[]{:T(128)S(6)} %select_n.157, ...), kind=kLoop, calls=%fused_computation.115 | loop fusion | bytes 6291472 | tf_op jit(solution)/shard_map/jit(dynamic_index_in_dim)/dynamic_slice | solution.py:45
  20.8 1.6 collective-permute-start.8
  23.4 7.1 %collective-permute-done.8 = bf16[512,256]{1,0:T(8,128)(2,1)S(1)} collective-permute-done((bf16[512,256]{1,0:T(8,128)(2,1)S(1)}, bf16[512,256]{1,0:T(8,128)(2,1)S(1)}, u32[]{:S(2)}, u32[]{:S(2)}) %collective-permute-start.8) | collective-permute-done | bytes 262176 | tf_op jit(solution)/shard_map/ppermute | solution.py:21
  31.0 5.1 %collective-permute-done.6 = bf16[512,256]{1,0:T(8,128)(2,1)S(1)} collective-permute-done((bf16[512,256]{1,0:T(8,128)(2,1)S(1)}, bf16[512,256]{1,0:T(8,128)(2,1)S(1)}, u32[]{:S(2)}, u32[]{:S(2)}) %collective-permute-start.6) | collective-permute-done | bytes 262176 | tf_op jit(solution)/shard_map/ppermute | solution.py:21
  45.8 1.5 collective-permute-start.10
  49.9 1.6 collective-permute-start.25
  51.5 2.9 %collective-permute-done.12 = f32[4,2,16,512]{3,2,1,0:T(8,128)S(1)} collective-permute-done((f32[4,2,16,512]{3,2,1,0:T(8,128)S(1)}, f32[4,2,16,512]{3,2,1,0:T(8,128)S(1)}, u32[]{:S(2)}, u32[]{:S(2)}) %collective-permute-start.12) | collective-permute-done | bytes 262176 | tf_op jit(solution)/shard_map/ppermute | solution.py:21
  59.1 2.2 %collective-permute-start.29 = (f32[16,1024]{1,0:T(8,128)S(1)}, f32[16,1024]{1,0:T(8,128)S(1)}, u32[]{:S(2)}, u32[]{:S(2)}) collective-permute-start(f32[16,1024]{1,0:T(8,128)S(1)} %get-tuple-element.55), channel_id=1, source_target_pairs={{0,16},{2,18},{4,20},{6,22},{8,24},{10,26},{12,28},{14,30},{16,0},... | collective-permute-start | bytes 196616 | tf_op jit(solution)/shard_map/ppermute | solution.py:21
  62.7 3.1 %collective-permute-start.15 = (f32[16,1024]{1,0:T(8,128)S(1)}, f32[16,1024]{1,0:T(8,128)S(1)}, u32[]{:S(2)}, u32[]{:S(2)}) collective-permute-start(f32[16,1024]{1,0:T(8,128)S(1)} %get-tuple-element.58), channel_id=1, source_target_pairs={{0,16},{2,18},{4,20},{6,22},{8,24},{10,26},{12,28},{14,30},{16,0},... | collective-permute-start | bytes 196616 | tf_op jit(solution)/shard_map/ppermute | solution.py:21
  69.0 4.9 %collective-permute-start.31 = (f32[16,1024]{1,0:T(8,128)S(1)}, f32[16,1024]{1,0:T(8,128)S(1)}, u32[]{:S(2)}, u32[]{:S(2)}) collective-permute-start(f32[16,1024]{1,0:T(8,128)S(1)} %get-tuple-element.40), channel_id=1, source_target_pairs={{0,8},{2,10},{4,12},{6,14},{8,0},{10,2},{12,4},{14,6},{16,24},{18,... | collective-permute-start | bytes 196616 | tf_op jit(solution)/shard_map/ppermute | solution.py:21
  73.9 2.4 %collective-permute-start.33 = (f32[16,1024]{1,0:T(8,128)S(1)}, f32[16,1024]{1,0:T(8,128)S(1)}, u32[]{:S(2)}, u32[]{:S(2)}) collective-permute-start(f32[16,1024]{1,0:T(8,128)S(1)} %get-tuple-element.40), channel_id=1, source_target_pairs={{0,24},{2,26},{4,28},{6,30},{8,16},{10,18},{12,20},{14,22},{16,8},... | collective-permute-start | bytes 196616 | tf_op jit(solution)/shard_map/ppermute | solution.py:21
  79.1 2.4 %collective-permute-start.19 = (f32[16,1024]{1,0:T(8,128)S(1)}, f32[16,1024]{1,0:T(8,128)S(1)}, u32[]{:S(2)}, u32[]{:S(2)}) collective-permute-start(f32[16,1024]{1,0:T(8,128)S(1)} %get-tuple-element.43), channel_id=1, source_target_pairs={{0,24},{2,26},{4,28},{6,30},{8,16},{10,18},{12,20},{14,22},{16,8},... | collective-permute-start | bytes 196616 | tf_op jit(solution)/shard_map/ppermute | solution.py:21
  83.1 2.3 %collective-permute-start.36 = (f32[4,16,1024]{2,1,0:T(8,128)S(1)}, f32[4,16,1024]{2,1,0:T(8,128)S(1)}, u32[]{:S(2)}, u32[]{:S(2)}) collective-permute-start(f32[4,16,1024]{2,1,0:T(8,128)S(1)} %pad_maximum_fusion.2.refs_0_), channel_id=1, source_target_pairs={{0,6},{2,4},{4,2},{6,0},{8,14},{10,12},{12,10},{14,8},{16,22},{18,... | collective-permute-start | bytes 786440 | tf_op jit(solution)/shard_map/ppermute | solution.py:21
  86.8 4.0 %collective-permute-done.34.refs_1_ = f32[4,16,1024]{2,1,0:T(8,128)S(1)} collective-permute-done((f32[4,16,1024]{2,1,0:T(8,128)S(1)}, f32[4,16,1024]{2,1,0:T(8,128)S(1)}, u32[]{:S(2)}, u32[]{:S(2)}) %collective-permute-start.34) | collective-permute-done | bytes 262176 | tf_op jit(solution)/shard_map/ppermute | solution.py:21
  91.8 4.2 %collective-permute-done.35.refs_2_ = f32[4,16,1024]{2,1,0:T(8,128)S(1)} collective-permute-done((f32[4,16,1024]{2,1,0:T(8,128)S(1)}, f32[4,16,1024]{2,1,0:T(8,128)S(1)}, u32[]{:S(2)}, u32[]{:S(2)}) %collective-permute-start.35) | collective-permute-done | bytes 262176 | tf_op jit(solution)/shard_map/ppermute | solution.py:21
  96.8 2.9 %directions.3 = (f32[128,1024]{1,0:T(8,128)}, f32[8,128]{1,0:T(8,128)}) custom-call(s32[1]{0:T(128)} %bitcast.me_ref, f32[256,256]{1,0:T(8,128)} %fusion.2.gram_ref, bf16[128,256]{1,0:T(8,128)(2,1)} %factor_ref.3, f32[4,16,1024]{2,1,0:T(8,128)} %copy-done.16, f32[4,16,1024]{2,1,0:T(8,128)} %copy-done.31, f32[4,16,1024]{2,1,0:T(8,128)} %copy-done.32, ...), custom_call_target="tpu_custom_call" | custom-call | flops 603979776 | bytes 2097152 | tf_op jit(solution)/shard_map/directions/pallas_call | solution.py:115
  99.7 1.9 collective-permute-done.21.refs_2_
  102.3 2.9 %directions.2 = (f32[128,1024]{1,0:T(8,128)}, f32[8,128]{1,0:T(8,128)}) custom-call(s32[1]{0:T(128)} %bitcast.me_ref, f32[256,256]{1,0:T(8,128)} %fusion.3.gram_ref, bf16[128,256]{1,0:T(8,128)(2,1)} %factor_ref.2, f32[4,16,1024]{2,1,0:T(8,128)} %copy-done.17, f32[4,16,1024]{2,1,0:T(8,128)} %copy-done.33, f32[4,16,1024]{2,1,0:T(8,128)} %copy-done.35, ...), custom_call_target="tpu_custom_call" | custom-call | flops 603979776 | bytes 2097152 | tf_op jit(solution)/shard_map/directions/pallas_call | solution.py:115
  105.8 2.2 %finish.3 = (f32[128,1024]{1,0:T(8,128)}, bf16[128,1024]{1,0:T(8,128)(2,1)}) custom-call(f32[128,1024]{1,0:T(8,128)} %get-tuple-element.27.moved_ref, f32[8,128]{1,0:T(8,128)} %get-tuple-element.28.square_ref, f32[8,128]{1,0:T(8,128)} %copy-done.30, f32[128,1024]{1,0:T(8,128)} %master_ref.3), custom_call_target="tpu_custom_call" | custom-call | flops 524288 | bytes 1835008 | tf_op jit(solution)/shard_map/finish/pallas_call | solution.py:141
  108.0 1.5 collective-permute-start.52
  109.5 1.6 collective-permute-start.60
  113.5 2.2 %finish.2 = (f32[128,1024]{1,0:T(8,128)}, bf16[128,1024]{1,0:T(8,128)(2,1)}) custom-call(f32[128,1024]{1,0:T(8,128)} %get-tuple-element.24.moved_ref, f32[8,128]{1,0:T(8,128)} %get-tuple-element.25.square_ref, f32[8,128]{1,0:T(8,128)} %copy-done.29, f32[128,1024]{1,0:T(8,128)} %master_ref.2), custom_call_target="tpu_custom_call" | custom-call | flops 524288 | bytes 1835008 | tf_op jit(solution)/shard_map/finish/pallas_call | solution.py:141
  118.3 4.7 %collective-permute-done.60.refs_3_ = bf16[128,1024]{1,0:T(8,128)(2,1)S(1)} collective-permute-done((bf16[128,1024]{1,0:T(8,128)(2,1)}, bf16[128,1024]{1,0:T(8,128)(2,1)S(1)}, u32[]{:S(2)}, u32[]{:S(2)}) %collective-permute-start.60) | collective-permute-done | bytes 262176 | tf_op jit(solution)/shard_map/ppermute | solution.py:21
  124.1 2.9 %collective-permute-done.38.refs_2_ = bf16[128,1024]{1,0:T(8,128)(2,1)S(1)} collective-permute-done((bf16[128,1024]{1,0:T(8,128)(2,1)}, bf16[128,1024]{1,0:T(8,128)(2,1)S(1)}, u32[]{:S(2)}, u32[]{:S(2)}) %collective-permute-start.38) | collective-permute-done | bytes 262176 | tf_op jit(solution)/shard_map/ppermute | solution.py:21
  127.9 6.4 %collective-permute-done.63.refs_7_ = bf16[128,1024]{1,0:T(8,128)(2,1)S(1)} collective-permute-done((bf16[128,1024]{1,0:T(8,128)(2,1)}, bf16[128,1024]{1,0:T(8,128)(2,1)S(1)}, u32[]{:S(2)}, u32[]{:S(2)}) %collective-permute-start.63) | collective-permute-done | bytes 262176 | tf_op jit(solution)/shard_map/ppermute | solution.py:21
  134.3 3.3 %collective-permute-done.45.refs_6_ = bf16[128,1024]{1,0:T(8,128)(2,1)S(1)} collective-permute-done((bf16[128,1024]{1,0:T(8,128)(2,1)}, bf16[128,1024]{1,0:T(8,128)(2,1)S(1)}, u32[]{:S(2)}, u32[]{:S(2)}) %collective-permute-start.45) | collective-permute-done | bytes 262176 | tf_op jit(solution)/shard_map/ppermute | solution.py:21
  138.4 3.0 %collective-permute-done.56.refs_3_ = bf16[128,1024]{1,0:T(8,128)(2,1)S(1)} collective-permute-done((bf16[128,1024]{1,0:T(8,128)(2,1)S(1)}, bf16[128,1024]{1,0:T(8,128)(2,1)S(1)}, u32[]{:S(2)}, u32[]{:S(2)}) %collective-permute-start.56) | collective-permute-done | bytes 262176 | tf_op jit(solution)/shard_map/ppermute | solution.py:21
  141.7 1.8 collective-permute-start.39
  144.1 2.2 %collective-permute-done.48.refs_7_ = bf16[128,1024]{1,0:T(8,128)(2,1)} collective-permute-done((bf16[128,1024]{1,0:T(8,128)(2,1)S(1)}, bf16[128,1024]{1,0:T(8,128)(2,1)}, u32[]{:S(2)}, u32[]{:S(2)}) %collective-permute-start.48) | collective-permute-done | bytes 262176 | tf_op jit(solution)/shard_map/ppermute | solution.py:21
  147.4 3.1 %collective-permute-done.65.refs_5_ = bf16[128,1024]{1,0:T(8,128)(2,1)S(1)} collective-permute-done((bf16[128,1024]{1,0:T(8,128)(2,1)S(1)}, bf16[128,1024]{1,0:T(8,128)(2,1)S(1)}, u32[]{:S(2)}, u32[]{:S(2)}) %collective-permute-start.65) | collective-permute-done | bytes 262176 | tf_op jit(solution)/shard_map/ppermute | solution.py:21
  150.8 5.3 %collective-permute-done.39.refs_3_ = bf16[128,1024]{1,0:T(8,128)(2,1)S(1)} collective-permute-done((bf16[128,1024]{1,0:T(8,128)(2,1)}, bf16[128,1024]{1,0:T(8,128)(2,1)S(1)}, u32[]{:S(2)}, u32[]{:S(2)}) %collective-permute-start.39) | collective-permute-done | bytes 262176 | tf_op jit(solution)/shard_map/ppermute | solution.py:21
  156.7 5.1 %collective-permute-done.53.refs_0_ = bf16[128,1024]{1,0:T(8,128)(2,1)S(1)} collective-permute-done((bf16[128,1024]{1,0:T(8,128)(2,1)S(1)}, bf16[128,1024]{1,0:T(8,128)(2,1)S(1)}, u32[]{:S(2)}, u32[]{:S(2)}) %collective-permute-start.53) | collective-permute-done | bytes 262176 | tf_op jit(solution)/shard_map/ppermute | solution.py:21
  162.3 1.6 collective-permute-start.54
  163.9 3.6 %collective-permute-done.43.refs_7_ = bf16[128,1024]{1,0:T(8,128)(2,1)} collective-permute-done((bf16[128,1024]{1,0:T(8,128)(2,1)S(1)}, bf16[128,1024]{1,0:T(8,128)(2,1)}, u32[]{:S(2)}, u32[]{:S(2)}) %collective-permute-start.43) | collective-permute-done | bytes 262176 | tf_op jit(solution)/shard_map/ppermute | solution.py:21
  168.0 2.7 %collective-permute-done.46.refs_9_ = bf16[128,1024]{1,0:T(8,128)(2,1)S(1)} collective-permute-done((bf16[128,1024]{1,0:T(8,128)(2,1)S(1)}, bf16[128,1024]{1,0:T(8,128)(2,1)S(1)}, u32[]{:S(2)}, u32[]{:S(2)}) %collective-permute-start.46) | collective-permute-done | bytes 262176 | tf_op jit(solution)/shard_map/ppermute | solution.py:21
  173.2 1.6 collective-permute-start.50
  176.3 1.8 collective-permute-start.44
  179.6 1.7 collective-permute-start.41
  182.0 1.9 collective-permute-start.51
  183.9 2.9 %place_copies.4 = (bf16[2048,1024]{1,0:T(8,128)(2,1)}, bf16[2048,1024]{1,0:T(8,128)(2,1)}) custom-call(s32[1]{0:T(128)} %bitcast.me_ref, bf16[128,1024]{1,0:T(8,128)(2,1)} %get-tuple-element.30.refs_0_, bf16[128,1024]{1,0:T(8,128)(2,1)} %copy-done.2, bf16[128,1024]{1,0:T(8,128)(2,1)} %copy-done.4, bf16[128,1024]{1,0:T(8,128)(2,1)} %copy-done.3, ...), custom_call_target="tpu_custom_call" | custom-call | bytes 4194304 | tf_op jit(solution)/shard_map/place_copies/pallas_call | solution.py:219
  186.8 2.9 %place_copies.5 = (bf16[2048,1024]{1,0:T(8,128)(2,1)}, bf16[2048,1024]{1,0:T(8,128)(2,1)}) custom-call(s32[1]{0:T(128)} %bitcast.me_ref, bf16[128,1024]{1,0:T(8,128)(2,1)} %copy-done.21, bf16[128,1024]{1,0:T(8,128)(2,1)} %copy-done.22, bf16[128,1024]{1,0:T(8,128)(2,1)} %copy-done.18, ...), custom_call_target="tpu_custom_call", output_to_operand_aliasing={{0}: (9, {}), {1}: (10, {})} | custom-call | bytes 4194304 | tf_op jit(solution)/shard_map/place_copies/pallas_call | solution.py:219
  189.7 3.2 %place_copies.6 = (bf16[2048,1024]{1,0:T(8,128)(2,1)}, bf16[2048,1024]{1,0:T(8,128)(2,1)}) custom-call(s32[1]{0:T(128)} %bitcast.me_ref, bf16[128,1024]{1,0:T(8,128)(2,1)} %copy-done.9, bf16[128,1024]{1,0:T(8,128)(2,1)} %copy-done.13, bf16[128,1024]{1,0:T(8,128)(2,1)} %copy-done.10, ...), custom_call_target="tpu_custom_call", output_to_operand_aliasing={{0}: (11, {}), {1}: (12, {})} | custom-call | bytes 5242880 | tf_op jit(solution)/shard_map/place_copies/pallas_call | solution.py:219
  193.0 2.5 %place_copies.7 = (bf16[2048,1024]{1,0:T(8,128)(2,1)}, bf16[2048,1024]{1,0:T(8,128)(2,1)}) custom-call(s32[1]{0:T(128)} %bitcast.me_ref, bf16[128,1024]{1,0:T(8,128)(2,1)} %collective-permute-done.41.refs_0_, bf16[128,1024]{1,0:T(8,128)(2,1)} %collective-permute-done.44.refs_1_, ...), custom_call_target="tpu_custom_call", output_to_operand_aliasing={{0}: (7, {}), {1}: (8, {})} | custom-call | bytes 3145728 | tf_op jit(solution)/shard_map/place_copies/pallas_call | solution.py:219
  (217 shorter events, 51.1 us)
Async XLA Ops:
  12.4 10.4 %collective-permute-start.4 = (bf16[512,256]{1,0:T(8,128)(2,1)S(1)}, bf16[512,256]{1,0:T(8,128)(2,1)S(1)}, u32[]{:S(2)}, u32[]{:S(2)}) collective-permute-start(bf16[512,256]{1,0:T(8,128)(2,1)S(1)} %pad_maximum_fusion), channel_id=1, source_target_pairs={{0,2},{2,0},{4,6},{6,4},{8,10},{10,8},{12,14},{14,12},{16,18},{18,... | collective-permute-start | bytes 786440 | tf_op jit(solution)/shard_map/ppermute | solution.py:21
  14.0 8.8 %collective-permute-start.3 = (bf16[512,256]{1,0:T(8,128)(2,1)S(1)}, bf16[512,256]{1,0:T(8,128)(2,1)S(1)}, u32[]{:S(2)}, u32[]{:S(2)}) collective-permute-start(bf16[512,256]{1,0:T(8,128)(2,1)S(1)} %pad_maximum_fusion), channel_id=1, source_target_pairs={{0,1},{1,0},{2,3},{3,2},{4,5},{5,4},{6,7},{7,6},{8,9},{9,8},{10,11... | collective-permute-start | bytes 786440 | tf_op jit(solution)/shard_map/ppermute | solution.py:21
  20.8 9.8 %collective-permute-start.8 = (bf16[512,256]{1,0:T(8,128)(2,1)S(1)}, bf16[512,256]{1,0:T(8,128)(2,1)S(1)}, u32[]{:S(2)}, u32[]{:S(2)}) collective-permute-start(bf16[512,256]{1,0:T(8,128)(2,1)S(1)} %pad_maximum_fusion), channel_id=1, source_target_pairs={{0,6},{2,4},{4,2},{6,0},{8,14},{10,12},{12,10},{14,8},{16,22},{18,... | collective-permute-start | bytes 786440 | tf_op jit(solution)/shard_map/ppermute | solution.py:21
  22.3 13.7 %collective-permute-start.6 = (bf16[512,256]{1,0:T(8,128)(2,1)S(1)}, bf16[512,256]{1,0:T(8,128)(2,1)S(1)}, u32[]{:S(2)}, u32[]{:S(2)}) collective-permute-start(bf16[512,256]{1,0:T(8,128)(2,1)S(1)} %pad_maximum_fusion), channel_id=1, source_target_pairs={{0,4},{2,6},{4,0},{6,2},{8,12},{10,14},{12,8},{14,10},{16,20},{18,... | collective-permute-start | bytes 786440 | tf_op jit(solution)/shard_map/ppermute | solution.py:21
  22.8 13.7 %collective-permute-start.5 = (bf16[512,256]{1,0:T(8,128)(2,1)S(1)}, bf16[512,256]{1,0:T(8,128)(2,1)S(1)}, u32[]{:S(2)}, u32[]{:S(2)}) collective-permute-start(bf16[512,256]{1,0:T(8,128)(2,1)S(1)} %collective-permute-done.4), channel_id=1, source_target_pairs={{0,1},{1,0},{2,3},{3,2},{4,5},{5,4},{6,7},{7,6},{8,9},{9,8},{10,11... | collective-permute-start | bytes 786440 | tf_op jit(solution)/shard_map/ppermute | solution.py:21
  39.4 9.8 %collective-permute-start.26 = (f32[4,2,16,512]{3,2,1,0:T(8,128)S(1)}, f32[4,2,16,512]{3,2,1,0:T(8,128)S(1)}, u32[]{:S(2)}, u32[]{:S(2)}) collective-permute-start(f32[4,2,16,512]{3,2,1,0:T(8,128)S(1)} %dynamic-slice_bitcast_fusion), channel_id=1, source_target_pairs={{0,4},{2,6},{4,0},{6,2},{8,12},{10,14},{12,8},{14,10},{16,20},{18,... | collective-permute-start | bytes 786440 | tf_op jit(solution)/shard_map/ppermute | solution.py:21
  40.3 9.5 %collective-permute-start.24 = (f32[4,2,16,512]{3,2,1,0:T(8,128)S(1)}, f32[4,2,16,512]{3,2,1,0:T(8,128)S(1)}, u32[]{:S(2)}, u32[]{:S(2)}) collective-permute-start(f32[4,2,16,512]{3,2,1,0:T(8,128)S(1)} %dynamic-slice_bitcast_fusion.1), channel_id=1, source_target_pairs={{0,2},{2,0},{4,6},{6,4},{8,10},{10,8},{12,14},{14,12},{16,18},{18,... | collective-permute-start | bytes 786440 | tf_op jit(solution)/shard_map/ppermute | solution.py:21
  45.2 9.2 %collective-permute-start.12 = (f32[4,2,16,512]{3,2,1,0:T(8,128)S(1)}, f32[4,2,16,512]{3,2,1,0:T(8,128)S(1)}, u32[]{:S(2)}, u32[]{:S(2)}) collective-permute-start(f32[4,2,16,512]{3,2,1,0:T(8,128)S(1)} %dynamic-slice_bitcast_fusion.2), channel_id=1, source_target_pairs={{0,4},{2,6},{4,0},{6,2},{8,12},{10,14},{12,8},{14,10},{16,20},{18,... | collective-permute-start | bytes 786440 | tf_op jit(solution)/shard_map/ppermute | solution.py:21
  45.8 9.6 %collective-permute-start.10 = (f32[4,2,16,512]{3,2,1,0:T(8,128)S(1)}, f32[4,2,16,512]{3,2,1,0:T(8,128)S(1)}, u32[]{:S(2)}, u32[]{:S(2)}) collective-permute-start(f32[4,2,16,512]{3,2,1,0:T(8,128)S(1)} %dynamic-slice_bitcast_fusion.3), channel_id=1, source_target_pairs={{0,2},{2,0},{4,6},{6,4},{8,10},{10,8},{12,14},{14,12},{16,18},{18,... | collective-permute-start | bytes 786440 | tf_op jit(solution)/shard_map/ppermute | solution.py:21
  59.1 9.2 %collective-permute-start.29 = (f32[16,1024]{1,0:T(8,128)S(1)}, f32[16,1024]{1,0:T(8,128)S(1)}, u32[]{:S(2)}, u32[]{:S(2)}) collective-permute-start(f32[16,1024]{1,0:T(8,128)S(1)} %get-tuple-element.55), channel_id=1, source_target_pairs={{0,16},{2,18},{4,20},{6,22},{8,24},{10,26},{12,28},{14,30},{16,0},... | collective-permute-start | bytes 196616 | tf_op jit(solution)/shard_map/ppermute | solution.py:21
  62.5 11.5 %collective-permute-start.14 = (f32[16,1024]{1,0:T(8,128)S(1)}, f32[16,1024]{1,0:T(8,128)S(1)}, u32[]{:S(2)}, u32[]{:S(2)}) collective-permute-start(f32[16,1024]{1,0:T(8,128)S(1)} %get-tuple-element.57), channel_id=1, source_target_pairs={{0,8},{2,10},{4,12},{6,14},{8,0},{10,2},{12,4},{14,6},{16,24},{18,... | collective-permute-start | bytes 196616 | tf_op jit(solution)/shard_map/ppermute | solution.py:21
  62.7 13.6 %collective-permute-start.15 = (f32[16,1024]{1,0:T(8,128)S(1)}, f32[16,1024]{1,0:T(8,128)S(1)}, u32[]{:S(2)}, u32[]{:S(2)}) collective-permute-start(f32[16,1024]{1,0:T(8,128)S(1)} %get-tuple-element.58), channel_id=1, source_target_pairs={{0,16},{2,18},{4,20},{6,22},{8,24},{10,26},{12,28},{14,30},{16,0},... | collective-permute-start | bytes 196616 | tf_op jit(solution)/shard_map/ppermute | solution.py:21
  65.8 10.5 %collective-permute-start.16 = (f32[16,1024]{1,0:T(8,128)S(1)}, f32[16,1024]{1,0:T(8,128)S(1)}, u32[]{:S(2)}, u32[]{:S(2)}) collective-permute-start(f32[16,1024]{1,0:T(8,128)S(1)} %get-tuple-element.59), channel_id=1, source_target_pairs={{0,24},{2,26},{4,28},{6,30},{8,16},{10,18},{12,20},{14,22},{16,8},... | collective-permute-start | bytes 196616 | tf_op jit(solution)/shard_map/ppermute | solution.py:21
  69.0 10.0 %collective-permute-start.31 = (f32[16,1024]{1,0:T(8,128)S(1)}, f32[16,1024]{1,0:T(8,128)S(1)}, u32[]{:S(2)}, u32[]{:S(2)}) collective-permute-start(f32[16,1024]{1,0:T(8,128)S(1)} %get-tuple-element.40), channel_id=1, source_target_pairs={{0,8},{2,10},{4,12},{6,14},{8,0},{10,2},{12,4},{14,6},{16,24},{18,... | collective-permute-start | bytes 196616 | tf_op jit(solution)/shard_map/ppermute | solution.py:21
  81.5 9.2 %collective-permute-start.34 = (f32[4,16,1024]{2,1,0:T(8,128)S(1)}, f32[4,16,1024]{2,1,0:T(8,128)S(1)}, u32[]{:S(2)}, u32[]{:S(2)}) collective-permute-start(f32[4,16,1024]{2,1,0:T(8,128)S(1)} %pad_maximum_fusion.2.refs_0_), channel_id=1, source_target_pairs={{0,2},{2,0},{4,6},{6,4},{8,10},{10,8},{12,14},{14,12},{16,18},{18,... | collective-permute-start | bytes 786440 | tf_op jit(solution)/shard_map/ppermute | solution.py:21
  83.0 12.9 %collective-permute-start.35 = (f32[4,16,1024]{2,1,0:T(8,128)S(1)}, f32[4,16,1024]{2,1,0:T(8,128)S(1)}, u32[]{:S(2)}, u32[]{:S(2)}) collective-permute-start(f32[4,16,1024]{2,1,0:T(8,128)S(1)} %pad_maximum_fusion.2.refs_0_), channel_id=1, source_target_pairs={{0,4},{2,6},{4,0},{6,2},{8,12},{10,14},{12,8},{14,10},{16,20},{18,... | collective-permute-start | bytes 786440 | tf_op jit(solution)/shard_map/ppermute | solution.py:21
  83.1 12.8 %collective-permute-start.36 = (f32[4,16,1024]{2,1,0:T(8,128)S(1)}, f32[4,16,1024]{2,1,0:T(8,128)S(1)}, u32[]{:S(2)}, u32[]{:S(2)}) collective-permute-start(f32[4,16,1024]{2,1,0:T(8,128)S(1)} %pad_maximum_fusion.2.refs_0_), channel_id=1, source_target_pairs={{0,6},{2,4},{4,2},{6,0},{8,14},{10,12},{12,10},{14,8},{16,22},{18,... | collective-permute-start | bytes 786440 | tf_op jit(solution)/shard_map/ppermute | solution.py:21
  85.5 14.2 %collective-permute-start.20 = (f32[4,16,1024]{2,1,0:T(8,128)S(1)}, f32[4,16,1024]{2,1,0:T(8,128)S(1)}, u32[]{:S(2)}, u32[]{:S(2)}) collective-permute-start(f32[4,16,1024]{2,1,0:T(8,128)S(1)} %pad_maximum_fusion.1.refs_0_), channel_id=1, source_target_pairs={{0,2},{2,0},{4,6},{6,4},{8,10},{10,8},{12,14},{14,12},{16,18},{18,... | collective-permute-start | bytes 786440 | tf_op jit(solution)/shard_map/ppermute | solution.py:21
  86.7 14.9 %collective-permute-start.21 = (f32[4,16,1024]{2,1,0:T(8,128)S(1)}, f32[4,16,1024]{2,1,0:T(8,128)S(1)}, u32[]{:S(2)}, u32[]{:S(2)}) collective-permute-start(f32[4,16,1024]{2,1,0:T(8,128)S(1)} %pad_maximum_fusion.1.refs_0_), channel_id=1, source_target_pairs={{0,4},{2,6},{4,0},{6,2},{8,12},{10,14},{12,8},{14,10},{16,20},{18,... | collective-permute-start | bytes 786440 | tf_op jit(solution)/shard_map/ppermute | solution.py:21
  90.8 10.8 %collective-permute-start.22 = (f32[4,16,1024]{2,1,0:T(8,128)S(1)}, f32[4,16,1024]{2,1,0:T(8,128)}, u32[]{:S(2)}, u32[]{:S(2)}) collective-permute-start(f32[4,16,1024]{2,1,0:T(8,128)S(1)} %pad_maximum_fusion.1.refs_0_), channel_id=1, source_target_pairs={{0,6},{2,4},{4,2},{6,0},{8,14},{10,12},{12,10},{14,8},{16,22},{18,... | collective-permute-start | bytes 786440 | tf_op jit(solution)/shard_map/ppermute | solution.py:21
  108.0 8.9 %collective-permute-start.52 = (bf16[128,1024]{1,0:T(8,128)(2,1)}, bf16[128,1024]{1,0:T(8,128)(2,1)S(1)}, u32[]{:S(2)}, u32[]{:S(2)}) collective-permute-start(bf16[128,1024]{1,0:T(8,128)(2,1)} %get-tuple-element.30.refs_0_), channel_id=1, source_target_pairs={{0,2},{2,0},{4,6},{6,4},{8,10},{10,8},{12,14},{14,12},{16,18},{18,... | collective-permute-start | bytes 786440 | tf_op jit(solution)/shard_map/ppermute | solution.py:21
  109.5 13.6 %collective-permute-start.60 = (bf16[128,1024]{1,0:T(8,128)(2,1)}, bf16[128,1024]{1,0:T(8,128)(2,1)S(1)}, u32[]{:S(2)}, u32[]{:S(2)}) collective-permute-start(bf16[128,1024]{1,0:T(8,128)(2,1)} %get-tuple-element.30.refs_0_), channel_id=1, source_target_pairs={{0,8},{2,10},{4,12},{6,14},{8,0},{10,2},{12,4},{14,6},{16,24},{18,... | collective-permute-start | bytes 786440 | tf_op jit(solution)/shard_map/ppermute | solution.py:21
  111.1 12.9 %collective-permute-start.66 = (bf16[128,1024]{1,0:T(8,128)(2,1)}, bf16[128,1024]{1,0:T(8,128)(2,1)S(1)}, u32[]{:S(2)}, u32[]{:S(2)}) collective-permute-start(bf16[128,1024]{1,0:T(8,128)(2,1)} %get-tuple-element.30.refs_0_), channel_id=1, source_target_pairs={{0,4},{2,6},{4,0},{6,2},{8,12},{10,14},{12,8},{14,10},{16,20},{18,... | collective-permute-start | bytes 786440 | tf_op jit(solution)/shard_map/ppermute | solution.py:21
  111.5 15.5 %collective-permute-start.38 = (bf16[128,1024]{1,0:T(8,128)(2,1)}, bf16[128,1024]{1,0:T(8,128)(2,1)S(1)}, u32[]{:S(2)}, u32[]{:S(2)}) collective-permute-start(bf16[128,1024]{1,0:T(8,128)(2,1)} %get-tuple-element.30.refs_0_), channel_id=1, source_target_pairs={{0,16},{2,18},{4,20},{6,22},{8,24},{10,26},{12,28},{14,30},{16,0},... | collective-permute-start | bytes 786440 | tf_op jit(solution)/shard_map/ppermute | solution.py:21
  115.7 11.4 %collective-permute-start.42 = (bf16[128,1024]{1,0:T(8,128)(2,1)}, bf16[128,1024]{1,0:T(8,128)(2,1)S(1)}, u32[]{:S(2)}, u32[]{:S(2)}) collective-permute-start(bf16[128,1024]{1,0:T(8,128)(2,1)} %get-tuple-element.31.refs_4_), channel_id=1, source_target_pairs={{0,2},{2,0},{4,6},{6,4},{8,10},{10,8},{12,14},{14,12},{16,18},{18,... | collective-permute-start | bytes 786440 | tf_op jit(solution)/shard_map/ppermute | solution.py:21
  116.9 17.4 %collective-permute-start.63 = (bf16[128,1024]{1,0:T(8,128)(2,1)}, bf16[128,1024]{1,0:T(8,128)(2,1)S(1)}, u32[]{:S(2)}, u32[]{:S(2)}) collective-permute-start(bf16[128,1024]{1,0:T(8,128)(2,1)} %get-tuple-element.31.refs_4_), channel_id=1, source_target_pairs={{0,8},{2,10},{4,12},{6,14},{8,0},{10,2},{12,4},{14,6},{16,24},{18,... | collective-permute-start | bytes 786440 | tf_op jit(solution)/shard_map/ppermute | solution.py:21
  123.1 14.5 %collective-permute-start.45 = (bf16[128,1024]{1,0:T(8,128)(2,1)}, bf16[128,1024]{1,0:T(8,128)(2,1)S(1)}, u32[]{:S(2)}, u32[]{:S(2)}) collective-permute-start(bf16[128,1024]{1,0:T(8,128)(2,1)} %get-tuple-element.31.refs_4_), channel_id=1, source_target_pairs={{0,16},{2,18},{4,20},{6,22},{8,24},{10,26},{12,28},{14,30},{16,0},... | collective-permute-start | bytes 786440 | tf_op jit(solution)/shard_map/ppermute | solution.py:21
  124.0 13.6 %collective-permute-start.67 = (bf16[128,1024]{1,0:T(8,128)(2,1)}, bf16[128,1024]{1,0:T(8,128)(2,1)S(1)}, u32[]{:S(2)}, u32[]{:S(2)}) collective-permute-start(bf16[128,1024]{1,0:T(8,128)(2,1)} %get-tuple-element.31.refs_4_), channel_id=1, source_target_pairs={{0,4},{2,6},{4,0},{6,2},{8,12},{10,14},{12,8},{14,10},{16,20},{18,... | collective-permute-start | bytes 786440 | tf_op jit(solution)/shard_map/ppermute | solution.py:21
  127.1 14.3 %collective-permute-start.56 = (bf16[128,1024]{1,0:T(8,128)(2,1)S(1)}, bf16[128,1024]{1,0:T(8,128)(2,1)S(1)}, u32[]{:S(2)}, u32[]{:S(2)}) collective-permute-start(bf16[128,1024]{1,0:T(8,128)(2,1)S(1)} %collective-permute-done.38.refs_2_), channel_id=1, source_target_pairs={{0,8},{2,10},{4,12},{6,14},{8,0},{10,2},{12,4},{14,6},{16,24},{18,... | collective-permute-start | bytes 786440 | tf_op jit(solution)/shard_map/ppermute | solution.py:21
  127.1 14.6 %collective-permute-start.61 = (bf16[128,1024]{1,0:T(8,128)(2,1)S(1)}, bf16[128,1024]{1,0:T(8,128)(2,1)S(1)}, u32[]{:S(2)}, u32[]{:S(2)}) collective-permute-start(bf16[128,1024]{1,0:T(8,128)(2,1)S(1)} %collective-permute-done.60.refs_3_), channel_id=1, source_target_pairs={{0,2},{2,0},{4,6},{6,4},{8,10},{10,8},{12,14},{14,12},{16,18},{18,... | collective-permute-start | bytes 786440 | tf_op jit(solution)/shard_map/ppermute | solution.py:21
  134.3 9.2 %collective-permute-start.62 = (bf16[128,1024]{1,0:T(8,128)(2,1)S(1)}, bf16[128,1024]{1,0:T(8,128)(2,1)S(1)}, u32[]{:S(2)}, u32[]{:S(2)}) collective-permute-start(bf16[128,1024]{1,0:T(8,128)(2,1)S(1)} %collective-permute-done.60.refs_3_), channel_id=1, source_target_pairs={{0,4},{2,6},{4,0},{6,2},{8,12},{10,14},{12,8},{14,10},{16,20},{18,... | collective-permute-start | bytes 786440 | tf_op jit(solution)/shard_map/ppermute | solution.py:21
  137.6 9.2 %collective-permute-start.64 = (bf16[128,1024]{1,0:T(8,128)(2,1)S(1)}, bf16[128,1024]{1,0:T(8,128)(2,1)S(1)}, u32[]{:S(2)}, u32[]{:S(2)}) collective-permute-start(bf16[128,1024]{1,0:T(8,128)(2,1)S(1)} %collective-permute-done.63.refs_7_), channel_id=1, source_target_pairs={{0,2},{2,0},{4,6},{6,4},{8,10},{10,8},{12,14},{14,12},{16,18},{18,... | collective-permute-start | bytes 786440 | tf_op jit(solution)/shard_map/ppermute | solution.py:21
  141.4 9.2 %collective-permute-start.65 = (bf16[128,1024]{1,0:T(8,128)(2,1)S(1)}, bf16[128,1024]{1,0:T(8,128)(2,1)S(1)}, u32[]{:S(2)}, u32[]{:S(2)}) collective-permute-start(bf16[128,1024]{1,0:T(8,128)(2,1)S(1)} %collective-permute-done.63.refs_7_), channel_id=1, source_target_pairs={{0,4},{2,6},{4,0},{6,2},{8,12},{10,14},{12,8},{14,10},{16,20},{18,... | collective-permute-start | bytes 786440 | tf_op jit(solution)/shard_map/ppermute | solution.py:21
  141.7 14.5 %collective-permute-start.39 = (bf16[128,1024]{1,0:T(8,128)(2,1)}, bf16[128,1024]{1,0:T(8,128)(2,1)S(1)}, u32[]{:S(2)}, u32[]{:S(2)}) collective-permute-start(bf16[128,1024]{1,0:T(8,128)(2,1)} %copy-done.18), channel_id=1, source_target_pairs={{0,4},{2,6},{4,0},{6,2},{8,12},{10,14},{12,8},{14,10},{16,20},{18,... | collective-permute-start | bytes 786440 | tf_op jit(solution)/shard_map/ppermute | solution.py:21
  143.5 18.3 %collective-permute-start.53 = (bf16[128,1024]{1,0:T(8,128)(2,1)S(1)}, bf16[128,1024]{1,0:T(8,128)(2,1)S(1)}, u32[]{:S(2)}, u32[]{:S(2)}) collective-permute-start(bf16[128,1024]{1,0:T(8,128)(2,1)S(1)} %collective-permute-done.52.refs_1_), channel_id=1, source_target_pairs={{0,4},{2,6},{4,0},{6,2},{8,12},{10,14},{12,8},{14,10},{16,20},{18,... | collective-permute-start | bytes 786440 | tf_op jit(solution)/shard_map/ppermute | solution.py:21
  146.3 15.9 %collective-permute-start.55 = (bf16[128,1024]{1,0:T(8,128)(2,1)}, bf16[128,1024]{1,0:T(8,128)(2,1)S(1)}, u32[]{:S(2)}, u32[]{:S(2)}) collective-permute-start(bf16[128,1024]{1,0:T(8,128)(2,1)} %copy-done.18), channel_id=1, source_target_pairs={{0,2},{2,0},{4,6},{6,4},{8,10},{10,8},{12,14},{14,12},{16,18},{18,... | collective-permute-start | bytes 786440 | tf_op jit(solution)/shard_map/ppermute | solution.py:21
  146.8 20.7 %collective-permute-start.43 = (bf16[128,1024]{1,0:T(8,128)(2,1)S(1)}, bf16[128,1024]{1,0:T(8,128)(2,1)}, u32[]{:S(2)}, u32[]{:S(2)}) collective-permute-start(bf16[128,1024]{1,0:T(8,128)(2,1)S(1)} %collective-permute-done.42.refs_5_), channel_id=1, source_target_pairs={{0,4},{2,6},{4,0},{6,2},{8,12},{10,14},{12,8},{14,10},{16,20},{18,... | collective-permute-start | bytes 786440 | tf_op jit(solution)/shard_map/ppermute | solution.py:21
  150.5 20.1 %collective-permute-start.46 = (bf16[128,1024]{1,0:T(8,128)(2,1)S(1)}, bf16[128,1024]{1,0:T(8,128)(2,1)S(1)}, u32[]{:S(2)}, u32[]{:S(2)}) collective-permute-start(bf16[128,1024]{1,0:T(8,128)(2,1)S(1)} %collective-permute-done.45.refs_6_), channel_id=1, source_target_pairs={{0,4},{2,6},{4,0},{6,2},{8,12},{10,14},{12,8},{14,10},{16,20},{18,... | collective-permute-start | bytes 786440 | tf_op jit(solution)/shard_map/ppermute | solution.py:21
  156.2 15.0 %collective-permute-start.59 = (bf16[128,1024]{1,0:T(8,128)(2,1)S(1)}, bf16[128,1024]{1,0:T(8,128)(2,1)S(1)}, u32[]{:S(2)}, u32[]{:S(2)}) collective-permute-start(bf16[128,1024]{1,0:T(8,128)(2,1)S(1)} %collective-permute-done.45.refs_6_), channel_id=1, source_target_pairs={{0,2},{2,0},{4,6},{6,4},{8,10},{10,8},{12,14},{14,12},{16,18},{18,... | collective-permute-start | bytes 786440 | tf_op jit(solution)/shard_map/ppermute | solution.py:21
  161.8 10.2 %collective-permute-start.40 = (bf16[128,1024]{1,0:T(8,128)(2,1)S(1)}, bf16[128,1024]{1,0:T(8,128)(2,1)}, u32[]{:S(2)}, u32[]{:S(2)}) collective-permute-start(bf16[128,1024]{1,0:T(8,128)(2,1)S(1)} %collective-permute-done.39.refs_3_), channel_id=1, source_target_pairs={{0,2},{2,0},{4,6},{6,4},{8,10},{10,8},{12,14},{14,12},{16,18},{18,... | collective-permute-start | bytes 786440 | tf_op jit(solution)/shard_map/ppermute | solution.py:21
  162.3 10.9 %collective-permute-start.54 = (bf16[128,1024]{1,0:T(8,128)(2,1)S(1)}, bf16[128,1024]{1,0:T(8,128)(2,1)S(1)}, u32[]{:S(2)}, u32[]{:S(2)}) collective-permute-start(bf16[128,1024]{1,0:T(8,128)(2,1)S(1)} %collective-permute-done.53.refs_0_), channel_id=1, source_target_pairs={{0,8},{2,10},{4,12},{6,14},{8,0},{10,2},{12,4},{14,6},{16,24},{18,... | collective-permute-start | bytes 786440 | tf_op jit(solution)/shard_map/ppermute | solution.py:21
  170.7 8.9 %collective-permute-start.58 = (bf16[128,1024]{1,0:T(8,128)(2,1)S(1)}, bf16[128,1024]{1,0:T(8,128)(2,1)S(1)}, u32[]{:S(2)}, u32[]{:S(2)}) collective-permute-start(bf16[128,1024]{1,0:T(8,128)(2,1)S(1)} %collective-permute-done.56.refs_3_), channel_id=1, source_target_pairs={{0,4},{2,6},{4,0},{6,2},{8,12},{10,14},{12,8},{14,10},{16,20},{18,... | collective-permute-start | bytes 786440 | tf_op jit(solution)/shard_map/ppermute | solution.py:21
  171.1 10.9 %collective-permute-start.47 = (bf16[128,1024]{1,0:T(8,128)(2,1)S(1)}, bf16[128,1024]{1,0:T(8,128)(2,1)}, u32[]{:S(2)}, u32[]{:S(2)}) collective-permute-start(bf16[128,1024]{1,0:T(8,128)(2,1)S(1)} %collective-permute-done.46.refs_9_), channel_id=1, source_target_pairs={{0,2},{2,0},{4,6},{6,4},{8,10},{10,8},{12,14},{14,12},{16,18},{18,... | collective-permute-start | bytes 786440 | tf_op jit(solution)/shard_map/ppermute | solution.py:21
  171.9 21.1 %collective-permute-start.49 = (bf16[128,1024]{1,0:T(8,128)(2,1)}, bf16[128,1024]{1,0:T(8,128)(2,1)}, u32[]{:S(2)}, u32[]{:S(2)}) collective-permute-start(bf16[128,1024]{1,0:T(8,128)(2,1)} %collective-permute-done.48.refs_7_), channel_id=1, source_target_pairs={{0,2},{2,0},{4,6},{6,4},{8,10},{10,8},{12,14},{14,12},{16,18},{18,... | collective-permute-start | bytes 786440 | tf_op jit(solution)/shard_map/ppermute | solution.py:21
  173.2 19.8 %collective-permute-start.50 = (bf16[128,1024]{1,0:T(8,128)(2,1)}, bf16[128,1024]{1,0:T(8,128)(2,1)}, u32[]{:S(2)}, u32[]{:S(2)}) collective-permute-start(bf16[128,1024]{1,0:T(8,128)(2,1)} %collective-permute-done.48.refs_7_), channel_id=1, source_target_pairs={{0,4},{2,6},{4,0},{6,2},{8,12},{10,14},{12,8},{14,10},{16,20},{18,... | collective-permute-start | bytes 786440 | tf_op jit(solution)/shard_map/ppermute | solution.py:21
  176.3 16.7 %collective-permute-start.44 = (bf16[128,1024]{1,0:T(8,128)(2,1)}, bf16[128,1024]{1,0:T(8,128)(2,1)}, u32[]{:S(2)}, u32[]{:S(2)}) collective-permute-start(bf16[128,1024]{1,0:T(8,128)(2,1)} %collective-permute-done.43.refs_7_), channel_id=1, source_target_pairs={{0,8},{2,10},{4,12},{6,14},{8,0},{10,2},{12,4},{14,6},{16,24},{18,... | collective-permute-start | bytes 786440 | tf_op jit(solution)/shard_map/ppermute | solution.py:21
  179.6 13.5 %collective-permute-start.41 = (bf16[128,1024]{1,0:T(8,128)(2,1)}, bf16[128,1024]{1,0:T(8,128)(2,1)}, u32[]{:S(2)}, u32[]{:S(2)}) collective-permute-start(bf16[128,1024]{1,0:T(8,128)(2,1)} %collective-permute-done.40.refs_4_), channel_id=1, source_target_pairs={{0,8},{2,10},{4,12},{6,14},{8,0},{10,2},{12,4},{14,6},{16,24},{18,... | collective-permute-start | bytes 786440 | tf_op jit(solution)/shard_map/ppermute | solution.py:21
  182.0 11.0 %collective-permute-start.51 = (bf16[128,1024]{1,0:T(8,128)(2,1)}, bf16[128,1024]{1,0:T(8,128)(2,1)}, u32[]{:S(2)}, u32[]{:S(2)}) collective-permute-start(bf16[128,1024]{1,0:T(8,128)(2,1)} %collective-permute-done.47.refs_2_), channel_id=1, source_target_pairs={{0,8},{2,10},{4,12},{6,14},{8,0},{10,2},{12,4},{14,6},{16,24},{18,... | collective-permute-start | bytes 786440 | tf_op jit(solution)/shard_map/ppermute | solution.py:21
  (56 other events, 832.8 us)

commit v3 on v2

--- a/solution.py
+++ b/solution.py
@@ -126,6 +126,7 @@
             bytes_accessed=8 * rank * width,
             transcendentals=0,
         ),
+        compiler_params=pltpu.CompilerParams(vmem_limit_bytes=16 * 2**20),
         name="directions",
     )(me.astype(jnp.int32).reshape(1), gram, factor, *stacks)
 
@@ -146,6 +147,7 @@
         cost_estimate=pl.CostEstimate(
             flops=4 * moved.size, bytes_accessed=14 * moved.size, transcendentals=0
         ),
+        compiler_params=pltpu.CompilerParams(vmem_limit_bytes=16 * 2**20),
         name="finish",
     )(moved, square, others, master)
 
@@ -176,7 +178,7 @@
     early = [0, 1, 2, 4]
     middle = [4 * k + c for k in range(1, lines - 2) for c in (0, 1, 2)]
     middle += [4 * k for k in range(max(lines - 2, 1), lines)]
-    later = [3] + [4 * k + c for k in range(max(lines - 2, 0), lines - 1) for c in (1, 2)]
+    later = [3] + [4 * k + c for k in range(max(lines - 2, 0), lines - 1) for c in (1, 2, 3)]
     groups = [(early, early), (middle, middle), (everything[:-1], later), (everything, everything)]
     rows, width = gate[0].shape
     shape = jax.ShapeDtypeStruct((4 * lines * rows, width), bf16)
@@ -213,7 +215,8 @@
             cost_estimate=pl.CostEstimate(
                 flops=0, bytes_accessed=4 * n * rows * width, transcendentals=0
             ),
-            name="place_copies",
+            compiler_params=pltpu.CompilerParams(vmem_limit_bytes=16 * 2**20),
+        name="place_copies",
         )
         blocks = [(gate, other)[i][mask] for i, mask in todo]
         outs = call(me.astype(jnp.int32).reshape(1), *blocks, *outs)

time: 196 us -> 188 us (0.959)
  Pallas kernels: 21.7 us -> 9.31 us
  waiting for transfers between devices: 80.4 us -> 87.1 us
  local copies, waits for them, and re-layouts: 10.8 us -> 8.11 us
    ppermute x68, waiting for transfers between devices: 80.4 us -> 87.1 us  [swap(): return lax.ppermute(a, axis, [(i, i ^ mask) for i in range(size)])]
    pallas_call x4, Pallas kernels: 11.5 us -> 5.51 us  [place_copies(): outs = call(me.astype(jnp.int32).reshape(1), *blocks, *outs)]
    pallas_call x2, Pallas kernels: 5.76 us -> 1.97 us  [directions(): pl.pallas_call(kernel, out_shape=(jax.ShapeDtypeStruct((factor.shape[0],...]
    unnamed x73 -> x21, local copies, waits for them, and re-layouts: 8.4 us -> 5.66 us
    pallas_call x2, Pallas kernels: 4.4 us -> 1.83 us  [finish(): pl.pallas_call(kernel, out_shape=(jax.ShapeDtypeStruct(moved.shape, f32),...]
  transfers between devices with their start and end apart: 68 -> 68, of which waited for: 27 -> 31; matrix products, arithmetic and copies ran while one was open for 8% -> 8% of each run, Pallas kernels for 10% -> 4%
where the time goes in v3:
time: 188 us; the launch traced here: 187 us
  waiting for transfers between devices  87.1 us (46%)
  starting transfers between devices  70.8 us (38%)
  Pallas kernels  9.31 us (5%)
  local copies, waits for them, and re-layouts  8.11 us (4%)
  matrix products  7.95 us (4%)
  other arithmetic  2.73 us (1%)
    ppermute x68, waiting for transfers between devices, swap(): return lax.ppermute(a, axis, [(i, i ^ mask) for i in range(size)])  87.1 us
    ppermute x68, starting transfers between devices, swap(): return lax.ppermute(a, axis, [(i, i ^ mask) for i in range(size)])  70.8 us
    dot_general x20, matrix products, dot(): return lax.dot_general(a, b, dims, preferred_element_type=f32)  7.95 us
    unnamed x21, local copies, waits for them, and re-layouts  5.66 us
    pallas_call x4, Pallas kernels, place_copies(): outs = call(me.astype(jnp.int32).reshape(1), *blocks, *outs)  5.51 us
  transfers between devices with their start and end apart: 68, of which 31 were waited for; matrix products, arithmetic and copies ran while one was open for 8% of the time, Pallas kernels for 4%

profile of v3, /device:TPU:0, one launch (start us, length us, event | category | flops | bytes accessed | tf_op | source)
XLA Modules:
  0.0 187.4 jit_solution(15729684040736475515)
XLA Ops:
  1.6 5.1 %collective-permute-start = (bf16[128,256]{1,0:T(8,128)(2,1)S(1)}, bf16[128,256]{1,0:T(8,128)(2,1)S(1)}, u32[]{:S(2)}, u32[]{:S(2)}) collective-permute-start(bf16[128,256]{1,0:T(8,128)(2,1)S(1)} %broadcast_select_fusion.24), channel_id=1, source_target_pairs={{0,24},{2,26},{4,28},{6,30},{8,16},{10,18},{12,20},{14,22},{16,8},... | collective-permute-start | bytes 196616 | tf_op jit(solution)/shard_map/ppermute | solution.py:21
  7.4 1.8 collective-permute-done
  9.3 3.1 %collective-permute-done.1 = bf16[128,256]{1,0:T(8,128)(2,1)S(1)} collective-permute-done((bf16[128,256]{1,0:T(8,128)(2,1)S(1)}, bf16[128,256]{1,0:T(8,128)(2,1)S(1)}, u32[]{:S(2)}, u32[]{:S(2)}) %collective-permute-start.1) | collective-permute-done | bytes 65568 | tf_op jit(solution)/shard_map/ppermute | solution.py:21
  12.4 1.6 collective-permute-start.4
  14.0 4.6 %copy.29 = bf16[768,2048]{0,1:T(8,128)(2,1)} copy(bf16[768,2048]{1,0:T(8,128)(2,1)} %param.11) | data formatting | bytes 6291456 | tf_op args[0]
  18.6 2.1 %constant_dynamic-slice_fusion.1 = (bf16[768,4,1,128]{0,3,2,1:T(8,128)(2,1)S(1)}, bf16[768,4,1,128]{0,3,2,1:T(8,128)(2,1)S(1)}, bf16[768,4,1,128]{0,3,2,1:T(8,128)(2,1)S(1)}, bf16[768,4,1,128]{0,3,2,1:T(8,128)(2,1)S(1)}) fusion(bf16[768,4,4,128]{0,3,2,1:T(8,128)(2,1)} %bitcast.104, s32[]{:T(128)S(6)} %select_n.156, s32[]{:T(128)S(6)} %select_n.157, ...), kind=kLoop, calls=%fused_computation.115 | loop fusion | bytes 6291472 | tf_op jit(solution)/shard_map/jit(dynamic_index_in_dim)/dynamic_slice | solution.py:45
  20.8 1.6 collective-permute-start.8
  23.4 7.1 %collective-permute-done.8 = bf16[512,256]{1,0:T(8,128)(2,1)S(1)} collective-permute-done((bf16[512,256]{1,0:T(8,128)(2,1)S(1)}, bf16[512,256]{1,0:T(8,128)(2,1)S(1)}, u32[]{:S(2)}, u32[]{:S(2)}) %collective-permute-start.8) | collective-permute-done | bytes 262176 | tf_op jit(solution)/shard_map/ppermute | solution.py:21
  31.0 5.1 %collective-permute-done.6 = bf16[512,256]{1,0:T(8,128)(2,1)S(1)} collective-permute-done((bf16[512,256]{1,0:T(8,128)(2,1)S(1)}, bf16[512,256]{1,0:T(8,128)(2,1)S(1)}, u32[]{:S(2)}, u32[]{:S(2)}) %collective-permute-start.6) | collective-permute-done | bytes 262176 | tf_op jit(solution)/shard_map/ppermute | solution.py:21
  45.8 1.5 collective-permute-start.10
  49.3 1.5 collective-permute-start.25
  50.8 3.6 %collective-permute-done.12 = f32[4,2,16,512]{3,2,1,0:T(8,128)S(1)} collective-permute-done((f32[4,2,16,512]{3,2,1,0:T(8,128)S(1)}, f32[4,2,16,512]{3,2,1,0:T(8,128)S(1)}, u32[]{:S(2)}, u32[]{:S(2)}) %collective-permute-start.12) | collective-permute-done | bytes 262176 | tf_op jit(solution)/shard_map/ppermute | solution.py:21
  59.1 2.2 %collective-permute-start.29 = (f32[16,1024]{1,0:T(8,128)S(1)}, f32[16,1024]{1,0:T(8,128)S(1)}, u32[]{:S(2)}, u32[]{:S(2)}) collective-permute-start(f32[16,1024]{1,0:T(8,128)S(1)} %get-tuple-element.55), channel_id=1, source_target_pairs={{0,16},{2,18},{4,20},{6,22},{8,24},{10,26},{12,28},{14,30},{16,0},... | collective-permute-start | bytes 196616 | tf_op jit(solution)/shard_map/ppermute | solution.py:21
  62.7 3.1 %collective-permute-start.15 = (f32[16,1024]{1,0:T(8,128)S(1)}, f32[16,1024]{1,0:T(8,128)S(1)}, u32[]{:S(2)}, u32[]{:S(2)}) collective-permute-start(f32[16,1024]{1,0:T(8,128)S(1)} %get-tuple-element.58), channel_id=1, source_target_pairs={{0,16},{2,18},{4,20},{6,22},{8,24},{10,26},{12,28},{14,30},{16,0},... | collective-permute-start | bytes 196616 | tf_op jit(solution)/shard_map/ppermute | solution.py:21
  69.0 4.9 %collective-permute-start.31 = (f32[16,1024]{1,0:T(8,128)S(1)}, f32[16,1024]{1,0:T(8,128)S(1)}, u32[]{:S(2)}, u32[]{:S(2)}) collective-permute-start(f32[16,1024]{1,0:T(8,128)S(1)} %get-tuple-element.40), channel_id=1, source_target_pairs={{0,8},{2,10},{4,12},{6,14},{8,0},{10,2},{12,4},{14,6},{16,24},{18,... | collective-permute-start | bytes 196616 | tf_op jit(solution)/shard_map/ppermute | solution.py:21
  73.9 2.4 %collective-permute-start.33 = (f32[16,1024]{1,0:T(8,128)S(1)}, f32[16,1024]{1,0:T(8,128)S(1)}, u32[]{:S(2)}, u32[]{:S(2)}) collective-permute-start(f32[16,1024]{1,0:T(8,128)S(1)} %get-tuple-element.40), channel_id=1, source_target_pairs={{0,24},{2,26},{4,28},{6,30},{8,16},{10,18},{12,20},{14,22},{16,8},... | collective-permute-start | bytes 196616 | tf_op jit(solution)/shard_map/ppermute | solution.py:21
  79.0 2.4 %collective-permute-start.19 = (f32[16,1024]{1,0:T(8,128)S(1)}, f32[16,1024]{1,0:T(8,128)S(1)}, u32[]{:S(2)}, u32[]{:S(2)}) collective-permute-start(f32[16,1024]{1,0:T(8,128)S(1)} %get-tuple-element.43), channel_id=1, source_target_pairs={{0,24},{2,26},{4,28},{6,30},{8,16},{10,18},{12,20},{14,22},{16,8},... | collective-permute-start | bytes 196616 | tf_op jit(solution)/shard_map/ppermute | solution.py:21
  82.1 3.3 %collective-permute-start.36 = (f32[4,16,1024]{2,1,0:T(8,128)S(1)}, f32[4,16,1024]{2,1,0:T(8,128)S(1)}, u32[]{:S(2)}, u32[]{:S(2)}) collective-permute-start(f32[4,16,1024]{2,1,0:T(8,128)S(1)} %pad_maximum_fusion.2.refs_0_), channel_id=1, source_target_pairs={{0,6},{2,4},{4,2},{6,0},{8,14},{10,12},{12,10},{14,8},{16,22},{18,... | collective-permute-start | bytes 786440 | tf_op jit(solution)/shard_map/ppermute | solution.py:21
  86.1 4.7 %collective-permute-done.34.refs_1_ = f32[4,16,1024]{2,1,0:T(8,128)S(1)} collective-permute-done((f32[4,16,1024]{2,1,0:T(8,128)S(1)}, f32[4,16,1024]{2,1,0:T(8,128)S(1)}, u32[]{:S(2)}, u32[]{:S(2)}) %collective-permute-start.34) | collective-permute-done | bytes 262176 | tf_op jit(solution)/shard_map/ppermute | solution.py:21
  91.0 4.9 %collective-permute-done.35.refs_2_ = f32[4,16,1024]{2,1,0:T(8,128)S(1)} collective-permute-done((f32[4,16,1024]{2,1,0:T(8,128)S(1)}, f32[4,16,1024]{2,1,0:T(8,128)S(1)}, u32[]{:S(2)}, u32[]{:S(2)}) %collective-permute-start.35) | collective-permute-done | bytes 262176 | tf_op jit(solution)/shard_map/ppermute | solution.py:21
  98.2 3.3 %collective-permute-done.21.refs_2_ = f32[4,16,1024]{2,1,0:T(8,128)S(1)} collective-permute-done((f32[4,16,1024]{2,1,0:T(8,128)S(1)}, f32[4,16,1024]{2,1,0:T(8,128)S(1)}, u32[]{:S(2)}, u32[]{:S(2)}) %collective-permute-start.21) | collective-permute-done | bytes 262176 | tf_op jit(solution)/shard_map/ppermute | solution.py:21
  103.5 1.5 collective-permute-start.52
  105.0 1.6 collective-permute-start.60
  109.9 2.8 %collective-permute-done.52.refs_1_ = bf16[128,1024]{1,0:T(8,128)(2,1)S(1)} collective-permute-done((bf16[128,1024]{1,0:T(8,128)(2,1)S(1)}, bf16[128,1024]{1,0:T(8,128)(2,1)S(1)}, u32[]{:S(2)}, u32[]{:S(2)}) %collective-permute-start.52) | collective-permute-done | bytes 262176 | tf_op jit(solution)/shard_map/ppermute | solution.py:21
  112.7 1.7 collective-permute-start.63
  114.4 4.0 %collective-permute-done.60.refs_3_ = bf16[128,1024]{1,0:T(8,128)(2,1)S(1)} collective-permute-done((bf16[128,1024]{1,0:T(8,128)(2,1)S(1)}, bf16[128,1024]{1,0:T(8,128)(2,1)S(1)}, u32[]{:S(2)}, u32[]{:S(2)}) %collective-permute-start.60) | collective-permute-done | bytes 262176 | tf_op jit(solution)/shard_map/ppermute | solution.py:21
  119.3 3.1 %collective-permute-done.38.refs_2_ = bf16[128,1024]{1,0:T(8,128)(2,1)S(1)} collective-permute-done((bf16[128,1024]{1,0:T(8,128)(2,1)S(1)}, bf16[128,1024]{1,0:T(8,128)(2,1)S(1)}, u32[]{:S(2)}, u32[]{:S(2)}) %collective-permute-start.38) | collective-permute-done | bytes 262176 | tf_op jit(solution)/shard_map/ppermute | solution.py:21
  122.5 1.7 collective-permute-start.61
  124.2 5.4 %collective-permute-done.63.refs_7_ = bf16[128,1024]{1,0:T(8,128)(2,1)S(1)} collective-permute-done((bf16[128,1024]{1,0:T(8,128)(2,1)S(1)}, bf16[128,1024]{1,0:T(8,128)(2,1)S(1)}, u32[]{:S(2)}, u32[]{:S(2)}) %collective-permute-start.63) | collective-permute-done | bytes 262176 | tf_op jit(solution)/shard_map/ppermute | solution.py:21
  129.6 3.2 %collective-permute-done.45.refs_6_ = bf16[128,1024]{1,0:T(8,128)(2,1)S(1)} collective-permute-done((bf16[128,1024]{1,0:T(8,128)(2,1)S(1)}, bf16[128,1024]{1,0:T(8,128)(2,1)S(1)}, u32[]{:S(2)}, u32[]{:S(2)}) %collective-permute-start.45) | collective-permute-done | bytes 262176 | tf_op jit(solution)/shard_map/ppermute | solution.py:21
  134.2 2.5 %collective-permute-done.56.refs_3_ = bf16[128,1024]{1,0:T(8,128)(2,1)S(1)} collective-permute-done((bf16[128,1024]{1,0:T(8,128)(2,1)S(1)}, bf16[128,1024]{1,0:T(8,128)(2,1)S(1)}, u32[]{:S(2)}, u32[]{:S(2)}) %collective-permute-start.56) | collective-permute-done | bytes 262176 | tf_op jit(solution)/shard_map/ppermute | solution.py:21
  137.0 1.7 collective-permute-start.39
  139.0 2.5 %collective-permute-done.46.refs_7_ = bf16[128,1024]{1,0:T(8,128)(2,1)S(1)} collective-permute-done((bf16[128,1024]{1,0:T(8,128)(2,1)S(1)}, bf16[128,1024]{1,0:T(8,128)(2,1)S(1)}, u32[]{:S(2)}, u32[]{:S(2)}) %collective-permute-start.46) | collective-permute-done | bytes 262176 | tf_op jit(solution)/shard_map/ppermute | solution.py:21
  143.2 2.7 %collective-permute-done.65.refs_5_ = bf16[128,1024]{1,0:T(8,128)(2,1)S(1)} collective-permute-done((bf16[128,1024]{1,0:T(8,128)(2,1)S(1)}, bf16[128,1024]{1,0:T(8,128)(2,1)S(1)}, u32[]{:S(2)}, u32[]{:S(2)}) %collective-permute-start.65) | collective-permute-done | bytes 262176 | tf_op jit(solution)/shard_map/ppermute | solution.py:21
  146.1 5.3 %collective-permute-done.39.refs_3_ = bf16[128,1024]{1,0:T(8,128)(2,1)S(1)} collective-permute-done((bf16[128,1024]{1,0:T(8,128)(2,1)S(1)}, bf16[128,1024]{1,0:T(8,128)(2,1)S(1)}, u32[]{:S(2)}, u32[]{:S(2)}) %collective-permute-start.39) | collective-permute-done | bytes 262176 | tf_op jit(solution)/shard_map/ppermute | solution.py:21
  152.0 5.1 %collective-permute-done.53.refs_0_ = bf16[128,1024]{1,0:T(8,128)(2,1)S(1)} collective-permute-done((bf16[128,1024]{1,0:T(8,128)(2,1)S(1)}, bf16[128,1024]{1,0:T(8,128)(2,1)S(1)}, u32[]{:S(2)}, u32[]{:S(2)}) %collective-permute-start.53) | collective-permute-done | bytes 262176 | tf_op jit(solution)/shard_map/ppermute | solution.py:21
  157.6 1.8 collective-permute-start.54
  159.4 3.3 %collective-permute-done.49.refs_9_ = bf16[128,1024]{1,0:T(8,128)(2,1)S(1)} collective-permute-done((bf16[128,1024]{1,0:T(8,128)(2,1)S(1)}, bf16[128,1024]{1,0:T(8,128)(2,1)S(1)}, u32[]{:S(2)}, u32[]{:S(2)}) %collective-permute-start.49) | collective-permute-done | bytes 262176 | tf_op jit(solution)/shard_map/ppermute | solution.py:21
  163.2 2.7 %collective-permute-done.43.refs_7_ = bf16[128,1024]{1,0:T(8,128)(2,1)S(1)} collective-permute-done((bf16[128,1024]{1,0:T(8,128)(2,1)S(1)}, bf16[128,1024]{1,0:T(8,128)(2,1)S(1)}, u32[]{:S(2)}, u32[]{:S(2)}) %collective-permute-start.43) | collective-permute-done | bytes 262176 | tf_op jit(solution)/shard_map/ppermute | solution.py:21
  168.4 1.6 collective-permute-start.48
  170.0 1.5 collective-permute-done.57.refs_5_
  171.5 1.8 collective-permute-start.44
  174.7 1.7 collective-permute-start.41
  177.2 1.8 collective-permute-start.51
  179.0 1.4 place_copies.4
  180.4 1.4 place_copies.5
  181.8 1.7 place_copies.6
  183.5 2.7 %collective-permute-done.51.refs_4_ = bf16[128,1024]{1,0:T(8,128)(2,1)S(1)} collective-permute-done((bf16[128,1024]{1,0:T(8,128)(2,1)S(1)}, bf16[128,1024]{1,0:T(8,128)(2,1)S(1)}, u32[]{:S(2)}, u32[]{:S(2)}) %collective-permute-start.51) | collective-permute-done | bytes 262176 | tf_op jit(solution)/shard_map/ppermute | solution.py:21
  (165 shorter events, 47.6 us)
Async XLA Ops:
  12.4 10.4 %collective-permute-start.4 = (bf16[512,256]{1,0:T(8,128)(2,1)S(1)}, bf16[512,256]{1,0:T(8,128)(2,1)S(1)}, u32[]{:S(2)}, u32[]{:S(2)}) collective-permute-start(bf16[512,256]{1,0:T(8,128)(2,1)S(1)} %pad_maximum_fusion), channel_id=1, source_target_pairs={{0,2},{2,0},{4,6},{6,4},{8,10},{10,8},{12,14},{14,12},{16,18},{18,... | collective-permute-start | bytes 786440 | tf_op jit(solution)/shard_map/ppermute | solution.py:21
  14.0 8.8 %collective-permute-start.3 = (bf16[512,256]{1,0:T(8,128)(2,1)S(1)}, bf16[512,256]{1,0:T(8,128)(2,1)S(1)}, u32[]{:S(2)}, u32[]{:S(2)}) collective-permute-start(bf16[512,256]{1,0:T(8,128)(2,1)S(1)} %pad_maximum_fusion), channel_id=1, source_target_pairs={{0,1},{1,0},{2,3},{3,2},{4,5},{5,4},{6,7},{7,6},{8,9},{9,8},{10,11... | collective-permute-start | bytes 786440 | tf_op jit(solution)/shard_map/ppermute | solution.py:21
  20.8 9.8 %collective-permute-start.8 = (bf16[512,256]{1,0:T(8,128)(2,1)S(1)}, bf16[512,256]{1,0:T(8,128)(2,1)S(1)}, u32[]{:S(2)}, u32[]{:S(2)}) collective-permute-start(bf16[512,256]{1,0:T(8,128)(2,1)S(1)} %pad_maximum_fusion), channel_id=1, source_target_pairs={{0,6},{2,4},{4,2},{6,0},{8,14},{10,12},{12,10},{14,8},{16,22},{18,... | collective-permute-start | bytes 786440 | tf_op jit(solution)/shard_map/ppermute | solution.py:21
  22.3 13.7 %collective-permute-start.6 = (bf16[512,256]{1,0:T(8,128)(2,1)S(1)}, bf16[512,256]{1,0:T(8,128)(2,1)S(1)}, u32[]{:S(2)}, u32[]{:S(2)}) collective-permute-start(bf16[512,256]{1,0:T(8,128)(2,1)S(1)} %pad_maximum_fusion), channel_id=1, source_target_pairs={{0,4},{2,6},{4,0},{6,2},{8,12},{10,14},{12,8},{14,10},{16,20},{18,... | collective-permute-start | bytes 786440 | tf_op jit(solution)/shard_map/ppermute | solution.py:21
  22.8 13.7 %collective-permute-start.5 = (bf16[512,256]{1,0:T(8,128)(2,1)S(1)}, bf16[512,256]{1,0:T(8,128)(2,1)S(1)}, u32[]{:S(2)}, u32[]{:S(2)}) collective-permute-start(bf16[512,256]{1,0:T(8,128)(2,1)S(1)} %collective-permute-done.4), channel_id=1, source_target_pairs={{0,1},{1,0},{2,3},{3,2},{4,5},{5,4},{6,7},{7,6},{8,9},{9,8},{10,11... | collective-permute-start | bytes 786440 | tf_op jit(solution)/shard_map/ppermute | solution.py:21
  39.4 9.1 %collective-permute-start.26 = (f32[4,2,16,512]{3,2,1,0:T(8,128)S(1)}, f32[4,2,16,512]{3,2,1,0:T(8,128)S(1)}, u32[]{:S(2)}, u32[]{:S(2)}) collective-permute-start(f32[4,2,16,512]{3,2,1,0:T(8,128)S(1)} %dynamic-slice_bitcast_fusion), channel_id=1, source_target_pairs={{0,4},{2,6},{4,0},{6,2},{8,12},{10,14},{12,8},{14,10},{16,20},{18,... | collective-permute-start | bytes 786440 | tf_op jit(solution)/shard_map/ppermute | solution.py:21
  40.3 8.9 %collective-permute-start.24 = (f32[4,2,16,512]{3,2,1,0:T(8,128)S(1)}, f32[4,2,16,512]{3,2,1,0:T(8,128)S(1)}, u32[]{:S(2)}, u32[]{:S(2)}) collective-permute-start(f32[4,2,16,512]{3,2,1,0:T(8,128)S(1)} %dynamic-slice_bitcast_fusion.1), channel_id=1, source_target_pairs={{0,2},{2,0},{4,6},{6,4},{8,10},{10,8},{12,14},{14,12},{16,18},{18,... | collective-permute-start | bytes 786440 | tf_op jit(solution)/shard_map/ppermute | solution.py:21
  45.2 9.2 %collective-permute-start.12 = (f32[4,2,16,512]{3,2,1,0:T(8,128)S(1)}, f32[4,2,16,512]{3,2,1,0:T(8,128)S(1)}, u32[]{:S(2)}, u32[]{:S(2)}) collective-permute-start(f32[4,2,16,512]{3,2,1,0:T(8,128)S(1)} %dynamic-slice_bitcast_fusion.2), channel_id=1, source_target_pairs={{0,4},{2,6},{4,0},{6,2},{8,12},{10,14},{12,8},{14,10},{16,20},{18,... | collective-permute-start | bytes 786440 | tf_op jit(solution)/shard_map/ppermute | solution.py:21
  45.8 9.6 %collective-permute-start.10 = (f32[4,2,16,512]{3,2,1,0:T(8,128)S(1)}, f32[4,2,16,512]{3,2,1,0:T(8,128)S(1)}, u32[]{:S(2)}, u32[]{:S(2)}) collective-permute-start(f32[4,2,16,512]{3,2,1,0:T(8,128)S(1)} %dynamic-slice_bitcast_fusion.3), channel_id=1, source_target_pairs={{0,2},{2,0},{4,6},{6,4},{8,10},{10,8},{12,14},{14,12},{16,18},{18,... | collective-permute-start | bytes 786440 | tf_op jit(solution)/shard_map/ppermute | solution.py:21
  48.6 9.3 %collective-permute-start.27 = (f32[4,16,512]{2,1,0:T(8,128)S(1)}, f32[4,16,512]{2,1,0:T(8,128)S(1)}, u32[]{:S(2)}, u32[]{:S(2)}) collective-permute-start(f32[4,16,512]{2,1,0:T(8,128)S(1)} %dynamic-slice_bitcast_fusion.4), channel_id=1, source_target_pairs={{0,2},{2,0},{4,6},{6,4},{8,10},{10,8},{12,14},{14,12},{16,18},{18,... | collective-permute-start | bytes 393224 | tf_op jit(solution)/shard_map/ppermute | solution.py:21
  59.1 9.2 %collective-permute-start.29 = (f32[16,1024]{1,0:T(8,128)S(1)}, f32[16,1024]{1,0:T(8,128)S(1)}, u32[]{:S(2)}, u32[]{:S(2)}) collective-permute-start(f32[16,1024]{1,0:T(8,128)S(1)} %get-tuple-element.55), channel_id=1, source_target_pairs={{0,16},{2,18},{4,20},{6,22},{8,24},{10,26},{12,28},{14,30},{16,0},... | collective-permute-start | bytes 196616 | tf_op jit(solution)/shard_map/ppermute | solution.py:21
  62.5 11.4 %collective-permute-start.14 = (f32[16,1024]{1,0:T(8,128)S(1)}, f32[16,1024]{1,0:T(8,128)S(1)}, u32[]{:S(2)}, u32[]{:S(2)}) collective-permute-start(f32[16,1024]{1,0:T(8,128)S(1)} %get-tuple-element.57), channel_id=1, source_target_pairs={{0,8},{2,10},{4,12},{6,14},{8,0},{10,2},{12,4},{14,6},{16,24},{18,... | collective-permute-start | bytes 196616 | tf_op jit(solution)/shard_map/ppermute | solution.py:21
  62.7 13.5 %collective-permute-start.15 = (f32[16,1024]{1,0:T(8,128)S(1)}, f32[16,1024]{1,0:T(8,128)S(1)}, u32[]{:S(2)}, u32[]{:S(2)}) collective-permute-start(f32[16,1024]{1,0:T(8,128)S(1)} %get-tuple-element.58), channel_id=1, source_target_pairs={{0,16},{2,18},{4,20},{6,22},{8,24},{10,26},{12,28},{14,30},{16,0},... | collective-permute-start | bytes 196616 | tf_op jit(solution)/shard_map/ppermute | solution.py:21
  65.8 10.5 %collective-permute-start.16 = (f32[16,1024]{1,0:T(8,128)S(1)}, f32[16,1024]{1,0:T(8,128)S(1)}, u32[]{:S(2)}, u32[]{:S(2)}) collective-permute-start(f32[16,1024]{1,0:T(8,128)S(1)} %get-tuple-element.59), channel_id=1, source_target_pairs={{0,24},{2,26},{4,28},{6,30},{8,16},{10,18},{12,20},{14,22},{16,8},... | collective-permute-start | bytes 196616 | tf_op jit(solution)/shard_map/ppermute | solution.py:21
  69.0 10.0 %collective-permute-start.31 = (f32[16,1024]{1,0:T(8,128)S(1)}, f32[16,1024]{1,0:T(8,128)S(1)}, u32[]{:S(2)}, u32[]{:S(2)}) collective-permute-start(f32[16,1024]{1,0:T(8,128)S(1)} %get-tuple-element.40), channel_id=1, source_target_pairs={{0,8},{2,10},{4,12},{6,14},{8,0},{10,2},{12,4},{14,6},{16,24},{18,... | collective-permute-start | bytes 196616 | tf_op jit(solution)/shard_map/ppermute | solution.py:21
  81.5 9.2 %collective-permute-start.34 = (f32[4,16,1024]{2,1,0:T(8,128)S(1)}, f32[4,16,1024]{2,1,0:T(8,128)S(1)}, u32[]{:S(2)}, u32[]{:S(2)}) collective-permute-start(f32[4,16,1024]{2,1,0:T(8,128)S(1)} %pad_maximum_fusion.2.refs_0_), channel_id=1, source_target_pairs={{0,2},{2,0},{4,6},{6,4},{8,10},{10,8},{12,14},{14,12},{16,18},{18,... | collective-permute-start | bytes 786440 | tf_op jit(solution)/shard_map/ppermute | solution.py:21
  81.9 14.1 %collective-permute-start.35 = (f32[4,16,1024]{2,1,0:T(8,128)S(1)}, f32[4,16,1024]{2,1,0:T(8,128)S(1)}, u32[]{:S(2)}, u32[]{:S(2)}) collective-permute-start(f32[4,16,1024]{2,1,0:T(8,128)S(1)} %pad_maximum_fusion.2.refs_0_), channel_id=1, source_target_pairs={{0,4},{2,6},{4,0},{6,2},{8,12},{10,14},{12,8},{14,10},{16,20},{18,... | collective-permute-start | bytes 786440 | tf_op jit(solution)/shard_map/ppermute | solution.py:21
  82.1 13.9 %collective-permute-start.36 = (f32[4,16,1024]{2,1,0:T(8,128)S(1)}, f32[4,16,1024]{2,1,0:T(8,128)S(1)}, u32[]{:S(2)}, u32[]{:S(2)}) collective-permute-start(f32[4,16,1024]{2,1,0:T(8,128)S(1)} %pad_maximum_fusion.2.refs_0_), channel_id=1, source_target_pairs={{0,6},{2,4},{4,2},{6,0},{8,14},{10,12},{12,10},{14,8},{16,22},{18,... | collective-permute-start | bytes 786440 | tf_op jit(solution)/shard_map/ppermute | solution.py:21
  85.5 12.8 %collective-permute-start.20 = (f32[4,16,1024]{2,1,0:T(8,128)S(1)}, f32[4,16,1024]{2,1,0:T(8,128)S(1)}, u32[]{:S(2)}, u32[]{:S(2)}) collective-permute-start(f32[4,16,1024]{2,1,0:T(8,128)S(1)} %pad_maximum_fusion.1.refs_0_), channel_id=1, source_target_pairs={{0,2},{2,0},{4,6},{6,4},{8,10},{10,8},{12,14},{14,12},{16,18},{18,... | collective-permute-start | bytes 786440 | tf_op jit(solution)/shard_map/ppermute | solution.py:21
  85.5 16.0 %collective-permute-start.21 = (f32[4,16,1024]{2,1,0:T(8,128)S(1)}, f32[4,16,1024]{2,1,0:T(8,128)S(1)}, u32[]{:S(2)}, u32[]{:S(2)}) collective-permute-start(f32[4,16,1024]{2,1,0:T(8,128)S(1)} %pad_maximum_fusion.1.refs_0_), channel_id=1, source_target_pairs={{0,4},{2,6},{4,0},{6,2},{8,12},{10,14},{12,8},{14,10},{16,20},{18,... | collective-permute-start | bytes 786440 | tf_op jit(solution)/shard_map/ppermute | solution.py:21
  90.8 10.8 %collective-permute-start.22 = (f32[4,16,1024]{2,1,0:T(8,128)S(1)}, f32[4,16,1024]{2,1,0:T(8,128)S(1)}, u32[]{:S(2)}, u32[]{:S(2)}) collective-permute-start(f32[4,16,1024]{2,1,0:T(8,128)S(1)} %pad_maximum_fusion.1.refs_0_), channel_id=1, source_target_pairs={{0,6},{2,4},{4,2},{6,0},{8,14},{10,12},{12,10},{14,8},{16,22},{18,... | collective-permute-start | bytes 786440 | tf_op jit(solution)/shard_map/ppermute | solution.py:21
  103.5 9.2 %collective-permute-start.52 = (bf16[128,1024]{1,0:T(8,128)(2,1)S(1)}, bf16[128,1024]{1,0:T(8,128)(2,1)S(1)}, u32[]{:S(2)}, u32[]{:S(2)}) collective-permute-start(bf16[128,1024]{1,0:T(8,128)(2,1)S(1)} %get-tuple-element.30.refs_0_), channel_id=1, source_target_pairs={{0,2},{2,0},{4,6},{6,4},{8,10},{10,8},{12,14},{14,12},{16,18},{18,... | collective-permute-start | bytes 786440 | tf_op jit(solution)/shard_map/ppermute | solution.py:21
  105.0 13.4 %collective-permute-start.60 = (bf16[128,1024]{1,0:T(8,128)(2,1)S(1)}, bf16[128,1024]{1,0:T(8,128)(2,1)S(1)}, u32[]{:S(2)}, u32[]{:S(2)}) collective-permute-start(bf16[128,1024]{1,0:T(8,128)(2,1)S(1)} %get-tuple-element.30.refs_0_), channel_id=1, source_target_pairs={{0,8},{2,10},{4,12},{6,14},{8,0},{10,2},{12,4},{14,6},{16,24},{18,... | collective-permute-start | bytes 786440 | tf_op jit(solution)/shard_map/ppermute | solution.py:21
  106.6 12.6 %collective-permute-start.66 = (bf16[128,1024]{1,0:T(8,128)(2,1)S(1)}, bf16[128,1024]{1,0:T(8,128)(2,1)S(1)}, u32[]{:S(2)}, u32[]{:S(2)}) collective-permute-start(bf16[128,1024]{1,0:T(8,128)(2,1)S(1)} %get-tuple-element.30.refs_0_), channel_id=1, source_target_pairs={{0,4},{2,6},{4,0},{6,2},{8,12},{10,14},{12,8},{14,10},{16,20},{18,... | collective-permute-start | bytes 786440 | tf_op jit(solution)/shard_map/ppermute | solution.py:21
  107.1 15.4 %collective-permute-start.38 = (bf16[128,1024]{1,0:T(8,128)(2,1)S(1)}, bf16[128,1024]{1,0:T(8,128)(2,1)S(1)}, u32[]{:S(2)}, u32[]{:S(2)}) collective-permute-start(bf16[128,1024]{1,0:T(8,128)(2,1)S(1)} %get-tuple-element.30.refs_0_), channel_id=1, source_target_pairs={{0,16},{2,18},{4,20},{6,22},{8,24},{10,26},{12,28},{14,30},{16,0},... | collective-permute-start | bytes 786440 | tf_op jit(solution)/shard_map/ppermute | solution.py:21
  109.3 13.1 %collective-permute-start.42 = (bf16[128,1024]{1,0:T(8,128)(2,1)S(1)}, bf16[128,1024]{1,0:T(8,128)(2,1)S(1)}, u32[]{:S(2)}, u32[]{:S(2)}) collective-permute-start(bf16[128,1024]{1,0:T(8,128)(2,1)S(1)} %get-tuple-element.31.refs_4_), channel_id=1, source_target_pairs={{0,2},{2,0},{4,6},{6,4},{8,10},{10,8},{12,14},{14,12},{16,18},{18,... | collective-permute-start | bytes 786440 | tf_op jit(solution)/shard_map/ppermute | solution.py:21
  112.7 16.9 %collective-permute-start.63 = (bf16[128,1024]{1,0:T(8,128)(2,1)S(1)}, bf16[128,1024]{1,0:T(8,128)(2,1)S(1)}, u32[]{:S(2)}, u32[]{:S(2)}) collective-permute-start(bf16[128,1024]{1,0:T(8,128)(2,1)S(1)} %get-tuple-element.31.refs_4_), channel_id=1, source_target_pairs={{0,8},{2,10},{4,12},{6,14},{8,0},{10,2},{12,4},{14,6},{16,24},{18,... | collective-permute-start | bytes 786440 | tf_op jit(solution)/shard_map/ppermute | solution.py:21
  118.4 14.5 %collective-permute-start.45 = (bf16[128,1024]{1,0:T(8,128)(2,1)S(1)}, bf16[128,1024]{1,0:T(8,128)(2,1)S(1)}, u32[]{:S(2)}, u32[]{:S(2)}) collective-permute-start(bf16[128,1024]{1,0:T(8,128)(2,1)S(1)} %get-tuple-element.31.refs_4_), channel_id=1, source_target_pairs={{0,16},{2,18},{4,20},{6,22},{8,24},{10,26},{12,28},{14,30},{16,0},... | collective-permute-start | bytes 786440 | tf_op jit(solution)/shard_map/ppermute | solution.py:21
  119.2 13.6 %collective-permute-start.67 = (bf16[128,1024]{1,0:T(8,128)(2,1)S(1)}, bf16[128,1024]{1,0:T(8,128)(2,1)S(1)}, u32[]{:S(2)}, u32[]{:S(2)}) collective-permute-start(bf16[128,1024]{1,0:T(8,128)(2,1)S(1)} %get-tuple-element.31.refs_4_), channel_id=1, source_target_pairs={{0,4},{2,6},{4,0},{6,2},{8,12},{10,14},{12,8},{14,10},{16,20},{18,... | collective-permute-start | bytes 786440 | tf_op jit(solution)/shard_map/ppermute | solution.py:21
  122.5 14.2 %collective-permute-start.56 = (bf16[128,1024]{1,0:T(8,128)(2,1)S(1)}, bf16[128,1024]{1,0:T(8,128)(2,1)S(1)}, u32[]{:S(2)}, u32[]{:S(2)}) collective-permute-start(bf16[128,1024]{1,0:T(8,128)(2,1)S(1)} %collective-permute-done.38.refs_2_), channel_id=1, source_target_pairs={{0,8},{2,10},{4,12},{6,14},{8,0},{10,2},{12,4},{14,6},{16,24},{18,... | collective-permute-start | bytes 786440 | tf_op jit(solution)/shard_map/ppermute | solution.py:21
  122.5 14.5 %collective-permute-start.61 = (bf16[128,1024]{1,0:T(8,128)(2,1)S(1)}, bf16[128,1024]{1,0:T(8,128)(2,1)S(1)}, u32[]{:S(2)}, u32[]{:S(2)}) collective-permute-start(bf16[128,1024]{1,0:T(8,128)(2,1)S(1)} %collective-permute-done.60.refs_3_), channel_id=1, source_target_pairs={{0,2},{2,0},{4,6},{6,4},{8,10},{10,8},{12,14},{14,12},{16,18},{18,... | collective-permute-start | bytes 786440 | tf_op jit(solution)/shard_map/ppermute | solution.py:21
  129.6 9.1 %collective-permute-start.62 = (bf16[128,1024]{1,0:T(8,128)(2,1)S(1)}, bf16[128,1024]{1,0:T(8,128)(2,1)S(1)}, u32[]{:S(2)}, u32[]{:S(2)}) collective-permute-start(bf16[128,1024]{1,0:T(8,128)(2,1)S(1)} %collective-permute-done.60.refs_3_), channel_id=1, source_target_pairs={{0,4},{2,6},{4,0},{6,2},{8,12},{10,14},{12,8},{14,10},{16,20},{18,... | collective-permute-start | bytes 786440 | tf_op jit(solution)/shard_map/ppermute | solution.py:21
  132.9 9.2 %collective-permute-start.64 = (bf16[128,1024]{1,0:T(8,128)(2,1)S(1)}, bf16[128,1024]{1,0:T(8,128)(2,1)S(1)}, u32[]{:S(2)}, u32[]{:S(2)}) collective-permute-start(bf16[128,1024]{1,0:T(8,128)(2,1)S(1)} %collective-permute-done.63.refs_7_), channel_id=1, source_target_pairs={{0,2},{2,0},{4,6},{6,4},{8,10},{10,8},{12,14},{14,12},{16,18},{18,... | collective-permute-start | bytes 786440 | tf_op jit(solution)/shard_map/ppermute | solution.py:21
  136.7 9.2 %collective-permute-start.65 = (bf16[128,1024]{1,0:T(8,128)(2,1)S(1)}, bf16[128,1024]{1,0:T(8,128)(2,1)S(1)}, u32[]{:S(2)}, u32[]{:S(2)}) collective-permute-start(bf16[128,1024]{1,0:T(8,128)(2,1)S(1)} %collective-permute-done.63.refs_7_), channel_id=1, source_target_pairs={{0,4},{2,6},{4,0},{6,2},{8,12},{10,14},{12,8},{14,10},{16,20},{18,... | collective-permute-start | bytes 786440 | tf_op jit(solution)/shard_map/ppermute | solution.py:21
  137.0 14.5 %collective-permute-start.39 = (bf16[128,1024]{1,0:T(8,128)(2,1)S(1)}, bf16[128,1024]{1,0:T(8,128)(2,1)S(1)}, u32[]{:S(2)}, u32[]{:S(2)}) collective-permute-start(bf16[128,1024]{1,0:T(8,128)(2,1)S(1)} %collective-permute-done.38.refs_2_), channel_id=1, source_target_pairs={{0,4},{2,6},{4,0},{6,2},{8,12},{10,14},{12,8},{14,10},{16,20},{18,... | collective-permute-start | bytes 786440 | tf_op jit(solution)/shard_map/ppermute | solution.py:21
  138.7 18.4 %collective-permute-start.53 = (bf16[128,1024]{1,0:T(8,128)(2,1)S(1)}, bf16[128,1024]{1,0:T(8,128)(2,1)S(1)}, u32[]{:S(2)}, u32[]{:S(2)}) collective-permute-start(bf16[128,1024]{1,0:T(8,128)(2,1)S(1)} %collective-permute-done.52.refs_1_), channel_id=1, source_target_pairs={{0,4},{2,6},{4,0},{6,2},{8,12},{10,14},{12,8},{14,10},{16,20},{18,... | collective-permute-start | bytes 786440 | tf_op jit(solution)/shard_map/ppermute | solution.py:21
  141.5 16.1 %collective-permute-start.55 = (bf16[128,1024]{1,0:T(8,128)(2,1)S(1)}, bf16[128,1024]{1,0:T(8,128)(2,1)S(1)}, u32[]{:S(2)}, u32[]{:S(2)}) collective-permute-start(bf16[128,1024]{1,0:T(8,128)(2,1)S(1)} %collective-permute-done.38.refs_2_), channel_id=1, source_target_pairs={{0,2},{2,0},{4,6},{6,4},{8,10},{10,8},{12,14},{14,12},{16,18},{18,... | collective-permute-start | bytes 786440 | tf_op jit(solution)/shard_map/ppermute | solution.py:21
  142.1 20.7 %collective-permute-start.49 = (bf16[128,1024]{1,0:T(8,128)(2,1)S(1)}, bf16[128,1024]{1,0:T(8,128)(2,1)S(1)}, u32[]{:S(2)}, u32[]{:S(2)}) collective-permute-start(bf16[128,1024]{1,0:T(8,128)(2,1)S(1)} %collective-permute-done.45.refs_6_), channel_id=1, source_target_pairs={{0,4},{2,6},{4,0},{6,2},{8,12},{10,14},{12,8},{14,10},{16,20},{18,... | collective-permute-start | bytes 786440 | tf_op jit(solution)/shard_map/ppermute | solution.py:21
  145.9 20.1 %collective-permute-start.43 = (bf16[128,1024]{1,0:T(8,128)(2,1)S(1)}, bf16[128,1024]{1,0:T(8,128)(2,1)S(1)}, u32[]{:S(2)}, u32[]{:S(2)}) collective-permute-start(bf16[128,1024]{1,0:T(8,128)(2,1)S(1)} %collective-permute-done.42.refs_5_), channel_id=1, source_target_pairs={{0,4},{2,6},{4,0},{6,2},{8,12},{10,14},{12,8},{14,10},{16,20},{18,... | collective-permute-start | bytes 786440 | tf_op jit(solution)/shard_map/ppermute | solution.py:21
  151.5 14.9 %collective-permute-start.59 = (bf16[128,1024]{1,0:T(8,128)(2,1)S(1)}, bf16[128,1024]{1,0:T(8,128)(2,1)S(1)}, u32[]{:S(2)}, u32[]{:S(2)}) collective-permute-start(bf16[128,1024]{1,0:T(8,128)(2,1)S(1)} %collective-permute-done.45.refs_6_), channel_id=1, source_target_pairs={{0,2},{2,0},{4,6},{6,4},{8,10},{10,8},{12,14},{14,12},{16,18},{18,... | collective-permute-start | bytes 786440 | tf_op jit(solution)/shard_map/ppermute | solution.py:21
  157.1 10.7 %collective-permute-start.40 = (bf16[128,1024]{1,0:T(8,128)(2,1)S(1)}, bf16[128,1024]{1,0:T(8,128)(2,1)S(1)}, u32[]{:S(2)}, u32[]{:S(2)}) collective-permute-start(bf16[128,1024]{1,0:T(8,128)(2,1)S(1)} %collective-permute-done.39.refs_3_), channel_id=1, source_target_pairs={{0,2},{2,0},{4,6},{6,4},{8,10},{10,8},{12,14},{14,12},{16,18},{18,... | collective-permute-start | bytes 786440 | tf_op jit(solution)/shard_map/ppermute | solution.py:21
  157.6 10.8 %collective-permute-start.54 = (bf16[128,1024]{1,0:T(8,128)(2,1)S(1)}, bf16[128,1024]{1,0:T(8,128)(2,1)S(1)}, u32[]{:S(2)}, u32[]{:S(2)}) collective-permute-start(bf16[128,1024]{1,0:T(8,128)(2,1)S(1)} %collective-permute-done.53.refs_0_), channel_id=1, source_target_pairs={{0,8},{2,10},{4,12},{6,14},{8,0},{10,2},{12,4},{14,6},{16,24},{18,... | collective-permute-start | bytes 786440 | tf_op jit(solution)/shard_map/ppermute | solution.py:21
  162.7 8.8 %collective-permute-start.57 = (bf16[128,1024]{1,0:T(8,128)(2,1)S(1)}, bf16[128,1024]{1,0:T(8,128)(2,1)S(1)}, u32[]{:S(2)}, u32[]{:S(2)}) collective-permute-start(bf16[128,1024]{1,0:T(8,128)(2,1)S(1)} %collective-permute-done.56.refs_3_), channel_id=1, source_target_pairs={{0,2},{2,0},{4,6},{6,4},{8,10},{10,8},{12,14},{14,12},{16,18},{18,... | collective-permute-start | bytes 786440 | tf_op jit(solution)/shard_map/ppermute | solution.py:21
  166.4 10.7 %collective-permute-start.50 = (bf16[128,1024]{1,0:T(8,128)(2,1)S(1)}, bf16[128,1024]{1,0:T(8,128)(2,1)S(1)}, u32[]{:S(2)}, u32[]{:S(2)}) collective-permute-start(bf16[128,1024]{1,0:T(8,128)(2,1)S(1)} %collective-permute-done.49.refs_9_), channel_id=1, source_target_pairs={{0,2},{2,0},{4,6},{6,4},{8,10},{10,8},{12,14},{14,12},{16,18},{18,... | collective-permute-start | bytes 786440 | tf_op jit(solution)/shard_map/ppermute | solution.py:21
  167.8 15.7 %collective-permute-start.47 = (bf16[128,1024]{1,0:T(8,128)(2,1)S(1)}, bf16[128,1024]{1,0:T(8,128)(2,1)S(1)}, u32[]{:S(2)}, u32[]{:S(2)}) collective-permute-start(bf16[128,1024]{1,0:T(8,128)(2,1)S(1)} %collective-permute-done.46.refs_7_), channel_id=1, source_target_pairs={{0,2},{2,0},{4,6},{6,4},{8,10},{10,8},{12,14},{14,12},{16,18},{18,... | collective-permute-start | bytes 786440 | tf_op jit(solution)/shard_map/ppermute | solution.py:21
  168.4 15.0 %collective-permute-start.48 = (bf16[128,1024]{1,0:T(8,128)(2,1)S(1)}, bf16[128,1024]{1,0:T(8,128)(2,1)S(1)}, u32[]{:S(2)}, u32[]{:S(2)}) collective-permute-start(bf16[128,1024]{1,0:T(8,128)(2,1)S(1)} %collective-permute-done.46.refs_7_), channel_id=1, source_target_pairs={{0,4},{2,6},{4,0},{6,2},{8,12},{10,14},{12,8},{14,10},{16,20},{18,... | collective-permute-start | bytes 786440 | tf_op jit(solution)/shard_map/ppermute | solution.py:21
  171.5 11.9 %collective-permute-start.44 = (bf16[128,1024]{1,0:T(8,128)(2,1)S(1)}, bf16[128,1024]{1,0:T(8,128)(2,1)S(1)}, u32[]{:S(2)}, u32[]{:S(2)}) collective-permute-start(bf16[128,1024]{1,0:T(8,128)(2,1)S(1)} %collective-permute-done.43.refs_7_), channel_id=1, source_target_pairs={{0,8},{2,10},{4,12},{6,14},{8,0},{10,2},{12,4},{14,6},{16,24},{18,... | collective-permute-start | bytes 786440 | tf_op jit(solution)/shard_map/ppermute | solution.py:21
  177.2 9.0 %collective-permute-start.51 = (bf16[128,1024]{1,0:T(8,128)(2,1)S(1)}, bf16[128,1024]{1,0:T(8,128)(2,1)S(1)}, u32[]{:S(2)}, u32[]{:S(2)}) collective-permute-start(bf16[128,1024]{1,0:T(8,128)(2,1)S(1)} %collective-permute-done.50.refs_10_), channel_id=1, source_target_pairs={{0,8},{2,10},{4,12},{6,14},{8,0},{10,2},{12,4},{14,6},{16,24},{18,... | collective-permute-start | bytes 786440 | tf_op jit(solution)/shard_map/ppermute | solution.py:21
  (30 other events, 290.6 us)
